TPU v7x, 256 devices: a whole 4x4x8 slice. The times are simulated.
256 devices in a mesh: ep: 32 (over z, x), tp: 8 (over y, core).
Axes of the slice: x: 4, y: 4, z: 8, core: 2. Of those that a mesh axis runs over, the one named last changes fastest.
Arguments:
- stream: bfloat16 [8192, 3072], P('ep'), may hold values from -30 to 30
- ffn_gain: bfloat16 [3072], replicated, may hold values from 0.099609375 to 1.8984375
- chosen: int32 [32, 1024], replicated, may hold values from 0 to 8191, as said below
- affinity: float32 [32, 1024], P('ep'), may hold values from 0.5 to 2
- w_gate: bfloat16 [32, 3072, 3072], P('ep', None, 'tp'), may hold values from -0.109375 to 0.109375
- w_up: bfloat16 [32, 3072, 3072], P('ep', None, 'tp'), may hold values from -0.109375 to 0.109375
- w_down: bfloat16 [32, 3072, 3072], P('ep', 'tp'), may hold values from -0.109375 to 0.109375
- final_gain: bfloat16 [3072], P('tp'), may hold values from 0.099609375 to 1.8984375
Outputs:
- normed: bfloat16 [8192, 3072], P('ep', 'tp')
Inputs may be any that keep to these rules, and one draw needn't show every extreme that they name: `chosen`: row e holds 1024 distinct token numbers in ascending order. Of the 256 tokens of one index of ep, each expert reads at least one and at most 48; in every draw some expert reads exactly 48 from some index.
All inputs are finite; a program needn't handle non-finite values.
Results may differ from a plain program's by a relative error of at most 0.015.
Values may be sent and summed in bfloat16 or wider, within the bound.
No kernel may reach another device: no remote copies, remote signals or barrier semaphores. Data moves between devices by JAX's collectives and lax.ppermute only.
A program may use at most 128 MiB of HBM per device.

v0:
```python
import jax
import jax.numpy as jnp
from jax import lax
from jax.sharding import PartitionSpec as P

EPSILON = 1e-06


def sent_to_all(array, axis):
    devices = lax.axis_size(axis)
    return lax.all_to_all(
        jnp.broadcast_to(array[None], (devices, *array.shape)), axis, 0, 0, tiled=True
    )


def over_copies(array, axis):
    return sent_to_all(array, axis).sum(axis=0)


def on_device(stream, ffn_gain, chosen, affinity, w_gate, w_up, w_down, final_gain):
    tok_rows = stream.shape[0]
    model_width = stream.shape[1]
    experts = chosen.shape[0]
    picks = chosen.shape[1]
    ep_count = lax.axis_size("ep")
    tp_count = lax.axis_size("tp")
    device = lax.axis_index("ep")
    column = lax.axis_index("tp")
    share_width = model_width // tp_count
    slots = 3 * tok_rows // 16
    widened = stream.astype(jnp.float32)
    scale_in = lax.rsqrt(jnp.mean(widened * widened, axis=-1, keepdims=True) + EPSILON)
    normed_in = (widened * scale_in * ffn_gain.astype(jnp.float32)).astype(jnp.bfloat16)
    source = chosen // tok_rows
    counts = jnp.sum(
        (source[:, :, None] == jnp.arange(ep_count)[None, None, :]).astype(jnp.int32), axis=1
    )
    starts = jnp.cumsum(counts, axis=1) - counts
    slot_range = jnp.arange(slots, dtype=jnp.int32)
    own_start = jnp.take(starts, device, axis=1)
    own_count = jnp.take(counts, device, axis=1)
    send_pos = jnp.clip(own_start[:, None] + slot_range[None, :], 0, picks - 1)
    send_valid = slot_range[None, :] < own_count[:, None]
    local_tok = jnp.where(
        send_valid, jnp.take_along_axis(chosen, send_pos, axis=1) - device * tok_rows, 0
    )
    local_flat = local_tok.reshape(-1)
    row_source = jnp.take(source, device, axis=0)
    row_starts = jnp.take(starts, device, axis=0)
    arrival = (
        row_source * slots + jnp.arange(picks, dtype=jnp.int32) - jnp.take(row_starts, row_source)
    )
    gate_rows = w_gate[0]
    up_rows = w_up[0]
    own_columns = lax.dynamic_slice_in_dim(normed_in, column * share_width, share_width, 1)
    outgoing = jnp.take(own_columns, local_flat, axis=0).reshape(experts, slots, share_width)
    arrived = lax.all_to_all(outgoing, "ep", split_axis=0, concat_axis=0, tiled=True)
    shared = jnp.take(arrived.reshape(-1, share_width), arrival, axis=0)
    piece = lax.all_gather(shared, "tp", axis=1, tiled=True)
    gate = jnp.dot(piece, gate_rows, preferred_element_type=jnp.float32)
    up = jnp.dot(piece, up_rows, preferred_element_type=jnp.float32)
    hidden = (jax.nn.silu(gate) * up).astype(jnp.bfloat16)
    down_rows = w_down[0]
    piece = down_rows
    expert_cols = lax.psum_scatter(
        lax.dot_general(
            piece, hidden, (((0,), (1,)), ((), ())), preferred_element_type=jnp.float32
        ).astype(jnp.bfloat16),
        "tp",
        scatter_dimension=0,
        tiled=True,
    ).astype(jnp.float32)
    weighted = (expert_cols * affinity[0][None, :]).astype(jnp.bfloat16)
    slot_pos = jnp.clip(row_starts[:, None] + slot_range[None, :], 0, picks - 1)
    leaving = jnp.take(weighted, slot_pos.reshape(-1), axis=1).reshape(share_width, ep_count, slots)
    returned = lax.all_to_all(leaving, "ep", split_axis=1, concat_axis=1, tiled=True)
    placing = (
        (local_flat[:, None] == jnp.arange(tok_rows, dtype=jnp.int32)[None, :])
        & send_valid.reshape(-1)[:, None]
    ).astype(jnp.bfloat16)
    update = lax.dot_general(
        placing,
        returned.reshape(share_width, -1),
        (((0,), (1,)), ((), ())),
        preferred_element_type=jnp.float32,
    )
    own_stream = lax.dynamic_slice_in_dim(widened, column * share_width, share_width, 1)
    merged = own_stream + update
    totals = over_copies(jnp.sum(merged * merged, axis=1), "tp")
    scale_out = lax.rsqrt(totals[:, None] / model_width + EPSILON)
    return (merged * scale_out * final_gain.astype(jnp.float32)[None, :]).astype(jnp.bfloat16)


def solution(mesh):
    return jax.shard_map(
        on_device,
        mesh=mesh,
        in_specs=(
            P("ep", None),
            P(),
            P(),
            P("ep", None),
            P("ep", None, "tp"),
            P("ep", None, "tp"),
            P("ep", "tp", None),
            P("tp"),
        ),
        out_specs=P("ep", "tp"),
        check_vma=False,
    )
```

profile of v0, /device:TPU:32, one launch (start us, length us, event | category | flops | bytes accessed | tf_op | source)
XLA Modules:
  0.0 271.6 jit_solution(4535225694800903247)
XLA Ops:
  6.5 2.0 multiply_reduce_fusion
  8.6 2.0 convert_element_type.34
  13.4 12.6 %gather_fusion.3 = s32[1536]{0:T(1024)S(1)} fusion(s32[32,1024]{1,0:T(8,128)S(1)} %copy-done.1, s32[1536]{0:T(1024)S(1)} %reshape.527), kind=kCustom, calls=%fused_computation.3 | custom fusion | bytes 24576 | tf_op jit(solution)/shard_map/jit(take_along_axis)/gather | solution.py:45
  28.3 5.3 %gather_fusion = bf16[1536,384]{1,0:T(8,128)(2,1)} fusion(bf16[256,384]{1,0:T(8,128)(2,1)S(1)} %multiply_convert_fusion.3, s32[2048]{0:T(1024)S(1)} %pad_clamp_fusion.1), kind=kCustom, calls=%fused_computation | custom fusion | bytes 2365440 | tf_op jit(solution)/shard_map/jit(_take)/gather | solution.py:56
  33.6 2.6 broadcast_select_fusion
  36.1 11.2 %all-to-all-start = ((bf16[32,48,384]{2,1,0:T(8,128)(2,1)}), bf16[32,48,384]{2,1,0:T(8,128)(2,1)S(1)}, u32[]{:S(2)}, u32[]{:S(2)}) async-start(bf16[32,48,384]{2,1,0:T(8,128)(2,1)} %broadcast_select_fusion), calls=%async_computation | async-start | bytes 2359296 | tf_op jit(solution)/shard_map/all_to_all | solution.py:57
  48.8 4.9 %compare_select_fusion.10 = (s32[1024,1]{0,1:T(1,128)S(1)}, s32[1024,1]{0,1:T(1,128)S(1)}, s32[1,1024]{1,0:T(1,128)S(1)}) fusion(s32[]{:T(128)} %bitcast.28, s32[]{:T(128)} %bitcast.29, s32[]{:T(128)} %bitcast.30, s32[]{:T(128)} %bitcast.31, s32[]{:T(128)} %bitcast.32, s32[]{:T(128)} %bitcast.34, s32[]{:T(128)} %bitcast.33, s32[32,1024]{1,0:T(8,128)} %copy-done.3, ...), kind=kLoop, calls=%fused_computation.80 | loop fusion | flops 16384 | bytes 16417 | tf_op jit(solution)/shard_map/jit(_take)/gather | solution.py:51
  54.7 16.2 %compare_and_fusion.2 = (pred[1024]{0:T(1024)(128)(4,1)}, s32[1024]{0:T(1024)S(1)}) fusion(s32[1024]{0:T(1024)S(1)} %bitcast.88, pred[1024]{0:T(1024)(128)(4,1)S(1)} %get-tuple-element.63, pred[1024]{0:T(1024)(128)(4,1)S(1)} %get-tuple-element.61, pred[1024]{0:T(1024)(128)(4,1)S(1)} %get-tuple-element.62, pred[1024]{0:T(1024)(128)(4,1)S(1)} %get-tuple-element.60, ...), kind=kLoop, calls=%fused_computation.101 | loop fusion | flops 41984 | bytes 39012 | tf_op jit(solution)/shard_map/jit(_take)/and | solution.py:58
  70.9 6.4 %all-to-all-done = bf16[32,48,384]{2,1,0:T(8,128)(2,1)S(1)} async-done(((bf16[32,48,384]{2,1,0:T(8,128)(2,1)}), bf16[32,48,384]{2,1,0:T(8,128)(2,1)S(1)}, u32[]{:S(2)}, u32[]{:S(2)}) %all-to-all-start) | async-done | bytes 1179680 | tf_op jit(solution)/shard_map/all_to_all | solution.py:57
  77.3 5.0 %gather_fusion.1 = bf16[1024,384]{1,0:T(8,128)(2,1)} fusion(bf16[1536,384]{1,0:T(8,128)(2,1)S(1)} %bitcast.84, s32[1024]{0:T(1024)S(1)} %broadcast_clamp_fusion), kind=kCustom, calls=%fused_computation.1 | custom fusion | bytes 1576960 | tf_op jit(solution)/shard_map/jit(_take)/gather | solution.py:58
  82.3 2.2 broadcast_select_fusion.2
  84.6 41.3 %all-gather.2.cloned.1.call-done = bf16[1024,3072]{1,0:T(8,128)(2,1)} async-done(((bf16[1024,384]{1,0:T(8,128)(2,1)}), bf16[1024,3072]{1,0:T(8,128)(2,1)}) %all-gather.2.cloned.1.call-update) | async-done | bytes 6291472 | tf_op jit(solution)/shard_map/all_gather | solution.py:59
  125.9 8.0 %fusion.3 = f32[1024,384]{1,0:T(8,128)} fusion(bf16[1024,3072]{1,0:T(8,128)(2,1)} %all-gather.2.cloned.1.call-done, bf16[1,3072,384]{2,1,0:T(8,128)(2,1)} %param.14), kind=kOutput, calls=%fused_computation.11 | convolution fusion | flops 2415919104 | bytes 10223616 | tf_op jit(solution)/shard_map/dot_general | solution.py:60
  133.9 11.4 %convert_bitcast_fusion = bf16[3072,1024]{0,1:T(8,128)(2,1)} fusion(bf16[1,384,3072]{2,1,0:T(8,128)(2,1)S(1)} %copy-done, f32[1024,384]{1,0:T(8,128)} %fusion.3, bf16[1024,3072]{1,0:T(8,128)(2,1)} %all-gather.2.cloned.1.call-done, bf16[1,3072,384]{2,1,0:T(8,128)(2,1)} %param.15), kind=kOutput, calls=%fused_computation.4 | convolution fusion | flops 4837343232 | bytes 18874368 | tf_op jit(solution)/shard_map/dot_general | solution.py:66
  145.3 8.7 %copy.10 = bf16[3072,1024]{1,0:T(8,128)(2,1)} copy(bf16[3072,1024]{0,1:T(8,128)(2,1)} %convert_bitcast_fusion) | data formatting | bytes 12582912
  155.0 44.3 %reduce-scatter.4.cloned.1.call-done = bf16[384,1024]{1,0:T(8,128)(2,1)} async-done(((bf16[3072,1024]{1,0:T(8,128)(2,1)}), bf16[384,1024]{1,0:T(8,128)(2,1)}) %reduce-scatter.4.cloned.1.call-update) | async-done | bytes 786448
  199.4 2.3 copy.11
  203.0 5.3 %gather_fusion.2 = bf16[1536,384]{1,0:T(8,128)(2,1)} fusion(bf16[384,1024]{0,1:T(8,128)(2,1)S(1)} %multiply_convert_fusion, s32[2048]{0:T(1024)S(1)} %pad_clamp_fusion), kind=kCustom, calls=%fused_computation.2 | custom fusion | bytes 2365440 | tf_op jit(solution)/shard_map/jit(_take)/gather | solution.py:75
  208.3 2.6 broadcast_select_fusion.1
  210.8 10.0 %all-to-all-start.1 = ((bf16[384,32,48]{0,2,1:T(8,128)(2,1)}), bf16[384,32,48]{0,2,1:T(8,128)(2,1)S(1)}, u32[]{:S(2)}, u32[]{:S(2)}) async-start(bf16[384,32,48]{0,2,1:T(8,128)(2,1)} %broadcast_select_fusion.1), calls=%async_computation.1 | async-start | bytes 2359296 | tf_op jit(solution)/shard_map/all_to_all | solution.py:76
  225.7 24.7 %all-to-all-done.1 = bf16[384,32,48]{0,2,1:T(8,128)(2,1)S(1)} async-done(((bf16[384,32,48]{0,2,1:T(8,128)(2,1)}), bf16[384,32,48]{0,2,1:T(8,128)(2,1)S(1)}, u32[]{:S(2)}, u32[]{:S(2)}) %all-to-all-start.1) | async-done | bytes 1179680 | tf_op jit(solution)/shard_map/all_to_all | solution.py:76
  250.3 2.9 %multiply_reduce_fusion.1 = (f32[256]{0:T(256)S(1)}, f32[256,384]{1,0:T(8,128)}) fusion(bf16[384,1536]{0,1:T(8,128)(2,1)S(1)} %bitcast.87, s32[1536]{0:T(1024)} %subtract_select_fusion, pred[1536]{0:T(1024)(128)(4,1)} %lt.182, f32[256,3072]{1,0:T(8,128)} %convert_element_type.34, s32[]{:T(128)S(6)} %select_n.231), kind=kOutput, calls=%fused_computation.25 | convolution fusion | flops 303070976 | bytes 1974788 | tf_op jit(solution)/shard_map/dot_general | solution.py:81
  253.8 3.8 %all-to-all-start.2 = ((f32[8,1,256]{2,1,0:T(1,128)}), f32[8,1,256]{2,1,0:T(1,128)S(1)}, u32[]{:S(2)}, u32[]{:S(2)}) async-start(f32[8,1,256]{2,1,0:T(1,128)} %broadcast_in_dim.111), calls=%async_computation.2 | async-start | bytes 16384 | tf_op jit(solution)/shard_map/all_to_all | solution.py:11
  257.6 5.3 %all-to-all-done.2 = f32[8,1,256]{2,1,0:T(1,128)S(1)} async-done(((f32[8,1,256]{2,1,0:T(1,128)}), f32[8,1,256]{2,1,0:T(1,128)S(1)}, u32[]{:S(2)}, u32[]{:S(2)}) %all-to-all-start.2) | async-done | bytes 8224 | tf_op jit(solution)/shard_map/all_to_all | solution.py:11
  (62 shorter events, 17.1 us)
Async XLA Ops:
  6.5 127.4 %copy-start = (bf16[1,384,3072]{2,1,0:T(8,128)(2,1)S(1)}, bf16[1,384,3072]{2,1,0:T(8,128)(2,1)}, u32[]{:S(2)}) copy-start(bf16[1,384,3072]{2,1,0:T(8,128)(2,1)} %param.16) | copy-start | bytes 7077892
  6.5 2.0 copy-start.2
  8.6 2.1 copy-start.1
  10.8 0.7 copy-start.3
  12.3 13.7 %copy-start.5 = (s32[32,32]{1,0:T(8,128)}, s32[32,32]{1,0:T(8,128)S(1)}, u32[]{:S(2)}) copy-start(s32[32,32]{1,0:T(8,128)S(1)} %sub.52) | copy-start | bytes 12292
  12.7 0.6 copy-start.4
  36.1 41.2 %all-to-all-start = ((bf16[32,48,384]{2,1,0:T(8,128)(2,1)}), bf16[32,48,384]{2,1,0:T(8,128)(2,1)S(1)}, u32[]{:S(2)}, u32[]{:S(2)}) async-start(bf16[32,48,384]{2,1,0:T(8,128)(2,1)} %broadcast_select_fusion), calls=%async_computation | async-start | bytes 2359296 | tf_op jit(solution)/shard_map/all_to_all | solution.py:57
  47.3 78.6 %all-gather.2.cloned.1.call-start = ((), (), s32[]{:S(2)}) async-start(), calls=%async_computation.4 | async-start | bytes 7077888 | tf_op jit(solution)/shard_map/all_gather | solution.py:59
  84.5 114.8 %reduce-scatter.4.cloned.1.call-start = ((), (), s32[]{:S(2)}) async-start(), calls=%async_computation.5 | async-start | bytes 7077888
  154.0 47.6 %copy-start.6 = (f32[1,1024]{1,0:T(1,128)S(1)}, f32[1,1024]{1,0:T(1,128)}, u32[]{:S(2)}) copy-start(f32[1,1024]{1,0:T(1,128)} %param.13) | copy-start | bytes 12292
  210.8 39.5 %all-to-all-start.1 = ((bf16[384,32,48]{0,2,1:T(8,128)(2,1)}), bf16[384,32,48]{0,2,1:T(8,128)(2,1)S(1)}, u32[]{:S(2)}, u32[]{:S(2)}) async-start(bf16[384,32,48]{0,2,1:T(8,128)(2,1)} %broadcast_select_fusion.1), calls=%async_computation.1 | async-start | bytes 2359296 | tf_op jit(solution)/shard_map/all_to_all | solution.py:76
  225.7 32.0 %copy-start.7 = (bf16[384]{0:T(512)(128)(2,1)S(1)}, bf16[384]{0:T(512)(128)(2,1)}, u32[]{:S(2)}) copy-start(bf16[384]{0:T(512)(128)(2,1)} %param.17) | copy-start | bytes 2308
  253.8 9.1 %all-to-all-start.2 = ((f32[8,1,256]{2,1,0:T(1,128)}), f32[8,1,256]{2,1,0:T(1,128)S(1)}, u32[]{:S(2)}, u32[]{:S(2)}) async-start(f32[8,1,256]{2,1,0:T(1,128)} %broadcast_in_dim.111), calls=%async_computation.2 | async-start | bytes 16384 | tf_op jit(solution)/shard_map/all_to_all | solution.py:11
Sparse Core Ops, SparseCore 0:
  84.7 41.1 all-gather.1
  154.1 45.1 reduce-scatter.3
where the time goes:
time: 275 us; the launch traced here: 272 us
  waiting for transfers between devices  122 us (44%)
  local copies, waits for them, and re-layouts  47.3 us (17%)
  other arithmetic  41.2 us (15%)
  starting transfers between devices  25.1 us (9%)
  matrix products  22.3 us (8%)
  between operations  13.6 us (5%)
    unnamed x3, waiting for transfers between devices  44.4 us
    all_gather x1, waiting for transfers between devices, on_device(): piece = lax.all_gather(shared, 'tp', axis=1, tiled=True)  41.3 us
    all_to_all x1, waiting for transfers between devices, on_device(): lax.all_to_all(leaving, 'ep', split_axis=1, concat_axis=1, tiled=True)  24.7 us
    and x1, other arithmetic, on_device(): shared = jnp.take(arrived.reshape(-1, share_width), arrival, axis=0)  16.2 us
    gather x3, local copies, waits for them, and re-layouts, on_device(): jnp.take_along_axis(chosen, send_pos, axis=1) - device * tok_rows  12.8 us
    unnamed x18, local copies, waits for them, and re-layouts  12.3 us
    dot_general x1, matrix products, on_device(): lax.dot_general(piece, hidden, (((0,), (1,)), ((), ())), preferred_elemen...  11.4 us
    all_to_all x1, starting transfers between devices, on_device(): lax.all_to_all(outgoing, 'ep', split_axis=0, concat_axis=0, tiled=True)  11.2 us
  transfers between devices with their start and end apart: 5, of which 5 were waited for; matrix products, arithmetic and copies ran while one was open for 11% of the time, Pallas kernels for 0%

commit v1 on v0

v1 whole, which is shorter than its diff:
```python
import functools

import jax
import jax.numpy as jnp
from jax import lax
from jax.experimental import pallas as pl
from jax.experimental.pallas import tpu as pltpu
from jax.sharding import PartitionSpec as P

EPSILON = 1e-06
LANES = 128
F32 = jnp.float32
BF16 = jnp.bfloat16


def exchanged(array, axis, mask):
    devices = lax.axis_size(axis)
    return lax.ppermute(array, axis, [(i, i ^ mask) for i in range(devices)])


def cost(flops, moved):
    return pl.CostEstimate(flops=int(flops), bytes_accessed=int(moved), transcendentals=0)


def shape_of(shape, dtype):
    return jax.ShapeDtypeStruct(shape, dtype)


def whole(shape):
    return pl.BlockSpec(shape, lambda *_: (0,) * len(shape))


def send_kernel(chunks, column_ref, stream_ref, own_ref, gain_ref, sel_ref, *out_refs):
    x = stream_ref[...].astype(F32)
    scale = lax.rsqrt(jnp.mean(x * x, axis=-1, keepdims=True) + EPSILON)
    own = (own_ref[...].astype(F32) * scale * gain_ref[...].astype(F32)).astype(BF16)
    tokens = own.shape[0]
    sel = sel_ref[...]
    hit = lax.broadcasted_iota(jnp.int32, (tokens, sel.shape[1]), 0) == sel
    placed = jnp.where(hit, 1.0, 0.0).astype(BF16)
    rows = lax.dot_general(
        placed, own, (((0,), (0,)), ((), ())), preferred_element_type=F32
    ).astype(BF16)
    for j in range(chunks):
        out_refs[j][...] = rows[:, j * LANES : (j + 1) * LANES]


def outgoing_rows(column, stream, gain, sel, share, chunks):
    tokens, width = stream.shape
    slots = sel.shape[1]
    return pl.pallas_call(
        functools.partial(send_kernel, chunks),
        grid_spec=pltpu.PrefetchScalarGridSpec(
            num_scalar_prefetch=1,
            grid=(1,),
            in_specs=[
                whole((tokens, width)),
                pl.BlockSpec((tokens, share), lambda i, col: (0, col[0])),
                pl.BlockSpec((1, share), lambda i, col: (0, col[0])),
                whole((1, slots)),
            ],
            out_specs=[whole((slots, LANES))] * chunks,
        ),
        out_shape=[shape_of((slots, LANES), BF16)] * chunks,
        cost_estimate=cost(2 * slots * tokens * share, 2 * tokens * width + 2 * slots * share),
        name="send_rows",
    )(column, stream, stream, gain, sel)


def compact_kernel(inv_ref, arrived_ref, out_ref):
    tile, slots = out_ref.shape[0], inv_ref.shape[1]
    at = lax.broadcasted_iota(jnp.int32, (tile, slots), 0) + pl.program_id(0) * tile
    hit = jnp.where(at == inv_ref[...], 1.0, 0.0).astype(BF16)
    out_ref[...] = jnp.dot(hit, arrived_ref[...], preferred_element_type=F32).astype(BF16)


def compacted(inv, arrived, picks):
    slots, width = arrived.shape
    tile = 256
    return pl.pallas_call(
        compact_kernel,
        grid=(picks // tile,),
        in_specs=[whole((1, slots)), whole((slots, width))],
        out_specs=pl.BlockSpec((tile, width), lambda i: (i, 0)),
        out_shape=shape_of((picks, width), BF16),
        cost_estimate=cost(2 * picks * slots * width, 2 * slots * width),
        name="compact_rows",
    )(inv, arrived)


ORDER = (0, 1, 2, 3, 6, 7)


def ffn_kernel(first, last, group_ref, *refs):
    pieces = refs[:6]
    halves = refs[6:10]
    gates = refs[10:18]
    ups = refs[18:26]
    rest = refs[26:]
    upper = pl.program_id(0) >= pl.num_programs(0) // 2
    far = [jnp.where(upper, halves[2 * k + 1][...], halves[2 * k][...]) for k in range(2)]
    by_mask = {mask: pieces[i][...] for i, mask in enumerate(ORDER)}
    by_mask[4], by_mask[5] = far
    units = gates[0].shape[1]
    total = None
    for pair in range(4):
        low, high = 2 * pair, 2 * pair + 1
        left = jnp.concatenate([by_mask[low], by_mask[high]], axis=1)
        weights = jnp.concatenate(
            [
                jnp.concatenate([gates[low][...], gates[high][...]], axis=0),
                jnp.concatenate([ups[low][...], ups[high][...]], axis=0),
            ],
            axis=1,
        )
        part = jnp.dot(left, weights, preferred_element_type=F32)
        total = part if total is None else total + part
    if not first:
        total = total + rest[0][...]
    out_ref = rest[-1]
    if last:
        gate, up = total[:, :units], total[:, units:]
        out_ref[...] = (gate / (1.0 + jnp.exp(-gate)) * up).astype(BF16)
    else:
        out_ref[...] = total


def ffn_chunk(group, pieces, halves, w_gate, w_up, acc, chunk, chunks, last):
    picks = pieces[0].shape[0]
    units = w_gate.shape[1]
    tile = 256
    steps = picks // tile
    first = acc is None
    row_spec = pl.BlockSpec((tile, LANES), lambda i, g: (i, 0))
    low_spec = pl.BlockSpec((tile, LANES), lambda i, g: (jnp.minimum(i, steps // 2 - 1), 0))
    high_spec = pl.BlockSpec((tile, LANES), lambda i, g: (jnp.maximum(i - steps // 2, 0), 0))

    def weight_spec(mask):
        return pl.BlockSpec((LANES, units), lambda i, g: ((g[0] ^ mask) * chunks + chunk, 0))

    weight_specs = [weight_spec(mask) for mask in range(8)]
    acc_spec = pl.BlockSpec((tile, 2 * units), lambda i, g: (i, 0))
    out_width, out_type = (units, BF16) if last else (2 * units, F32)
    return pl.pallas_call(
        functools.partial(ffn_kernel, first, last),
        grid_spec=pltpu.PrefetchScalarGridSpec(
            num_scalar_prefetch=1,
            grid=(steps,),
            in_specs=[row_spec] * 6
            + [low_spec, high_spec] * 2
            + weight_specs * 2
            + ([] if first else [acc_spec]),
            out_specs=pl.BlockSpec((tile, out_width), lambda i, g: (i, 0)),
        ),
        out_shape=shape_of((picks, out_width), out_type),
        input_output_aliases={} if first or last else {27: 0},
        cost_estimate=cost(2 * picks * 8 * LANES * 2 * units, 12 * picks * units),
        name="gate_up",
    )(group, *pieces, *halves, *([w_gate] * 8), *([w_up] * 8), *([] if first else [acc]))


def down_kernel(group_ref, hidden_ref, *refs):
    weights, (keep_ref, give_ref) = refs[:8], refs[8:]
    hidden = hidden_ref[...]
    for k, out_ref in enumerate((keep_ref, give_ref)):
        side = jnp.concatenate([weights[2 * d + k][...] for d in range(4)], axis=1)
        out_ref[...] = jnp.dot(hidden, side, preferred_element_type=F32).astype(BF16)


def down_chunk(group, hidden, w_down, chunk, chunks):
    picks, units = hidden.shape
    tile = 256

    def weight_spec(mask):
        return pl.BlockSpec((units, LANES), lambda i, g: (0, (g[0] ^ mask) * chunks + chunk))

    row_spec = pl.BlockSpec((tile, 4 * LANES), lambda i, g: (i, 0))
    return pl.pallas_call(
        down_kernel,
        grid_spec=pltpu.PrefetchScalarGridSpec(
            num_scalar_prefetch=1,
            grid=(picks // tile,),
            in_specs=[pl.BlockSpec((tile, units), lambda i, g: (i, 0))]
            + [weight_spec(mask) for mask in range(8)],
            out_specs=[row_spec, row_spec],
        ),
        out_shape=[shape_of((picks, 4 * LANES), BF16)] * 2,
        cost_estimate=cost(2 * picks * 8 * LANES * units, 16 * picks * LANES),
        name="down",
    )(group, hidden, *([w_down] * 8))


def pair_kernel(keep_ref, came_ref, a_keep, a_send, b_keep, b_send):
    total = (keep_ref[...].astype(F32) + came_ref[...].astype(F32)).astype(BF16)
    half = total.shape[0] // 2
    block = [total[:, d * LANES : (d + 1) * LANES] for d in range(4)]
    for ref, masks, low in (
        (a_keep, (0, 3), True),
        (a_send, (1, 2), True),
        (b_keep, (0, 1), False),
        (b_send, (3, 2), False),
    ):
        for n, d in enumerate(masks):
            rows = block[d][:half] if low else block[d][half:]
            ref[:, n * LANES : (n + 1) * LANES] = rows


def pair_sums(keep, came):
    picks = keep.shape[0]
    half = (picks // 2, 2 * LANES)
    return pl.pallas_call(
        pair_kernel,
        out_shape=[shape_of(half, BF16)] * 4,
        cost_estimate=cost(picks * 4 * LANES, 3 * picks * 4 * LANES * 2),
        name="pair_sums",
    )(keep, came)


def quad_kernel(a_keep, a_came, b_keep, b_came, a_own, a_next, b_own, b_next):
    for keep, came, own, following in (
        (a_keep, a_came, a_own, a_next),
        (b_keep, b_came, b_own, b_next),
    ):
        total = keep[...].astype(F32) + came[...].astype(F32)
        own[...] = total[:, :LANES]
        following[...] = total[:, LANES:].astype(BF16)


def quad_sums(a_keep, a_came, b_keep, b_came):
    half = a_keep.shape[0]
    kinds = [shape_of((half, LANES), F32), shape_of((half, LANES), BF16)]
    return pl.pallas_call(
        quad_kernel,
        out_shape=kinds * 2,
        cost_estimate=cost(half * 4 * LANES, half * LANES * 20),
        name="quad_sums",
    )(a_keep, a_came, b_keep, b_came)


def leave_kernel(a_own, a_came, b_own, b_came, weight_ref, arrival_ref, out_ref, rows_ref):
    half = a_own.shape[0]

    @pl.when(pl.program_id(0) == 0)
    def _():
        weight = weight_ref[...]
        top = (a_own[...] + a_came[...].astype(F32)) * weight[:half]
        low = (b_own[...] + b_came[...].astype(F32)) * weight[half:]
        rows_ref[:half] = top.astype(BF16)
        rows_ref[half:] = low.astype(BF16)

    tile, picks = out_ref.shape[0], arrival_ref.shape[1]
    at = lax.broadcasted_iota(jnp.int32, (tile, picks), 0) + pl.program_id(0) * tile
    hit = jnp.where(at == arrival_ref[...], 1.0, 0.0).astype(BF16)
    out_ref[...] = jnp.dot(hit, rows_ref[...], preferred_element_type=F32).astype(BF16)


def leaving_rows(a_own, a_came, b_own, b_came, weight, arrival, slots):
    half = a_own.shape[0]
    tile = 256
    return pl.pallas_call(
        leave_kernel,
        grid=(slots // tile,),
        in_specs=[whole((half, LANES))] * 4 + [whole((2 * half, 1)), whole((1, 2 * half))],
        out_specs=pl.BlockSpec((tile, LANES), lambda i: (i, 0)),
        out_shape=shape_of((slots, LANES), BF16),
        scratch_shapes=[pltpu.VMEM((2 * half, LANES), BF16)],
        cost_estimate=cost(4 * slots * half * LANES, 2 * slots * LANES),
        name="leave_rows",
    )(a_own, a_came, b_own, b_came, weight, arrival)


def merge_kernel(chunks, column_ref, own_ref, sel_ref, *refs):
    returned, (merged_ref, square_ref) = refs[:chunks], refs[chunks:]
    tokens = own_ref.shape[0]
    sel = sel_ref[...]
    hit = lax.broadcasted_iota(jnp.int32, (tokens, sel.shape[1]), 0) == sel
    placed = jnp.where(hit, 1.0, 0.0).astype(BF16)
    came = jnp.concatenate([ref[...] for ref in returned], axis=1)
    merged = own_ref[...].astype(F32) + jnp.dot(placed, came, preferred_element_type=F32)
    merged_ref[...] = merged
    square_ref[...] = jnp.sum(merged * merged, axis=1, keepdims=True)


def merged_rows(column, stream, sel, returned, share):
    tokens = stream.shape[0]
    slots = sel.shape[1]
    chunks = len(returned)
    return pl.pallas_call(
        functools.partial(merge_kernel, chunks),
        grid_spec=pltpu.PrefetchScalarGridSpec(
            num_scalar_prefetch=1,
            grid=(1,),
            in_specs=[
                pl.BlockSpec((tokens, share), lambda i, col: (0, col[0])),
                whole((1, slots)),
            ]
            + [whole((slots, LANES))] * chunks,
            out_specs=[whole((tokens, share)), whole((tokens, 1))],
        ),
        out_shape=[shape_of((tokens, share), F32), shape_of((tokens, 1), F32)],
        cost_estimate=cost(2 * slots * tokens * share, 2 * slots * share),
        name="merge_rows",
    )(column, stream, sel, *returned)


def on_device(stream, ffn_gain, chosen, affinity, w_gate, w_up, w_down, final_gain):
    tok_rows, model_width = stream.shape
    experts, picks = chosen.shape
    ep_count = lax.axis_size("ep")
    tp_count = lax.axis_size("tp")
    device = lax.axis_index("ep")
    column = lax.axis_index("tp").astype(jnp.int32)
    share = model_width // tp_count
    chunks = share // LANES
    slots = 3 * tok_rows // 16
    group = column.reshape(1)

    base = device * tok_rows
    begin = jnp.sum((chosen < base).astype(jnp.int32), axis=1)
    end = jnp.sum((chosen < base + tok_rows).astype(jnp.int32), axis=1)
    slot_range = jnp.arange(slots, dtype=jnp.int32)
    places = jnp.arange(picks, dtype=jnp.int32)
    want = begin[:, None] + slot_range[None, :]
    found = jnp.sum(
        jnp.where(places[None, None, :] == want[:, :, None], chosen[:, None, :], 0), axis=2
    )
    sel = jnp.where(want < end[:, None], found - base, -1).reshape(1, experts * slots)

    row = lax.dynamic_index_in_dim(chosen, device, 0, keepdims=True)
    edges = jnp.arange(ep_count, dtype=jnp.int32)[:, None] * tok_rows
    starts = jnp.sum((row < edges).astype(jnp.int32), axis=1)
    stops = jnp.sum((row < edges + tok_rows).astype(jnp.int32), axis=1)
    row_want = starts[:, None] + slot_range[None, :]
    inv = jnp.where(row_want < stops[:, None], row_want, -1).reshape(1, ep_count * slots)
    mine = (row >= edges) & (row < edges + tok_rows)
    arrival = jnp.sum(
        jnp.where(
            mine,
            jnp.arange(ep_count, dtype=jnp.int32)[:, None] * slots
            + places[None, :]
            - starts[:, None],
            0,
        ),
        axis=0,
        keepdims=True,
    )
    weight = affinity.reshape(picks, 1)

    half = picks // 2
    gate_rows, up_rows, down_rows = w_gate[0], w_up[0], w_down[0]
    outgoing = outgoing_rows(group, stream, ffn_gain.reshape(1, -1), sel, share, chunks)
    hidden = None
    for j in range(chunks):
        arrived = lax.all_to_all(
            outgoing[j].reshape(experts, slots, LANES), "ep", split_axis=0, concat_axis=0, tiled=True
        )
        own = compacted(inv, arrived.reshape(-1, LANES), picks)
        near = exchanged(own, "tp", 2)
        back = exchanged(own, "tp", 6)
        far_low = exchanged(near[:half], "tp", 6)
        far_high = exchanged(back[half:], "tp", 2)
        pieces = []
        for piece in (own, near, back):
            pieces += [piece, exchanged(piece, "tp", 1)]
        halves = [far_low, far_high, exchanged(far_low, "tp", 1), exchanged(far_high, "tp", 1)]
        hidden = ffn_chunk(
            group, pieces, halves, gate_rows, up_rows, hidden, j, chunks, j == chunks - 1
        )
    returned = []
    for j in range(chunks):
        keep, give = down_chunk(group, hidden, down_rows, j, chunks)
        a_keep, a_send, b_keep, b_send = pair_sums(keep, exchanged(give, "tp", 1))
        a_own, a_next, b_own, b_next = quad_sums(
            a_keep, exchanged(a_send, "tp", 2), b_keep, exchanged(b_send, "tp", 6)
        )
        leaving = leaving_rows(
            a_own,
            exchanged(a_next, "tp", 6),
            b_own,
            exchanged(b_next, "tp", 2),
            weight,
            arrival,
            ep_count * slots,
        )
        came = lax.all_to_all(
            leaving.reshape(ep_count, slots, LANES), "ep", split_axis=0, concat_axis=0, tiled=True
        )
        returned.append(came.reshape(-1, LANES))
    merged, squares = merged_rows(group, stream, sel, returned, share)
    totals = squares.reshape(1, tok_rows)
    for mask in (1, 2, 6):
        totals = totals + exchanged(totals, "tp", mask)
    scale_out = lax.rsqrt(totals.reshape(tok_rows, 1) / model_width + EPSILON)
    return (merged * scale_out * final_gain.astype(F32)[None, :]).astype(BF16)


def solution(mesh):
    return jax.shard_map(
        on_device,
        mesh=mesh,
        in_specs=(
            P("ep", None),
            P(),
            P(),
            P("ep", None),
            P("ep", None, "tp"),
            P("ep", None, "tp"),
            P("ep", "tp", None),
            P("tp"),
        ),
        out_specs=P("ep", "tp"),
        check_vma=False,
    )
```

time: 275 us -> 290 us (1.055)
  Pallas kernels: 0 us -> 77 us
  waiting for transfers between devices: 122 us -> 67 us
  blocking collectives: 0 us -> 47.8 us
  starting transfers between devices: 25.1 us -> 70.8 us
  local copies, waits for them, and re-layouts: 47.3 us -> 13.2 us
  other arithmetic: 41.2 us -> 7.85 us
  matrix products: 22.3 us -> 0 us
  between operations: 13.6 us -> 0.65 us
    pallas_call x0 -> x20, Pallas kernels: none -> 77 us  [the longest x3 18.9 us: ffn_chunk(): pl.pallas_call(functools.partial(ffn_kernel, first, last), grid_spec=pltp...]
    ppermute x0 -> x45, waiting for transfers between devices: none -> 53.9 us  [exchanged(): return lax.ppermute(array, axis, [(i, i ^ mask) for i in range(devices)])]
    all_to_all x0 -> x2, blocking collectives: none -> 47.8 us  [the longest x1 26 us: on_device(): lax.all_to_all(outgoing[j].reshape(experts, slots, LANES), 'ep', split_ax...]
    unnamed x3 -> x0, waiting for transfers between devices: 44.4 us -> none
    ppermute x0 -> x45, starting transfers between devices: none -> 42.1 us  [exchanged(): return lax.ppermute(array, axis, [(i, i ^ mask) for i in range(devices)])]
    all_gather x1 -> x0, waiting for transfers between devices: 41.3 us -> none  [on_device(): piece = lax.all_gather(shared, 'tp', axis=1, tiled=True)]
    gather x8 -> x0, local copies, waits for them, and re-layouts: 29.8 us -> none  [the longest x3 12.8 us: on_device(): jnp.take_along_axis(chosen, send_pos, axis=1) - device * tok_rows]
    all_to_all x3 -> x4, waiting for transfers between devices: 36.4 us -> 13.2 us  [the longest x2 13.2 us: on_device(): lax.all_to_all(outgoing[j].reshape(experts, slots, LANES), 'ep', split_ax...]
  transfers between devices with their start and end apart: 5 -> 49, of which waited for: 5 -> 25; matrix products, arithmetic and copies ran while one was open for 11% -> 1% of each run, Pallas kernels for 0% -> 21%
where the time goes in v1:
time: 290 us; the launch traced here: 284 us
  Pallas kernels  77 us (27%)
  starting transfers between devices  70.8 us (24%)
  waiting for transfers between devices  67 us (23%)
  blocking collectives  47.8 us (16%)
  local copies, waits for them, and re-layouts  13.2 us (5%)
  other arithmetic  7.85 us (3%)
    ppermute x45, waiting for transfers between devices, exchanged(): return lax.ppermute(array, axis, [(i, i ^ mask) for i in range(devices)])  53.9 us
    ppermute x45, starting transfers between devices, exchanged(): return lax.ppermute(array, axis, [(i, i ^ mask) for i in range(devices)])  42.1 us
    all_to_all x1, blocking collectives, on_device(): lax.all_to_all(outgoing[j].reshape(experts, slots, LANES), 'ep', split_ax...  26 us
    all_to_all x1, blocking collectives, on_device(): lax.all_to_all(leaving.reshape(ep_count, slots, LANES), 'ep', split_axis=...  21.8 us
    all_to_all x2, starting transfers between devices, on_device(): lax.all_to_all(leaving.reshape(ep_count, slots, LANES), 'ep', split_axis=...  19 us
    pallas_call x3, Pallas kernels, ffn_chunk(): pl.pallas_call(functools.partial(ffn_kernel, first, last), grid_spec=pltp...  18.9 us
    pallas_call x3, Pallas kernels, leaving_rows(): pl.pallas_call(leave_kernel, grid=(slots // tile,), in_specs=[whole((half...  13.9 us
    pallas_call x3, Pallas kernels, down_chunk(): pl.pallas_call(down_kernel, grid_spec=pltpu.PrefetchScalarGridSpec(num_sc...  13.8 us
  transfers between devices with their start and end apart: 49, of which 25 were waited for; matrix products, arithmetic and copies ran while one was open for 1% of the time, Pallas kernels for 21%

profile of v1, /device:TPU:32, one launch (start us, length us, event | category | flops | bytes accessed | tf_op | source)
XLA Modules:
  0.0 284.4 jit_solution(10573184474146003214)
XLA Ops:
  8.8 26.0 %all_to_all.30 = bf16[32,48,128]{2,1,0:T(8,128)(2,1)} all-to-all(bf16[32,48,128]{2,1,0:T(8,128)(2,1)} %bitcast.104), channel_id=1, replica_groups=mesh['ep'=32,'tp'=8] {'ep'}, dimensions={0} | all-to-all | bytes 786432 | tf_op jit(solution)/shard_map/all_to_all | solution.py:354
  34.8 4.9 %all-to-all-start.1 = ((bf16[32,48,128]{2,1,0:T(8,128)(2,1)}), bf16[32,48,128]{2,1,0:T(8,128)(2,1)S(1)}, u32[]{:S(2)}, u32[]{:S(2)}) async-start(bf16[32,48,128]{2,1,0:T(8,128)(2,1)} %bitcast.103), calls=%async_computation.1 | async-start | bytes 786432 | tf_op jit(solution)/shard_map/all_to_all | solution.py:354
  40.8 12.9 %all-to-all-done.1 = bf16[32,48,128]{2,1,0:T(8,128)(2,1)S(1)} async-done(((bf16[32,48,128]{2,1,0:T(8,128)(2,1)}), bf16[32,48,128]{2,1,0:T(8,128)(2,1)S(1)}, u32[]{:S(2)}, u32[]{:S(2)}) %all-to-all-start.1) | async-done | bytes 393248 | tf_op jit(solution)/shard_map/all_to_all | solution.py:354
  53.7 4.9 %all-to-all-start = ((bf16[32,48,128]{2,1,0:T(8,128)(2,1)}), bf16[32,48,128]{2,1,0:T(8,128)(2,1)S(1)}, u32[]{:S(2)}, u32[]{:S(2)}) async-start(bf16[32,48,128]{2,1,0:T(8,128)(2,1)} %bitcast.99), calls=%async_computation | async-start | bytes 786432 | tf_op jit(solution)/shard_map/all_to_all | solution.py:354
  81.9 3.9 %collective-permute-done.1.refs_2_ = bf16[1024,128]{1,0:T(8,128)(2,1)S(1)} collective-permute-done((bf16[1024,128]{1,0:T(8,128)(2,1)}, bf16[1024,128]{1,0:T(8,128)(2,1)S(1)}, u32[]{:S(2)}, u32[]{:S(2)}) %collective-permute-start.1) | collective-permute-done | bytes 262176 | tf_op jit(solution)/shard_map/ppermute | solution.py:18
  99.2 6.0 %gate_up.3.refs_26_ = f32[1024,768]{1,0:T(8,128)} custom-call(s32[1]{0:T(128)} %bitcast.column_ref.group_ref, bf16[1024,128]{1,0:T(8,128)(2,1)} %compact_rows.5.refs_0_, bf16[1024,128]{1,0:T(8,128)(2,1)} %copy-done.13, bf16[1024,128]{1,0:T(8,128)(2,1)} %copy-done.9, bf16[1024,128]{1,0:T(8,128)(2,1)} %copy-done.15, bf16[1024,128]{1,0:T(8,128)(2,1)} %copy-done.10, ...), custom_call_target="tpu_custom_call" | custom-call | flops 1610612736 | bytes 4718592 | tf_op jit(solution)/shard_map/gate_up/pallas_call | solution.py:144
  106.0 6.6 %gate_up.4.refs_26_ = f32[1024,768]{1,0:T(8,128)} custom-call(s32[1]{0:T(128)} %bitcast.column_ref.group_ref, bf16[1024,128]{1,0:T(8,128)(2,1)} %compact_rows.4.refs_0_, bf16[1024,128]{1,0:T(8,128)(2,1)} %copy-done.14, bf16[1024,128]{1,0:T(8,128)(2,1)} %copy-done.7, bf16[1024,128]{1,0:T(8,128)(2,1)} %copy-done.19, ...), custom_call_target="tpu_custom_call", output_to_operand_aliasing={{}: (27, {})} | custom-call | flops 1610612736 | bytes 4718592 | tf_op jit(solution)/shard_map/gate_up/pallas_call | solution.py:144
  113.5 6.3 %gate_up.5.hidden_ref = bf16[1024,384]{1,0:T(8,128)(2,1)} custom-call(s32[1]{0:T(128)} %bitcast.column_ref.group_ref, bf16[1024,128]{1,0:T(8,128)(2,1)} %compact_rows.3.refs_0_, bf16[1024,128]{1,0:T(8,128)(2,1)} %copy-done.16, bf16[1024,128]{1,0:T(8,128)(2,1)} %copy-done.5, bf16[1024,128]{1,0:T(8,128)(2,1)} %copy-done.18, bf16[1024,128]{1,0:T(8,128)(2,1)} %copy-done.6, ...), custom_call_target="tpu_custom_call" | custom-call | flops 1610612736 | bytes 4718592 | tf_op jit(solution)/shard_map/gate_up/pallas_call | solution.py:144
  119.8 4.6 %down.5 = (bf16[1024,512]{1,0:T(8,128)(2,1)}, bf16[1024,512]{1,0:T(8,128)(2,1)}) custom-call(s32[1]{0:T(128)} %bitcast.column_ref.group_ref, bf16[1024,384]{1,0:T(8,128)(2,1)} %gate_up.5.hidden_ref, bf16[384,3072]{1,0:T(8,128)(2,1)} %bitcast.69, bf16[384,3072]{1,0:T(8,128)(2,1)} %bitcast.70, bf16[384,3072]{1,0:T(8,128)(2,1)} %bitcast.71, ...), custom_call_target="tpu_custom_call" | custom-call | flops 805306368 | bytes 2097152 | tf_op jit(solution)/shard_map/down/pallas_call | solution.py:178
  124.8 4.5 %down.4 = (bf16[1024,512]{1,0:T(8,128)(2,1)}, bf16[1024,512]{1,0:T(8,128)(2,1)}) custom-call(s32[1]{0:T(128)} %bitcast.column_ref.group_ref, bf16[1024,384]{1,0:T(8,128)(2,1)} %gate_up.5.hidden_ref, bf16[384,3072]{1,0:T(8,128)(2,1)} %bitcast.80, bf16[384,3072]{1,0:T(8,128)(2,1)} %bitcast.78, bf16[384,3072]{1,0:T(8,128)(2,1)} %bitcast.79, ...), custom_call_target="tpu_custom_call" | custom-call | flops 805306368 | bytes 2097152 | tf_op jit(solution)/shard_map/down/pallas_call | solution.py:178
  133.1 10.9 %collective-permute-start.38 = (bf16[512,256]{1,0:T(8,128)(2,1)}, bf16[512,256]{1,0:T(8,128)(2,1)S(1)}, u32[]{:S(2)}, u32[]{:S(2)}) collective-permute-start(bf16[512,256]{1,0:T(8,128)(2,1)} %get-tuple-element.66), channel_id=1, source_target_pairs={{0,2},{1,3},{2,0},{3,1},{4,6},{5,7},{6,4},{7,5},{8,10},{9,11},{10,... | collective-permute-start | bytes 786440 | tf_op jit(solution)/shard_map/ppermute | solution.py:18
  145.3 6.1 %collective-permute-done.38.a_came = bf16[512,256]{1,0:T(8,128)(2,1)S(1)} collective-permute-done((bf16[512,256]{1,0:T(8,128)(2,1)}, bf16[512,256]{1,0:T(8,128)(2,1)S(1)}, u32[]{:S(2)}, u32[]{:S(2)}) %collective-permute-start.38) | collective-permute-done | bytes 262176 | tf_op jit(solution)/shard_map/ppermute | solution.py:18
  159.2 3.7 %collective-permute-done.40.a_came = bf16[512,128]{1,0:T(8,128)(2,1)S(1)} collective-permute-done((bf16[512,128]{1,0:T(8,128)(2,1)}, bf16[512,128]{1,0:T(8,128)(2,1)S(1)}, u32[]{:S(2)}, u32[]{:S(2)}) %collective-permute-start.40) | collective-permute-done | bytes 131104 | tf_op jit(solution)/shard_map/ppermute | solution.py:18
  164.0 4.6 %leave_rows.5 = bf16[1536,128]{1,0:T(8,128)(2,1)} custom-call(f32[512,128]{1,0:T(8,128)} %get-tuple-element.69.a_own, bf16[512,128]{1,0:T(8,128)(2,1)} %copy-done.38, f32[512,128]{1,0:T(8,128)} %get-tuple-element.71.b_own, bf16[512,128]{1,0:T(8,128)(2,1)} %copy-done.41, f32[1024,1]{1,0:T(8,128)} %copy.13.weight_ref, s32[1,1024]{1,0:T(1,128)} %bitcast.105), custom_call_target="tpu_custom_call" | custom-call | flops 402653184 | bytes 393216 | tf_op jit(solution)/shard_map/leave_rows/pallas_call | solution.py:260
  168.6 9.2 %all-to-all-start.5 = ((bf16[32,48,128]{2,1,0:T(8,128)(2,1)}), bf16[32,48,128]{2,1,0:T(8,128)(2,1)S(1)}, u32[]{:S(2)}, u32[]{:S(2)}) async-start(bf16[32,48,128]{2,1,0:T(8,128)(2,1)} %bitcast.95), calls=%async_computation.5 | async-start | bytes 786432 | tf_op jit(solution)/shard_map/all_to_all | solution.py:385
  177.8 4.6 %down.3 = (bf16[1024,512]{1,0:T(8,128)(2,1)}, bf16[1024,512]{1,0:T(8,128)(2,1)}) custom-call(s32[1]{0:T(128)} %bitcast.column_ref.group_ref, bf16[1024,384]{1,0:T(8,128)(2,1)} %gate_up.5.hidden_ref, bf16[384,3072]{1,0:T(8,128)(2,1)} %bitcast.85, bf16[384,3072]{1,0:T(8,128)(2,1)} %bitcast.86, bf16[384,3072]{1,0:T(8,128)(2,1)} %bitcast.87, ...), custom_call_target="tpu_custom_call" | custom-call | flops 805306368 | bytes 2097152 | tf_op jit(solution)/shard_map/down/pallas_call | solution.py:178
  187.7 7.3 %collective-permute-done.33.a_came = bf16[512,256]{1,0:T(8,128)(2,1)S(1)} collective-permute-done((bf16[512,256]{1,0:T(8,128)(2,1)}, bf16[512,256]{1,0:T(8,128)(2,1)S(1)}, u32[]{:S(2)}, u32[]{:S(2)}) %collective-permute-start.33) | collective-permute-done | bytes 262176 | tf_op jit(solution)/shard_map/ppermute | solution.py:18
  200.6 4.8 %collective-permute-done.35.a_came = bf16[512,128]{1,0:T(8,128)(2,1)S(1)} collective-permute-done((bf16[512,128]{1,0:T(8,128)(2,1)}, bf16[512,128]{1,0:T(8,128)(2,1)S(1)}, u32[]{:S(2)}, u32[]{:S(2)}) %collective-permute-start.35) | collective-permute-done | bytes 131104 | tf_op jit(solution)/shard_map/ppermute | solution.py:18
  206.5 4.6 %leave_rows.4 = bf16[1536,128]{1,0:T(8,128)(2,1)} custom-call(f32[512,128]{1,0:T(8,128)} %get-tuple-element.59.a_own, bf16[512,128]{1,0:T(8,128)(2,1)} %copy-done.40, f32[512,128]{1,0:T(8,128)} %get-tuple-element.61.b_own, bf16[512,128]{1,0:T(8,128)(2,1)} %copy-done.43, f32[1024,1]{1,0:T(8,128)} %copy.13.weight_ref, s32[1,1024]{1,0:T(1,128)} %bitcast.106), custom_call_target="tpu_custom_call" | custom-call | flops 402653184 | bytes 393216 | tf_op jit(solution)/shard_map/leave_rows/pallas_call | solution.py:260
  211.1 9.8 %all-to-all-start.4 = ((bf16[32,48,128]{2,1,0:T(8,128)(2,1)}), bf16[32,48,128]{2,1,0:T(8,128)(2,1)S(1)}, u32[]{:S(2)}, u32[]{:S(2)}) async-start(bf16[32,48,128]{2,1,0:T(8,128)(2,1)} %bitcast.96), calls=%async_computation.4 | async-start | bytes 786432 | tf_op jit(solution)/shard_map/all_to_all | solution.py:385
  226.2 4.9 %collective-permute-done.28.a_came = bf16[512,256]{1,0:T(8,128)(2,1)S(1)} collective-permute-done((bf16[512,256]{1,0:T(8,128)(2,1)}, bf16[512,256]{1,0:T(8,128)(2,1)S(1)}, u32[]{:S(2)}, u32[]{:S(2)}) %collective-permute-start.28) | collective-permute-done | bytes 262176 | tf_op jit(solution)/shard_map/ppermute | solution.py:18
  236.9 4.6 %collective-permute-done.30.a_came = bf16[512,128]{1,0:T(8,128)(2,1)S(1)} collective-permute-done((bf16[512,128]{1,0:T(8,128)(2,1)}, bf16[512,128]{1,0:T(8,128)(2,1)S(1)}, u32[]{:S(2)}, u32[]{:S(2)}) %collective-permute-start.30) | collective-permute-done | bytes 131104 | tf_op jit(solution)/shard_map/ppermute | solution.py:18
  242.6 4.6 %leave_rows.3 = bf16[1536,128]{1,0:T(8,128)(2,1)} custom-call(f32[512,128]{1,0:T(8,128)} %get-tuple-element.49.a_own, bf16[512,128]{1,0:T(8,128)(2,1)} %copy-done.39, f32[512,128]{1,0:T(8,128)} %get-tuple-element.51.b_own, bf16[512,128]{1,0:T(8,128)(2,1)} %copy-done.42, f32[1024,1]{1,0:T(8,128)} %copy.13.weight_ref, s32[1,1024]{1,0:T(1,128)} %bitcast.107), custom_call_target="tpu_custom_call" | custom-call | flops 402653184 | bytes 393216 | tf_op jit(solution)/shard_map/leave_rows/pallas_call | solution.py:260
  247.2 21.8 %all_to_all.31 = bf16[32,48,128]{2,1,0:T(8,128)(2,1)} all-to-all(bf16[32,48,128]{2,1,0:T(8,128)(2,1)} %bitcast.97), channel_id=1, replica_groups=mesh['ep'=32,'tp'=8] {'ep'}, dimensions={0} | all-to-all | bytes 786432 | tf_op jit(solution)/shard_map/all_to_all | solution.py:385
  (217 shorter events, 101.4 us)
Async XLA Ops:
  34.8 18.9 %all-to-all-start.1 = ((bf16[32,48,128]{2,1,0:T(8,128)(2,1)}), bf16[32,48,128]{2,1,0:T(8,128)(2,1)S(1)}, u32[]{:S(2)}, u32[]{:S(2)}) async-start(bf16[32,48,128]{2,1,0:T(8,128)(2,1)} %bitcast.103), calls=%async_computation.1 | async-start | bytes 786432 | tf_op jit(solution)/shard_map/all_to_all | solution.py:354
  53.7 18.6 %all-to-all-start = ((bf16[32,48,128]{2,1,0:T(8,128)(2,1)}), bf16[32,48,128]{2,1,0:T(8,128)(2,1)S(1)}, u32[]{:S(2)}, u32[]{:S(2)}) async-start(bf16[32,48,128]{2,1,0:T(8,128)(2,1)} %bitcast.99), calls=%async_computation | async-start | bytes 786432 | tf_op jit(solution)/shard_map/all_to_all | solution.py:354
  63.6 12.8 %collective-permute-start.19 = (bf16[1024,128]{1,0:T(8,128)(2,1)}, bf16[1024,128]{1,0:T(8,128)(2,1)S(1)}, u32[]{:S(2)}, u32[]{:S(2)}) collective-permute-start(bf16[1024,128]{1,0:T(8,128)(2,1)} %compact_rows.5.refs_0_), channel_id=1, source_target_pairs={{0,2},{1,3},{2,0},{3,1},{4,6},{5,7},{6,4},{7,5},{8,10},{9,11},{10,... | collective-permute-start | bytes 786440 | tf_op jit(solution)/shard_map/ppermute | solution.py:18
  65.2 12.8 %collective-permute-start.21 = (bf16[1024,128]{1,0:T(8,128)(2,1)}, bf16[1024,128]{1,0:T(8,128)(2,1)S(1)}, u32[]{:S(2)}, u32[]{:S(2)}) collective-permute-start(bf16[1024,128]{1,0:T(8,128)(2,1)} %compact_rows.5.refs_0_), channel_id=1, source_target_pairs={{0,6},{1,7},{2,4},{3,5},{4,2},{5,3},{6,0},{7,1},{8,14},{9,15},{10,... | collective-permute-start | bytes 786440 | tf_op jit(solution)/shard_map/ppermute | solution.py:18
  67.4 12.8 %collective-permute-start.18 = (bf16[1024,128]{1,0:T(8,128)(2,1)}, bf16[1024,128]{1,0:T(8,128)(2,1)S(1)}, u32[]{:S(2)}, u32[]{:S(2)}) collective-permute-start(bf16[1024,128]{1,0:T(8,128)(2,1)} %compact_rows.5.refs_0_), channel_id=1, source_target_pairs={{0,1},{1,0},{2,3},{3,2},{4,5},{5,4},{6,7},{7,6},{8,9},{9,8},{10,11... | collective-permute-start | bytes 786440 | tf_op jit(solution)/shard_map/ppermute | solution.py:18
  70.8 9.4 %collective-permute-start.10 = (bf16[1024,128]{1,0:T(8,128)(2,1)}, bf16[1024,128]{1,0:T(8,128)(2,1)S(1)}, u32[]{:S(2)}, u32[]{:S(2)}) collective-permute-start(bf16[1024,128]{1,0:T(8,128)(2,1)} %compact_rows.4.refs_0_), channel_id=1, source_target_pairs={{0,2},{1,3},{2,0},{3,1},{4,6},{5,7},{6,4},{7,5},{8,10},{9,11},{10,... | collective-permute-start | bytes 786440 | tf_op jit(solution)/shard_map/ppermute | solution.py:18
  71.4 10.1 %collective-permute-start.12 = (bf16[1024,128]{1,0:T(8,128)(2,1)}, bf16[1024,128]{1,0:T(8,128)(2,1)S(1)}, u32[]{:S(2)}, u32[]{:S(2)}) collective-permute-start(bf16[1024,128]{1,0:T(8,128)(2,1)} %compact_rows.4.refs_0_), channel_id=1, source_target_pairs={{0,6},{1,7},{2,4},{3,5},{4,2},{5,3},{6,0},{7,1},{8,14},{9,15},{10,... | collective-permute-start | bytes 786440 | tf_op jit(solution)/shard_map/ppermute | solution.py:18
  76.4 9.4 %collective-permute-start.1 = (bf16[1024,128]{1,0:T(8,128)(2,1)}, bf16[1024,128]{1,0:T(8,128)(2,1)S(1)}, u32[]{:S(2)}, u32[]{:S(2)}) collective-permute-start(bf16[1024,128]{1,0:T(8,128)(2,1)} %compact_rows.3.refs_0_), channel_id=1, source_target_pairs={{0,2},{1,3},{2,0},{3,1},{4,6},{5,7},{6,4},{7,5},{8,10},{9,11},{10,... | collective-permute-start | bytes 786440 | tf_op jit(solution)/shard_map/ppermute | solution.py:18
  78.0 10.3 %collective-permute-start.3 = (bf16[1024,128]{1,0:T(8,128)(2,1)}, bf16[1024,128]{1,0:T(8,128)(2,1)S(1)}, u32[]{:S(2)}, u32[]{:S(2)}) collective-permute-start(bf16[1024,128]{1,0:T(8,128)(2,1)} %compact_rows.3.refs_0_), channel_id=1, source_target_pairs={{0,6},{1,7},{2,4},{3,5},{4,2},{5,3},{6,0},{7,1},{8,14},{9,15},{10,... | collective-permute-start | bytes 786440 | tf_op jit(solution)/shard_map/ppermute | solution.py:18
  80.2 8.2 %collective-permute-start.9 = (bf16[1024,128]{1,0:T(8,128)(2,1)}, bf16[1024,128]{1,0:T(8,128)(2,1)S(1)}, u32[]{:S(2)}, u32[]{:S(2)}) collective-permute-start(bf16[1024,128]{1,0:T(8,128)(2,1)} %compact_rows.4.refs_0_), channel_id=1, source_target_pairs={{0,1},{1,0},{2,3},{3,2},{4,5},{5,4},{6,7},{7,6},{8,9},{9,8},{10,11... | collective-permute-start | bytes 786440 | tf_op jit(solution)/shard_map/ppermute | solution.py:18
  80.2 10.8 %collective-permute-start.23 = (bf16[512,128]{1,0:T(8,128)(2,1)S(1)}, bf16[512,128]{1,0:T(8,128)(2,1)S(1)}, u32[]{:S(2)}, u32[]{:S(2)}) collective-permute-start(bf16[512,128]{1,0:T(8,128)(2,1)S(1)} %slice.28), channel_id=1, source_target_pairs={{0,6},{1,7},{2,4},{3,5},{4,2},{5,3},{6,0},{7,1},{8,14},{9,15},{10,... | collective-permute-start | bytes 393224 | tf_op jit(solution)/shard_map/ppermute | solution.py:18
  81.5 11.0 %collective-permute-start.24 = (bf16[512,128]{1,0:T(8,128)(2,1)S(1)}, bf16[512,128]{1,0:T(8,128)(2,1)S(1)}, u32[]{:S(2)}, u32[]{:S(2)}) collective-permute-start(bf16[512,128]{1,0:T(8,128)(2,1)S(1)} %slice.29), channel_id=1, source_target_pairs={{0,2},{1,3},{2,0},{3,1},{4,6},{5,7},{6,4},{7,5},{8,10},{9,11},{10,... | collective-permute-start | bytes 393224 | tf_op jit(solution)/shard_map/ppermute | solution.py:18
  96.7 8.5 %collective-permute-start.11 = (bf16[1024,128]{1,0:T(8,128)(2,1)S(1)}, bf16[1024,128]{1,0:T(8,128)(2,1)S(1)}, u32[]{:S(2)}, u32[]{:S(2)}) collective-permute-start(bf16[1024,128]{1,0:T(8,128)(2,1)S(1)} %collective-permute-done.10.refs_2_), channel_id=1, source_target_pairs={{0,1},{1,0},{2,3},{3,2},{4,5},{5,4},{6,7},{7,6},{8,9},{9,8},{10,11... | collective-permute-start | bytes 786440 | tf_op jit(solution)/shard_map/ppermute | solution.py:18
  97.7 14.8 %collective-permute-start = (bf16[1024,128]{1,0:T(8,128)(2,1)}, bf16[1024,128]{1,0:T(8,128)(2,1)S(1)}, u32[]{:S(2)}, u32[]{:S(2)}) collective-permute-start(bf16[1024,128]{1,0:T(8,128)(2,1)} %compact_rows.3.refs_0_), channel_id=1, source_target_pairs={{0,1},{1,0},{2,3},{3,2},{4,5},{5,4},{6,7},{7,6},{8,9},{9,8},{10,11... | collective-permute-start | bytes 786440 | tf_op jit(solution)/shard_map/ppermute | solution.py:18
  98.2 14.4 %collective-permute-start.2 = (bf16[1024,128]{1,0:T(8,128)(2,1)S(1)}, bf16[1024,128]{1,0:T(8,128)(2,1)S(1)}, u32[]{:S(2)}, u32[]{:S(2)}) collective-permute-start(bf16[1024,128]{1,0:T(8,128)(2,1)S(1)} %collective-permute-done.1.refs_2_), channel_id=1, source_target_pairs={{0,1},{1,0},{2,3},{3,2},{4,5},{5,4},{6,7},{7,6},{8,9},{9,8},{10,11... | collective-permute-start | bytes 786440 | tf_op jit(solution)/shard_map/ppermute | solution.py:18
  98.4 14.2 %collective-permute-start.4 = (bf16[1024,128]{1,0:T(8,128)(2,1)S(1)}, bf16[1024,128]{1,0:T(8,128)(2,1)}, u32[]{:S(2)}, u32[]{:S(2)}) collective-permute-start(bf16[1024,128]{1,0:T(8,128)(2,1)S(1)} %collective-permute-done.3.refs_4_), channel_id=1, source_target_pairs={{0,1},{1,0},{2,3},{3,2},{4,5},{5,4},{6,7},{7,6},{8,9},{9,8},{10,11... | collective-permute-start | bytes 786440 | tf_op jit(solution)/shard_map/ppermute | solution.py:18
  129.3 53.1 %collective-permute-start.32 = (bf16[1024,512]{1,0:T(8,128)(2,1)}, bf16[1024,512]{1,0:T(8,128)(2,1)S(1)}, u32[]{:S(2)}, u32[]{:S(2)}) collective-permute-start(bf16[1024,512]{1,0:T(8,128)(2,1)} %get-tuple-element.54), channel_id=1, source_target_pairs={{0,1},{1,0},{2,3},{3,2},{4,5},{5,4},{6,7},{7,6},{8,9},{9,8},{10,11... | collective-permute-start | bytes 3145736 | tf_op jit(solution)/shard_map/ppermute | solution.py:18
  133.1 18.3 %collective-permute-start.38 = (bf16[512,256]{1,0:T(8,128)(2,1)}, bf16[512,256]{1,0:T(8,128)(2,1)S(1)}, u32[]{:S(2)}, u32[]{:S(2)}) collective-permute-start(bf16[512,256]{1,0:T(8,128)(2,1)} %get-tuple-element.66), channel_id=1, source_target_pairs={{0,2},{1,3},{2,0},{3,1},{4,6},{5,7},{6,4},{7,5},{8,10},{9,11},{10,... | collective-permute-start | bytes 786440 | tf_op jit(solution)/shard_map/ppermute | solution.py:18
  144.0 9.7 %collective-permute-start.39 = (bf16[512,256]{1,0:T(8,128)(2,1)}, bf16[512,256]{1,0:T(8,128)(2,1)S(1)}, u32[]{:S(2)}, u32[]{:S(2)}) collective-permute-start(bf16[512,256]{1,0:T(8,128)(2,1)} %get-tuple-element.68), channel_id=1, source_target_pairs={{0,6},{1,7},{2,4},{3,5},{4,2},{5,3},{6,0},{7,1},{8,14},{9,15},{10,... | collective-permute-start | bytes 786440 | tf_op jit(solution)/shard_map/ppermute | solution.py:18
  168.6 42.5 %all-to-all-start.5 = ((bf16[32,48,128]{2,1,0:T(8,128)(2,1)}), bf16[32,48,128]{2,1,0:T(8,128)(2,1)S(1)}, u32[]{:S(2)}, u32[]{:S(2)}) async-start(bf16[32,48,128]{2,1,0:T(8,128)(2,1)} %bitcast.95), calls=%async_computation.5 | async-start | bytes 786432 | tf_op jit(solution)/shard_map/all_to_all | solution.py:385
  182.4 38.5 %collective-permute-start.27 = (bf16[1024,512]{1,0:T(8,128)(2,1)}, bf16[1024,512]{1,0:T(8,128)(2,1)S(1)}, u32[]{:S(2)}, u32[]{:S(2)}) collective-permute-start(bf16[1024,512]{1,0:T(8,128)(2,1)} %get-tuple-element.44), channel_id=1, source_target_pairs={{0,1},{1,0},{2,3},{3,2},{4,5},{5,4},{6,7},{7,6},{8,9},{9,8},{10,11... | collective-permute-start | bytes 3145736 | tf_op jit(solution)/shard_map/ppermute | solution.py:18
  186.1 8.9 %collective-permute-start.33 = (bf16[512,256]{1,0:T(8,128)(2,1)}, bf16[512,256]{1,0:T(8,128)(2,1)S(1)}, u32[]{:S(2)}, u32[]{:S(2)}) collective-permute-start(bf16[512,256]{1,0:T(8,128)(2,1)} %get-tuple-element.56), channel_id=1, source_target_pairs={{0,2},{1,3},{2,0},{3,1},{4,6},{5,7},{6,4},{7,5},{8,10},{9,11},{10,... | collective-permute-start | bytes 786440 | tf_op jit(solution)/shard_map/ppermute | solution.py:18
  186.1 10.1 %collective-permute-start.34 = (bf16[512,256]{1,0:T(8,128)(2,1)}, bf16[512,256]{1,0:T(8,128)(2,1)S(1)}, u32[]{:S(2)}, u32[]{:S(2)}) collective-permute-start(bf16[512,256]{1,0:T(8,128)(2,1)} %get-tuple-element.58), channel_id=1, source_target_pairs={{0,6},{1,7},{2,4},{3,5},{4,2},{5,3},{6,0},{7,1},{8,14},{9,15},{10,... | collective-permute-start | bytes 786440 | tf_op jit(solution)/shard_map/ppermute | solution.py:18
  211.1 36.1 %all-to-all-start.4 = ((bf16[32,48,128]{2,1,0:T(8,128)(2,1)}), bf16[32,48,128]{2,1,0:T(8,128)(2,1)S(1)}, u32[]{:S(2)}, u32[]{:S(2)}) async-start(bf16[32,48,128]{2,1,0:T(8,128)(2,1)} %bitcast.96), calls=%async_computation.4 | async-start | bytes 786432 | tf_op jit(solution)/shard_map/all_to_all | solution.py:385
  (71 other events, 521.5 us)

commit v2 on v1

v2 whole, which is shorter than its diff:
```python
import functools

import jax
import jax.numpy as jnp
from jax import lax
from jax.experimental import pallas as pl
from jax.experimental.pallas import tpu as pltpu
from jax.sharding import PartitionSpec as P

EPSILON = 1e-06
F32 = jnp.float32
BF16 = jnp.bfloat16


def exchanged(array, axis, mask):
    devices = lax.axis_size(axis)
    return lax.ppermute(array, axis, [(i, i ^ mask) for i in range(devices)])


def cost(flops, moved):
    return pl.CostEstimate(flops=int(flops), bytes_accessed=int(moved), transcendentals=0)


PARAMS = pltpu.CompilerParams(vmem_limit_bytes=28 * 1024 * 1024)


def shape_of(shape, dtype):
    return jax.ShapeDtypeStruct(shape, dtype)


def whole(shape):
    return pl.BlockSpec(shape, lambda *_: (0,) * len(shape))


def send_kernel(column_ref, stream_ref, own_ref, gain_ref, sel_ref, out_ref):
    x = stream_ref[...].astype(F32)
    scale = lax.rsqrt(jnp.mean(x * x, axis=-1, keepdims=True) + EPSILON)
    own = (own_ref[...].astype(F32) * scale * gain_ref[...].astype(F32)).astype(BF16)
    tokens = own.shape[0]
    sel = sel_ref[...]
    hit = lax.broadcasted_iota(jnp.int32, (tokens, sel.shape[1]), 0) == sel
    placed = jnp.where(hit, 1.0, 0.0).astype(BF16)
    out_ref[...] = lax.dot_general(
        placed, own, (((0,), (0,)), ((), ())), preferred_element_type=F32
    ).astype(BF16)


def outgoing_rows(column, stream, gain, sel, share):
    tokens, width = stream.shape
    slots = sel.shape[1]
    return pl.pallas_call(
        send_kernel,
        grid_spec=pltpu.PrefetchScalarGridSpec(
            num_scalar_prefetch=1,
            grid=(1,),
            in_specs=[
                whole((tokens, width)),
                pl.BlockSpec((tokens, share), lambda i, col: (0, col[0])),
                pl.BlockSpec((1, share), lambda i, col: (0, col[0])),
                whole((1, slots)),
            ],
            out_specs=whole((slots, share)),
        ),
        out_shape=shape_of((slots, share), BF16),
        cost_estimate=cost(2 * slots * tokens * share, 2 * tokens * width + 2 * slots * share),
        compiler_params=PARAMS,
        name="send_rows",
    )(column, stream, stream, gain, sel)


def compact_kernel(inv_ref, arrived_ref, out_ref):
    tile, slots = out_ref.shape[0], inv_ref.shape[1]
    at = lax.broadcasted_iota(jnp.int32, (tile, slots), 0) + pl.program_id(0) * tile
    hit = jnp.where(at == inv_ref[...], 1.0, 0.0).astype(BF16)
    out_ref[...] = jnp.dot(hit, arrived_ref[...], preferred_element_type=F32).astype(BF16)


def compacted(inv, arrived, picks):
    slots, width = arrived.shape
    tile = picks // 2
    return pl.pallas_call(
        compact_kernel,
        grid=(picks // tile,),
        in_specs=[whole((1, slots)), whole((slots, width))],
        out_specs=pl.BlockSpec((tile, width), lambda i: (i, 0)),
        out_shape=shape_of((picks, width), BF16),
        cost_estimate=cost(2 * picks * slots * width, 2 * slots * width),
        compiler_params=PARAMS,
        name="compact_rows",
    )(inv, arrived)


EARLY = (0, 1, 2, 3, 6, 7)


def products(pieces, gates, ups):
    total = None
    for piece, gate, up in zip(pieces, gates, ups):
        weights = jnp.concatenate([gate[...], up[...]], axis=1)
        part = jnp.dot(piece, weights, preferred_element_type=F32)
        total = part if total is None else total + part
    return total


def early_kernel(group_ref, *refs):
    n = len(EARLY)
    pieces = [ref[...] for ref in refs[:n]]
    refs[-1][...] = products(pieces, refs[n : 2 * n], refs[2 * n : 3 * n])


def late_kernel(group_ref, low, high, low_x, high_x, g4, g5, u4, u5, acc_ref, out_ref):
    upper = pl.program_id(0) >= pl.num_programs(0) // 2
    pieces = [
        jnp.where(upper, high[...], low[...]),
        jnp.where(upper, high_x[...], low_x[...]),
    ]
    total = acc_ref[...] + products(pieces, (g4, g5), (u4, u5))
    units = out_ref.shape[1]
    gate, up = total[:, :units], total[:, units:]
    out_ref[...] = (gate / (1.0 + jnp.exp(-gate)) * up).astype(BF16)


def weight_specs(masks, share, units):
    def spec(mask):
        return pl.BlockSpec((share, units), lambda i, g: (g[0] ^ mask, 0))

    return [spec(mask) for mask in masks]


def early_products(group, pieces, w_gate, w_up):
    picks, share = pieces[0].shape
    units = w_gate.shape[1]
    tile = 256
    n = len(EARLY)
    return pl.pallas_call(
        early_kernel,
        grid_spec=pltpu.PrefetchScalarGridSpec(
            num_scalar_prefetch=1,
            grid=(picks // tile,),
            in_specs=[pl.BlockSpec((tile, share), lambda i, g: (i, 0))] * n
            + weight_specs(EARLY, share, units) * 2,
            out_specs=pl.BlockSpec((tile, 2 * units), lambda i, g: (i, 0)),
        ),
        out_shape=shape_of((picks, 2 * units), F32),
        cost_estimate=cost(4 * picks * n * share * units, 2 * n * share * (picks + 2 * units)),
        compiler_params=PARAMS,
        name="gate_up_early",
    )(group, *pieces, *([w_gate] * n), *([w_up] * n))


def late_products(group, halves, w_gate, w_up, acc):
    half, share = halves[0].shape
    picks = 2 * half
    units = w_gate.shape[1]
    tile = 256
    steps = picks // tile
    low_spec = pl.BlockSpec((tile, share), lambda i, g: (jnp.minimum(i, steps // 2 - 1), 0))
    high_spec = pl.BlockSpec((tile, share), lambda i, g: (jnp.maximum(i - steps // 2, 0), 0))
    return pl.pallas_call(
        late_kernel,
        grid_spec=pltpu.PrefetchScalarGridSpec(
            num_scalar_prefetch=1,
            grid=(steps,),
            in_specs=[low_spec, high_spec] * 2
            + weight_specs((4, 5), share, units) * 2
            + [pl.BlockSpec((tile, 2 * units), lambda i, g: (i, 0))],
            out_specs=pl.BlockSpec((tile, units), lambda i, g: (i, 0)),
        ),
        out_shape=shape_of((picks, units), BF16),
        cost_estimate=cost(8 * picks * share * units, 4 * share * (picks + 2 * units)),
        compiler_params=PARAMS,
        name="gate_up_late",
    )(group, *halves, *([w_gate] * 2), *([w_up] * 2), acc)


def down_kernel(group_ref, hidden_ref, *refs):
    weights, out_ref = refs[:4], refs[4]
    side = jnp.concatenate([ref[...] for ref in weights], axis=1)
    out_ref[...] = jnp.dot(hidden_ref[...], side, preferred_element_type=F32).astype(BF16)


def down_products(group, hidden, w_down, core):
    picks, units = hidden.shape
    share = w_down.shape[1] // 8
    tile = 256

    def spec(mask):
        return pl.BlockSpec((units, share), lambda i, g: (0, g[0] ^ mask))

    return pl.pallas_call(
        down_kernel,
        grid_spec=pltpu.PrefetchScalarGridSpec(
            num_scalar_prefetch=1,
            grid=(picks // tile,),
            in_specs=[pl.BlockSpec((tile, units), lambda i, g: (i, 0))]
            + [spec(2 * d + core) for d in range(4)],
            out_specs=pl.BlockSpec((tile, 4 * share), lambda i, g: (i, 0)),
        ),
        out_shape=shape_of((picks, 4 * share), BF16),
        cost_estimate=cost(8 * picks * share * units, 8 * (picks + units) * share),
        compiler_params=PARAMS,
        name="down",
    )(group, hidden, *([w_down] * 4))


def added(*refs):
    total = refs[0][...].astype(F32)
    for ref in refs[1:]:
        total = total + ref[...].astype(F32)
    return total


def pair_kernel(*refs):
    (a_ref, b_ref) = refs[8:]
    share = refs[0].shape[1]
    for out_ref, first in ((a_ref, 0), (b_ref, 4)):
        for n in range(2):
            out_ref[:, n * share : (n + 1) * share] = added(
                refs[first + 2 * n], refs[first + 2 * n + 1]
            ).astype(BF16)


def pair_sums(keep, came, share):
    picks = keep.shape[0]
    half = picks // 2
    tile = half // 2

    def spec(side, d):
        return pl.BlockSpec((tile, share), lambda i: (i + side * (half // tile), d))

    picked = [(0, 1), (0, 2), (1, 3), (1, 2)]
    specs = []
    for side, d in picked:
        specs += [spec(side, d)] * 2
    return pl.pallas_call(
        pair_kernel,
        grid=(half // tile,),
        in_specs=specs,
        out_specs=[pl.BlockSpec((tile, 2 * share), lambda i: (i, 0))] * 2,
        out_shape=[shape_of((half, 2 * share), BF16)] * 2,
        cost_estimate=cost(half * 4 * share, 24 * half * share),
        compiler_params=PARAMS,
        name="pair_sums",
    )(*([keep, came] * 4))


def quad_kernel(a0, a1, a2, b0, b1, b2, a_ref, b_ref):
    a_ref[...] = added(a0, a1, a2).astype(BF16)
    b_ref[...] = added(b0, b1, b2).astype(BF16)


def quad_sums(keep, came, a_came, b_came, share):
    picks = keep.shape[0]
    half = picks // 2
    tile = half // 2

    def spec(side, d):
        return pl.BlockSpec((tile, share), lambda i: (i + side * (half // tile), d))

    second = pl.BlockSpec((tile, share), lambda i: (i, 1))
    out = pl.BlockSpec((tile, share), lambda i: (i, 0))
    return pl.pallas_call(
        quad_kernel,
        grid=(half // tile,),
        in_specs=[spec(0, 3), spec(0, 3), second, spec(1, 1), spec(1, 1), second],
        out_specs=[out, out],
        out_shape=[shape_of((half, share), BF16)] * 2,
        cost_estimate=cost(half * 4 * share, 16 * half * share),
        compiler_params=PARAMS,
        name="quad_sums",
    )(keep, came, a_came, keep, came, b_came)


def leave_kernel(keep, came, a1, b1, a2, b2, weight_ref, arrival_ref, out_ref, rows_ref):
    half = a1.shape[0]

    @pl.when(pl.program_id(0) == 0)
    def _():
        total = added(keep, came)
        weight = weight_ref[...]
        rows_ref[:half] = ((total[:half] + added(a1, a2)) * weight[:half]).astype(BF16)
        rows_ref[half:] = ((total[half:] + added(b1, b2)) * weight[half:]).astype(BF16)

    tile, picks = out_ref.shape[0], arrival_ref.shape[1]
    at = lax.broadcasted_iota(jnp.int32, (tile, picks), 0) + pl.program_id(0) * tile
    hit = jnp.where(at == arrival_ref[...], 1.0, 0.0).astype(BF16)
    out_ref[...] = jnp.dot(hit, rows_ref[...], preferred_element_type=F32).astype(BF16)


def leaving_rows(keep, came, a1, b1, a2, b2, weight, arrival, slots, share):
    picks = keep.shape[0]
    half = picks // 2
    tile = slots // 3
    return pl.pallas_call(
        leave_kernel,
        grid=(slots // tile,),
        in_specs=[whole((picks, share))] * 2
        + [whole((half, share))] * 4
        + [whole((picks, 1)), whole((1, picks))],
        out_specs=pl.BlockSpec((tile, share), lambda i: (i, 0)),
        out_shape=shape_of((slots, share), BF16),
        scratch_shapes=[pltpu.VMEM((picks, share), BF16)],
        cost_estimate=cost(2 * slots * picks * share, 2 * (slots + 4 * picks) * share),
        compiler_params=PARAMS,
        name="leave_rows",
    )(keep, came, a1, b1, a2, b2, weight, arrival)


def merge_kernel(column_ref, own_ref, sel_ref, came_ref, merged_ref, square_ref):
    tokens = own_ref.shape[0]
    sel = sel_ref[...]
    hit = lax.broadcasted_iota(jnp.int32, (tokens, sel.shape[1]), 0) == sel
    placed = jnp.where(hit, 1.0, 0.0).astype(BF16)
    update = jnp.dot(placed, came_ref[...], preferred_element_type=F32)
    merged = own_ref[...].astype(F32) + update
    merged_ref[...] = merged
    square_ref[...] = jnp.sum(merged * merged, axis=1, keepdims=True)


def merged_rows(column, stream, sel, came, share):
    tokens = stream.shape[0]
    slots = sel.shape[1]
    return pl.pallas_call(
        merge_kernel,
        grid_spec=pltpu.PrefetchScalarGridSpec(
            num_scalar_prefetch=1,
            grid=(1,),
            in_specs=[
                pl.BlockSpec((tokens, share), lambda i, col: (0, col[0])),
                whole((1, slots)),
                whole((slots, share)),
            ],
            out_specs=[whole((tokens, share)), whole((tokens, 1))],
        ),
        out_shape=[shape_of((tokens, share), F32), shape_of((tokens, 1), F32)],
        cost_estimate=cost(2 * slots * tokens * share, 2 * slots * share),
        compiler_params=PARAMS,
        name="merge_rows",
    )(column, stream, sel, came)


def on_device(stream, ffn_gain, chosen, affinity, w_gate, w_up, w_down, final_gain):
    tok_rows, model_width = stream.shape
    experts, picks = chosen.shape
    ep_count = lax.axis_size("ep")
    tp_count = lax.axis_size("tp")
    device = lax.axis_index("ep")
    column = lax.axis_index("tp").astype(jnp.int32)
    share = model_width // tp_count
    slots = 3 * tok_rows // 16
    group = column.reshape(1)

    base = device * tok_rows
    begin = jnp.sum((chosen < base).astype(jnp.int32), axis=1)
    end = jnp.sum((chosen < base + tok_rows).astype(jnp.int32), axis=1)
    slot_range = jnp.arange(slots, dtype=jnp.int32)
    places = jnp.arange(picks, dtype=jnp.int32)
    want = begin[:, None] + slot_range[None, :]
    found = jnp.sum(
        jnp.where(places[None, None, :] == want[:, :, None], chosen[:, None, :], 0), axis=2
    )
    sel = jnp.where(want < end[:, None], found - base, -1).reshape(1, experts * slots)

    row = lax.dynamic_index_in_dim(chosen, device, 0, keepdims=True)
    edges = jnp.arange(ep_count, dtype=jnp.int32)[:, None] * tok_rows
    starts = jnp.sum((row < edges).astype(jnp.int32), axis=1)
    stops = jnp.sum((row < edges + tok_rows).astype(jnp.int32), axis=1)
    row_want = starts[:, None] + slot_range[None, :]
    inv = jnp.where(row_want < stops[:, None], row_want, -1).reshape(1, ep_count * slots)
    mine = (row >= edges) & (row < edges + tok_rows)
    arrival = jnp.sum(
        jnp.where(
            mine,
            jnp.arange(ep_count, dtype=jnp.int32)[:, None] * slots
            + places[None, :]
            - starts[:, None],
            0,
        ),
        axis=0,
        keepdims=True,
    )
    weight = affinity.reshape(picks, 1)

    half = picks // 2
    gate_rows, up_rows, down_rows = w_gate[0], w_up[0], w_down[0]
    outgoing = outgoing_rows(group, stream, ffn_gain.reshape(1, -1), sel, share)
    arrived = lax.all_to_all(
        outgoing.reshape(experts, slots, share), "ep", split_axis=0, concat_axis=0, tiled=True
    )
    own = compacted(inv, arrived.reshape(-1, share), picks)
    near = exchanged(own, "tp", 2)
    back = exchanged(own, "tp", 6)
    far_low = exchanged(near[:half], "tp", 6)
    far_high = exchanged(back[half:], "tp", 2)
    pieces = []
    for piece in (own, near, back):
        pieces += [piece, exchanged(piece, "tp", 1)]
    acc = early_products(group, pieces, gate_rows, up_rows)
    far_low, far_high, acc = lax.optimization_barrier((far_low, far_high, acc))
    halves = [far_low, far_high, exchanged(far_low, "tp", 1), exchanged(far_high, "tp", 1)]
    hidden = late_products(group, halves, gate_rows, up_rows, acc)

    came = exchanged(down_products(group, hidden, down_rows, 1), "tp", 1)
    keep = down_products(group, hidden, down_rows, 0)
    a_send, b_send = pair_sums(keep, came, share)
    a1, b1 = exchanged(a_send, "tp", 2), exchanged(b_send, "tp", 6)
    a_next, b_next = quad_sums(keep, came, a1, b1, share)
    a2, b2 = exchanged(a_next, "tp", 6), exchanged(b_next, "tp", 2)
    leaving = leaving_rows(
        keep, came, a1, b1, a2, b2, weight, arrival, ep_count * slots, share
    )
    returned = lax.all_to_all(
        leaving.reshape(ep_count, slots, share), "ep", split_axis=0, concat_axis=0, tiled=True
    )
    merged, squares = merged_rows(group, stream, sel, returned.reshape(-1, share), share)
    totals = squares.reshape(1, tok_rows)
    for mask in (1, 2, 6):
        totals = totals + exchanged(totals, "tp", mask)
    scale_out = lax.rsqrt(totals.reshape(tok_rows, 1) / model_width + EPSILON)
    return (merged * scale_out * final_gain.astype(F32)[None, :]).astype(BF16)


def solution(mesh):
    return jax.shard_map(
        on_device,
        mesh=mesh,
        in_specs=(
            P("ep", None),
            P(),
            P(),
            P("ep", None),
            P("ep", None, "tp"),
            P("ep", None, "tp"),
            P("ep", "tp", None),
            P("tp"),
        ),
        out_specs=P("ep", "tp"),
        check_vma=False,
    )
```

time: 290 us -> 192 us (0.66); the launches traced: 284 us -> 191 us
  Pallas kernels: 77 us -> 23.7 us
  starting transfers between devices: 70.8 us -> 23.6 us
  waiting for transfers between devices: 67 us -> 85.6 us
  blocking collectives: 47.8 us -> 37.4 us
    pallas_call x17 -> x9, Pallas kernels: 67 us -> 21.7 us  [the longest x1 5.6 us: early_products(): pl.pallas_call(early_kernel, grid_spec=pltpu.PrefetchScalarGridSpec(num_s...]
    ppermute x45 -> x17, starting transfers between devices: 42.1 us -> 12.4 us  [exchanged(): return lax.ppermute(array, axis, [(i, i ^ mask) for i in range(devices)])]
    all_to_all x4 -> x1, starting transfers between devices: 28.7 us -> 11.2 us  [on_device(): lax.all_to_all(outgoing.reshape(experts, slots, share), 'ep', split_axis=...]
    all_to_all x2 -> x1, blocking collectives: 47.8 us -> 37.4 us  [on_device(): lax.all_to_all(leaving.reshape(ep_count, slots, share), 'ep', split_axis=...]
    all_to_all x4 -> x1, waiting for transfers between devices: 13.2 us -> 23.2 us  [on_device(): lax.all_to_all(outgoing.reshape(experts, slots, share), 'ep', split_axis=...]
    ppermute x45 -> x17, waiting for transfers between devices: 53.9 us -> 62.5 us  [exchanged(): return lax.ppermute(array, axis, [(i, i ^ mask) for i in range(devices)])]
    pallas_call x3 -> x1, Pallas kernels: 10.1 us -> 1.97 us  [compacted(): pl.pallas_call(compact_kernel, grid=(picks // tile,), in_specs=[whole((1,...]
    unnamed x92 -> x30, local copies, waits for them, and re-layouts: 9.08 us -> 7.48 us
  transfers between devices with their start and end apart: 49 -> 18, of which waited for: 25 -> 15; matrix products, arithmetic and copies ran while one was open for 1% -> 4% of each run, Pallas kernels for 21% -> 4%
where the time goes in v2:
time: 192 us; the launch traced here: 191 us
  waiting for transfers between devices  85.6 us (45%)
  blocking collectives  37.4 us (19%)
  Pallas kernels  23.7 us (12%)
  starting transfers between devices  23.6 us (12%)
  local copies, waits for them, and re-layouts  13.8 us (7%)
  other arithmetic  6.67 us (3%)
    ppermute x17, waiting for transfers between devices, exchanged(): return lax.ppermute(array, axis, [(i, i ^ mask) for i in range(devices)])  62.5 us
    all_to_all x1, blocking collectives, on_device(): lax.all_to_all(leaving.reshape(ep_count, slots, share), 'ep', split_axis=...  37.4 us
    all_to_all x1, waiting for transfers between devices, on_device(): lax.all_to_all(outgoing.reshape(experts, slots, share), 'ep', split_axis=...  23.2 us
    ppermute x17, starting transfers between devices, exchanged(): return lax.ppermute(array, axis, [(i, i ^ mask) for i in range(devices)])  12.4 us
    all_to_all x1, starting transfers between devices, on_device(): lax.all_to_all(outgoing.reshape(experts, slots, share), 'ep', split_axis=...  11.2 us
    unnamed x30, local copies, waits for them, and re-layouts  7.48 us
    pallas_call x1, Pallas kernels, early_products(): pl.pallas_call(early_kernel, grid_spec=pltpu.PrefetchScalarGridSpec(num_s...  5.6 us
    pallas_call x2, Pallas kernels, down_products(): pl.pallas_call(down_kernel, grid_spec=pltpu.PrefetchScalarGridSpec(num_sc...  5.04 us
  transfers between devices with their start and end apart: 18, of which 15 were waited for; matrix products, arithmetic and copies ran while one was open for 4% of the time, Pallas kernels for 4%

profile of v2, /device:TPU:32, one launch (start us, length us, event | category | flops | bytes accessed | tf_op | source)
XLA Modules:
  0.0 191.1 jit_solution(15650254076720825340)
XLA Ops:
  1.1 2.2 %select_reduce_fusion = s32[32,48]{1,0:T(8,128)S(1)} fusion(s32[32,1024]{1,0:T(8,128)} %param.10, s32[32,48]{1,0:T(8,128)S(1)} %iota_add_fusion.1), kind=kLoop, calls=%fused_computation | loop fusion | flops 4717056 | bytes 143360 | tf_op jit(solution)/shard_map/reduce_sum | solution.py:359
  5.6 2.0 %send_rows.1 = bf16[1536,384]{1,0:T(8,128)(2,1)} custom-call(s32[1]{0:T(128)} %bitcast.column_ref.group_ref, bf16[256,3072]{1,0:T(8,128)(2,1)S(1)} %copy-done.5, bf16[256,3072]{1,0:T(8,128)(2,1)S(1)} %copy-done.5, bf16[1,3072]{1,0:T(2,128)(2,1)S(1)} %reshape.171.gain_ref, s32[1,1536]{1,0:T(1,128)S(1)} %select_n.38.sel_ref), custom_call_target="tpu_custom_call" | custom-call | flops 301989888 | bytes 2752512 | tf_op jit(solution)/shard_map/send_rows/pallas_call | solution.py:51
  7.6 11.2 %all-to-all-start = ((bf16[32,48,384]{2,1,0:T(8,128)(2,1)}), bf16[32,48,384]{2,1,0:T(8,128)(2,1)S(1)}, u32[]{:S(2)}, u32[]{:S(2)}) async-start(bf16[32,48,384]{2,1,0:T(8,128)(2,1)} %bitcast.2), calls=%async_computation | async-start | bytes 2359296 | tf_op jit(solution)/shard_map/all_to_all | solution.py:387
  25.6 23.2 %all-to-all-done = bf16[32,48,384]{2,1,0:T(8,128)(2,1)S(1)} async-done(((bf16[32,48,384]{2,1,0:T(8,128)(2,1)}), bf16[32,48,384]{2,1,0:T(8,128)(2,1)S(1)}, u32[]{:S(2)}, u32[]{:S(2)}) %all-to-all-start) | async-done | bytes 1179680 | tf_op jit(solution)/shard_map/all_to_all | solution.py:387
  49.6 2.0 %compact_rows.1.refs_0_ = bf16[1024,384]{1,0:T(8,128)(2,1)S(1)} custom-call(s32[1,1536]{1,0:T(1,128)S(1)} %copy-done.12, bf16[1536,384]{1,0:T(8,128)(2,1)S(1)} %bitcast.39), custom_call_target="tpu_custom_call" | custom-call | flops 1207959552 | bytes 1179648 | tf_op jit(solution)/shard_map/compact_rows/pallas_call | solution.py:81
  51.6 1.7 collective-permute-start
  53.3 2.2 %collective-permute-start.2 = (bf16[1024,384]{1,0:T(8,128)(2,1)S(1)}, bf16[1024,384]{1,0:T(8,128)(2,1)S(1)}, u32[]{:S(2)}, u32[]{:S(2)}) collective-permute-start(bf16[1024,384]{1,0:T(8,128)(2,1)S(1)} %compact_rows.1.refs_0_), channel_id=1, source_target_pairs={{0,6},{1,7},{2,4},{3,5},{4,2},{5,3},{6,0},{7,1},{8,14},{9,15},{10,... | collective-permute-start | bytes 2359304 | tf_op jit(solution)/shard_map/ppermute | solution.py:17
  55.4 13.6 %collective-permute-done.refs_2_ = bf16[1024,384]{1,0:T(8,128)(2,1)S(1)} collective-permute-done((bf16[1024,384]{1,0:T(8,128)(2,1)S(1)}, bf16[1024,384]{1,0:T(8,128)(2,1)S(1)}, u32[]{:S(2)}, u32[]{:S(2)}) %collective-permute-start) | collective-permute-done | bytes 786464 | tf_op jit(solution)/shard_map/ppermute | solution.py:17
  69.1 2.5 %collective-permute-done.2.refs_4_ = bf16[1024,384]{1,0:T(8,128)(2,1)S(1)} collective-permute-done((bf16[1024,384]{1,0:T(8,128)(2,1)S(1)}, bf16[1024,384]{1,0:T(8,128)(2,1)S(1)}, u32[]{:S(2)}, u32[]{:S(2)}) %collective-permute-start.2) | collective-permute-done | bytes 786464 | tf_op jit(solution)/shard_map/ppermute | solution.py:17
  71.6 2.3 %collective-permute-start.1 = (bf16[512,384]{1,0:T(8,128)(2,1)S(1)}, bf16[512,384]{1,0:T(8,128)(2,1)S(1)}, u32[]{:S(2)}, u32[]{:S(2)}) collective-permute-start(bf16[512,384]{1,0:T(8,128)(2,1)S(1)} %slice.8), channel_id=1, source_target_pairs={{0,6},{1,7},{2,4},{3,5},{4,2},{5,3},{6,0},{7,1},{8,14},{9,15},{10,... | collective-permute-start | bytes 1179656 | tf_op jit(solution)/shard_map/ppermute | solution.py:17
  74.1 5.6 %gate_up_early.1.acc_ref = f32[1024,768]{1,0:T(8,128)S(1)} custom-call(s32[1]{0:T(128)} %bitcast.column_ref.group_ref, bf16[1024,384]{1,0:T(8,128)(2,1)S(1)} %compact_rows.1.refs_0_, bf16[1024,384]{1,0:T(8,128)(2,1)S(1)} %collective-permute-done.4.refs_1_, bf16[1024,384]{1,0:T(8,128)(2,1)S(1)} %collective-permute-done.refs_2_, ...), custom_call_target="tpu_custom_call" | custom-call | flops 3623878656 | bytes 8257536 | tf_op jit(solution)/shard_map/gate_up_early/pallas_call | solution.py:135
  79.7 4.7 %collective-permute-done.1.low = bf16[512,384]{1,0:T(8,128)(2,1)S(1)} collective-permute-done((bf16[512,384]{1,0:T(8,128)(2,1)S(1)}, bf16[512,384]{1,0:T(8,128)(2,1)S(1)}, u32[]{:S(2)}, u32[]{:S(2)}) %collective-permute-start.1) | collective-permute-done | bytes 393248 | tf_op jit(solution)/shard_map/ppermute | solution.py:17
  87.5 2.4 %gate_up_late.1.hidden_ref = bf16[1024,384]{1,0:T(8,128)(2,1)S(1)} custom-call(s32[1]{0:T(128)} %bitcast.column_ref.group_ref, bf16[512,384]{1,0:T(8,128)(2,1)S(1)} %collective-permute-done.1.low, bf16[512,384]{1,0:T(8,128)(2,1)S(1)} %collective-permute-done.3.high, bf16[512,384]{1,0:T(8,128)(2,1)S(1)} %collective-permute-done.7.low_x, ...), custom_call_target="tpu_custom_call" | custom-call | flops 1207959552 | bytes 2752512 | tf_op jit(solution)/shard_map/gate_up_late/pallas_call | solution.py:159
  90.0 2.5 %down.3 = bf16[1024,1536]{1,0:T(8,128)(2,1)S(1)} custom-call(s32[1]{0:T(128)} %bitcast.column_ref.group_ref, bf16[1024,384]{1,0:T(8,128)(2,1)S(1)} %gate_up_late.1.hidden_ref, bf16[384,3072]{1,0:T(8,128)(2,1)S(1)} %bitcast.29, bf16[384,3072]{1,0:T(8,128)(2,1)S(1)} %bitcast.30, bf16[384,3072]{1,0:T(8,128)(2,1)S(1)} %bitcast.31, bf16[384,3072]{1,0:T(8,128)(2,1)S(1)} %bitcast.32), custom_call_target="tpu_custom_call" | custom-call | flops 1207959552 | bytes 4325376 | tf_op jit(solution)/shard_map/down/pallas_call | solution.py:190
  92.8 2.5 %down.2.refs_0_.refs_2_.refs_4_.refs_6_.a0.b0.keep = bf16[1024,1536]{1,0:T(8,128)(2,1)S(1)} custom-call(s32[1]{0:T(128)} %bitcast.column_ref.group_ref, bf16[1024,384]{1,0:T(8,128)(2,1)S(1)} %gate_up_late.1.hidden_ref, bf16[384,3072]{1,0:T(8,128)(2,1)S(1)} %bitcast.33, bf16[384,3072]{1,0:T(8,128)(2,1)S(1)} %bitcast.34, bf16[384,3072]{1,0:T(8,128)(2,1)S(1)} %bitcast.35, ...), custom_call_target="tpu_custom_call" | custom-call | flops 1207959552 | bytes 4325376 | tf_op jit(solution)/shard_map/down/pallas_call | solution.py:190
  95.3 3.0 %collective-permute-done.9.refs_1_.refs_3_.refs_5_.refs_7_.a1.b1.came = bf16[1024,1536]{1,0:T(8,128)(2,1)S(1)} collective-permute-done((bf16[1024,1536]{1,0:T(8,128)(2,1)S(1)}, bf16[1024,1536]{1,0:T(8,128)(2,1)S(1)}, u32[]{:S(2)}, u32[]{:S(2)}) %collective-permute-start.9) | collective-permute-done | bytes 3145760 | tf_op jit(solution)/shard_map/ppermute | solution.py:17
  100.8 18.1 %collective-permute-done.10.a2.a1 = bf16[512,768]{1,0:T(8,128)(2,1)S(1)} collective-permute-done((bf16[512,768]{1,0:T(8,128)(2,1)S(1)}, bf16[512,768]{1,0:T(8,128)(2,1)S(1)}, u32[]{:S(2)}, u32[]{:S(2)}) %collective-permute-start.10) | collective-permute-done | bytes 786464 | tf_op jit(solution)/shard_map/ppermute | solution.py:17
  124.0 9.1 %collective-permute-done.12.a2 = bf16[512,384]{1,0:T(8,128)(2,1)S(1)} collective-permute-done((bf16[512,384]{1,0:T(8,128)(2,1)}, bf16[512,384]{1,0:T(8,128)(2,1)S(1)}, u32[]{:S(2)}, u32[]{:S(2)}) %collective-permute-start.12) | collective-permute-done | bytes 393248 | tf_op jit(solution)/shard_map/ppermute | solution.py:17
  133.3 1.9 copy-done.1
  138.5 3.9 %leave_rows.1 = bf16[1536,384]{1,0:T(8,128)(2,1)S(1)} custom-call(bf16[1024,1536]{1,0:T(8,128)(2,1)S(1)} %down.2.refs_0_.refs_2_.refs_4_.refs_6_.a0.b0.keep, bf16[1024,1536]{1,0:T(8,128)(2,1)S(1)} %copy-done.1, bf16[512,768]{1,0:T(8,128)(2,1)S(1)} %copy-done.8, bf16[512,768]{1,0:T(8,128)(2,1)S(1)} %copy-done.10, ...), custom_call_target="tpu_custom_call" | custom-call | flops 1207959552 | bytes 4325376 | tf_op jit(solution)/shard_map/leave_rows/pallas_call | solution.py:294
  142.5 37.4 %all_to_all.10 = bf16[32,48,384]{2,1,0:T(8,128)(2,1)S(1)} all-to-all(bf16[32,48,384]{2,1,0:T(8,128)(2,1)S(1)} %bitcast.37), channel_id=1, replica_groups=mesh['ep'=32,'tp'=8] {'ep'}, dimensions={0} | all-to-all | bytes 2359296 | tf_op jit(solution)/shard_map/all_to_all | solution.py:412
  182.5 3.0 %collective-permute-done.15 = f32[1,256]{1,0:T(1,128)S(1)} collective-permute-done((f32[1,256]{1,0:T(1,128)S(1)}, f32[1,256]{1,0:T(1,128)S(1)}, u32[]{:S(2)}, u32[]{:S(2)}) %collective-permute-start.15) | collective-permute-done | bytes 1056 | tf_op jit(solution)/shard_map/ppermute | solution.py:17
  185.5 1.7 collective-permute-start.16
  187.2 3.1 %collective-permute-done.16 = f32[1,256]{1,0:T(1,128)S(1)} collective-permute-done((f32[1,256]{1,0:T(1,128)S(1)}, f32[1,256]{1,0:T(1,128)S(1)}, u32[]{:S(2)}, u32[]{:S(2)}) %collective-permute-start.16) | collective-permute-done | bytes 1056 | tf_op jit(solution)/shard_map/ppermute | solution.py:17
  (78 shorter events, 29.0 us)
Async XLA Ops:
  7.6 41.2 %all-to-all-start = ((bf16[32,48,384]{2,1,0:T(8,128)(2,1)}), bf16[32,48,384]{2,1,0:T(8,128)(2,1)S(1)}, u32[]{:S(2)}, u32[]{:S(2)}) async-start(bf16[32,48,384]{2,1,0:T(8,128)(2,1)} %bitcast.2), calls=%async_computation | async-start | bytes 2359296 | tf_op jit(solution)/shard_map/all_to_all | solution.py:387
  18.8 55.3 %copy-start.2 = (bf16[1,3072,384]{2,1,0:T(8,128)(2,1)S(1)}, bf16[1,3072,384]{2,1,0:T(8,128)(2,1)}, u32[]{:S(2)}) copy-start(bf16[1,3072,384]{2,1,0:T(8,128)(2,1)} %param.12) | copy-start | bytes 7077892
  48.8 25.3 %copy-start.3 = (bf16[1,3072,384]{2,1,0:T(8,128)(2,1)S(1)}, bf16[1,3072,384]{2,1,0:T(8,128)(2,1)}, u32[]{:S(2)}) copy-start(bf16[1,3072,384]{2,1,0:T(8,128)(2,1)} %param.13) | copy-start | bytes 7077892
  51.6 17.5 %collective-permute-start = (bf16[1024,384]{1,0:T(8,128)(2,1)S(1)}, bf16[1024,384]{1,0:T(8,128)(2,1)S(1)}, u32[]{:S(2)}, u32[]{:S(2)}) collective-permute-start(bf16[1024,384]{1,0:T(8,128)(2,1)S(1)} %compact_rows.1.refs_0_), channel_id=1, source_target_pairs={{0,2},{1,3},{2,0},{3,1},{4,6},{5,7},{6,4},{7,5},{8,10},{9,11},{10,... | collective-permute-start | bytes 2359304 | tf_op jit(solution)/shard_map/ppermute | solution.py:17
  53.3 18.3 %collective-permute-start.2 = (bf16[1024,384]{1,0:T(8,128)(2,1)S(1)}, bf16[1024,384]{1,0:T(8,128)(2,1)S(1)}, u32[]{:S(2)}, u32[]{:S(2)}) collective-permute-start(bf16[1024,384]{1,0:T(8,128)(2,1)S(1)} %compact_rows.1.refs_0_), channel_id=1, source_target_pairs={{0,6},{1,7},{2,4},{3,5},{4,2},{5,3},{6,0},{7,1},{8,14},{9,15},{10,... | collective-permute-start | bytes 2359304 | tf_op jit(solution)/shard_map/ppermute | solution.py:17
  55.4 18.6 %collective-permute-start.4 = (bf16[1024,384]{1,0:T(8,128)(2,1)S(1)}, bf16[1024,384]{1,0:T(8,128)(2,1)S(1)}, u32[]{:S(2)}, u32[]{:S(2)}) collective-permute-start(bf16[1024,384]{1,0:T(8,128)(2,1)S(1)} %compact_rows.1.refs_0_), channel_id=1, source_target_pairs={{0,1},{1,0},{2,3},{3,2},{4,5},{5,4},{6,7},{7,6},{8,9},{9,8},{10,11... | collective-permute-start | bytes 2359304 | tf_op jit(solution)/shard_map/ppermute | solution.py:17
  69.1 5.0 %collective-permute-start.5 = (bf16[1024,384]{1,0:T(8,128)(2,1)S(1)}, bf16[1024,384]{1,0:T(8,128)(2,1)S(1)}, u32[]{:S(2)}, u32[]{:S(2)}) collective-permute-start(bf16[1024,384]{1,0:T(8,128)(2,1)S(1)} %collective-permute-done.refs_2_), channel_id=1, source_target_pairs={{0,1},{1,0},{2,3},{3,2},{4,5},{5,4},{6,7},{7,6},{8,9},{9,8},{10,11... | collective-permute-start | bytes 2359304 | tf_op jit(solution)/shard_map/ppermute | solution.py:17
  71.6 2.5 %collective-permute-start.6 = (bf16[1024,384]{1,0:T(8,128)(2,1)S(1)}, bf16[1024,384]{1,0:T(8,128)(2,1)S(1)}, u32[]{:S(2)}, u32[]{:S(2)}) collective-permute-start(bf16[1024,384]{1,0:T(8,128)(2,1)S(1)} %collective-permute-done.2.refs_4_), channel_id=1, source_target_pairs={{0,1},{1,0},{2,3},{3,2},{4,5},{5,4},{6,7},{7,6},{8,9},{9,8},{10,11... | collective-permute-start | bytes 2359304 | tf_op jit(solution)/shard_map/ppermute | solution.py:17
  71.6 12.8 %collective-permute-start.1 = (bf16[512,384]{1,0:T(8,128)(2,1)S(1)}, bf16[512,384]{1,0:T(8,128)(2,1)S(1)}, u32[]{:S(2)}, u32[]{:S(2)}) collective-permute-start(bf16[512,384]{1,0:T(8,128)(2,1)S(1)} %slice.8), channel_id=1, source_target_pairs={{0,6},{1,7},{2,4},{3,5},{4,2},{5,3},{6,0},{7,1},{8,14},{9,15},{10,... | collective-permute-start | bytes 1179656 | tf_op jit(solution)/shard_map/ppermute | solution.py:17
  73.9 11.3 %collective-permute-start.3 = (bf16[512,384]{1,0:T(8,128)(2,1)S(1)}, bf16[512,384]{1,0:T(8,128)(2,1)S(1)}, u32[]{:S(2)}, u32[]{:S(2)}) collective-permute-start(bf16[512,384]{1,0:T(8,128)(2,1)S(1)} %slice.9), channel_id=1, source_target_pairs={{0,2},{1,3},{2,0},{3,1},{4,6},{5,7},{6,4},{7,5},{8,10},{9,11},{10,... | collective-permute-start | bytes 1179656 | tf_op jit(solution)/shard_map/ppermute | solution.py:17
  85.3 1.7 collective-permute-start.7
  85.3 2.3 %collective-permute-start.8 = (bf16[512,384]{1,0:T(8,128)(2,1)S(1)}, bf16[512,384]{1,0:T(8,128)(2,1)S(1)}, u32[]{:S(2)}, u32[]{:S(2)}) collective-permute-start(bf16[512,384]{1,0:T(8,128)(2,1)S(1)} %collective-permute-done.3.high), channel_id=1, source_target_pairs={{0,1},{1,0},{2,3},{3,2},{4,5},{5,4},{6,7},{7,6},{8,9},{9,8},{10,11... | collective-permute-start | bytes 1179656 | tf_op jit(solution)/shard_map/ppermute | solution.py:17
  92.5 5.7 %collective-permute-start.9 = (bf16[1024,1536]{1,0:T(8,128)(2,1)S(1)}, bf16[1024,1536]{1,0:T(8,128)(2,1)S(1)}, u32[]{:S(2)}, u32[]{:S(2)}) collective-permute-start(bf16[1024,1536]{1,0:T(8,128)(2,1)S(1)} %down.3), channel_id=1, source_target_pairs={{0,1},{1,0},{2,3},{3,2},{4,5},{5,4},{6,7},{7,6},{8,9},{9,8},{10,11... | collective-permute-start | bytes 9437192 | tf_op jit(solution)/shard_map/ppermute | solution.py:17
  98.3 22.0 %copy-start = (bf16[1024,1536]{1,0:T(8,128)(2,1)}, bf16[1024,1536]{1,0:T(8,128)(2,1)S(1)}, u32[]{:S(2)}) copy-start(bf16[1024,1536]{1,0:T(8,128)(2,1)S(1)} %collective-permute-done.9.refs_1_.refs_3_.refs_5_.refs_7_.a1.b1.came) | copy-start | bytes 9437188
  99.1 19.9 %collective-permute-start.10 = (bf16[512,768]{1,0:T(8,128)(2,1)S(1)}, bf16[512,768]{1,0:T(8,128)(2,1)S(1)}, u32[]{:S(2)}, u32[]{:S(2)}) collective-permute-start(bf16[512,768]{1,0:T(8,128)(2,1)S(1)} %get-tuple-element.17), channel_id=1, source_target_pairs={{0,2},{1,3},{2,0},{3,1},{4,6},{5,7},{6,4},{7,5},{8,10},{9,11},{10,... | collective-permute-start | bytes 2359304 | tf_op jit(solution)/shard_map/ppermute | solution.py:17
  99.7 23.3 %copy-start.13 = (f32[1,1024]{1,0:T(1,128)S(1)}, f32[1,1024]{1,0:T(1,128)}, u32[]{:S(2)}) copy-start(f32[1,1024]{1,0:T(1,128)} %param.11) | copy-start | bytes 12292
  99.7 20.6 %collective-permute-start.11 = (bf16[512,768]{1,0:T(8,128)(2,1)S(1)}, bf16[512,768]{1,0:T(8,128)(2,1)S(1)}, u32[]{:S(2)}, u32[]{:S(2)}) collective-permute-start(bf16[512,768]{1,0:T(8,128)(2,1)S(1)} %get-tuple-element.18), channel_id=1, source_target_pairs={{0,6},{1,7},{2,4},{3,5},{4,2},{5,3},{6,0},{7,1},{8,14},{9,15},{10,... | collective-permute-start | bytes 2359304 | tf_op jit(solution)/shard_map/ppermute | solution.py:17
  121.6 11.6 %collective-permute-start.12 = (bf16[512,384]{1,0:T(8,128)(2,1)}, bf16[512,384]{1,0:T(8,128)(2,1)S(1)}, u32[]{:S(2)}, u32[]{:S(2)}) collective-permute-start(bf16[512,384]{1,0:T(8,128)(2,1)} %get-tuple-element.19), channel_id=1, source_target_pairs={{0,6},{1,7},{2,4},{3,5},{4,2},{5,3},{6,0},{7,1},{8,14},{9,15},{10,... | collective-permute-start | bytes 1179656 | tf_op jit(solution)/shard_map/ppermute | solution.py:17
  123.0 10.3 %collective-permute-start.13 = (bf16[512,384]{1,0:T(8,128)(2,1)}, bf16[512,384]{1,0:T(8,128)(2,1)}, u32[]{:S(2)}, u32[]{:S(2)}) collective-permute-start(bf16[512,384]{1,0:T(8,128)(2,1)} %get-tuple-element.20), channel_id=1, source_target_pairs={{0,2},{1,3},{2,0},{3,1},{4,6},{5,7},{6,4},{7,5},{8,10},{9,11},{10,... | collective-permute-start | bytes 1179656 | tf_op jit(solution)/shard_map/ppermute | solution.py:17
  142.4 37.5 %copy-start.6 = (bf16[256,3072]{1,0:T(8,128)(2,1)S(1)}, bf16[256,3072]{1,0:T(8,128)(2,1)}, u32[]{:S(2)}) copy-start(bf16[256,3072]{1,0:T(8,128)(2,1)} %own_ref.3) | copy-start | bytes 4718596
  142.4 44.7 %copy-start.14 = (bf16[384]{0:T(512)(128)(2,1)S(1)}, bf16[384]{0:T(512)(128)(2,1)}, u32[]{:S(2)}) copy-start(bf16[384]{0:T(512)(128)(2,1)} %param.15) | copy-start | bytes 2308
  180.7 1.2 collective-permute-start.14
  181.9 3.6 %collective-permute-start.15 = (f32[1,256]{1,0:T(1,128)S(1)}, f32[1,256]{1,0:T(1,128)S(1)}, u32[]{:S(2)}, u32[]{:S(2)}) collective-permute-start(f32[1,256]{1,0:T(1,128)S(1)} %add.111), channel_id=1, source_target_pairs={{0,2},{1,3},{2,0},{3,1},{4,6},{5,7},{6,4},{7,5},{8,10},{9,11},{10,... | collective-permute-start | bytes 3080 | tf_op jit(solution)/shard_map/ppermute | solution.py:17
  185.5 4.8 %collective-permute-start.16 = (f32[1,256]{1,0:T(1,128)S(1)}, f32[1,256]{1,0:T(1,128)S(1)}, u32[]{:S(2)}, u32[]{:S(2)}) collective-permute-start(f32[1,256]{1,0:T(1,128)S(1)} %add.112), channel_id=1, source_target_pairs={{0,6},{1,7},{2,4},{3,5},{4,2},{5,3},{6,0},{7,1},{8,14},{9,15},{10,... | collective-permute-start | bytes 3080 | tf_op jit(solution)/shard_map/ppermute | solution.py:17
  (9 other events, 21.6 us)

commit v3 on v2

--- a/solution.py
+++ b/solution.py
@@ -7,7 +7,9 @@
 from jax.experimental.pallas import tpu as pltpu
 from jax.sharding import PartitionSpec as P
 
+
 EPSILON = 1e-06
+FIRST_ROWS = 640
 F32 = jnp.float32
 BF16 = jnp.bfloat16
 
@@ -32,54 +34,95 @@
     return pl.BlockSpec(shape, lambda *_: (0,) * len(shape))
 
 
-def send_kernel(column_ref, stream_ref, own_ref, gain_ref, sel_ref, out_ref):
-    x = stream_ref[...].astype(F32)
+def send_kernel(slots, where_ref, chosen_ref, stream_ref, gain_ref, out_ref, held, copied):
+    load = pltpu.make_async_copy(stream_ref, held, copied)
+    load.start()
+    tokens, _ = held.shape
+    share = out_ref.shape[1]
+    column, base = where_ref[0], where_ref[1]
+    chosen = chosen_ref[...]
+    experts = chosen.shape[0]
+    lane = lax.broadcasted_iota(jnp.int32, chosen.shape, 1)
+    before = chosen < base
+    inside = jnp.logical_not(before) & (chosen < base + tokens)
+    begin = jnp.sum(jnp.where(before, 1.0, 0.0), axis=1, keepdims=True).astype(jnp.int32)
+    slot = jnp.where(inside, lane - begin, -1)
+    number = (chosen - base).astype(F32)
+    lanes = gain_ref.shape[1]
+    out_lane = lax.broadcasted_iota(jnp.int32, (experts, lanes), 1)
+    picked = jnp.full((experts, lanes), -1.0, F32)
+    for s in range(slots):
+        hit = slot == s
+        value = jnp.sum(jnp.where(hit, number + 1.0, 0.0), axis=1, keepdims=True) - 1.0
+        picked = jnp.where(out_lane == s, value, picked)
+    if experts < lanes:
+        filler = jnp.full((lanes - experts, lanes), -1.0, F32)
+        picked = jnp.concatenate([picked, filler], axis=0)
+    by_slot = picked.T
+    token = lax.broadcasted_iota(jnp.int32, (slots, tokens), 1).astype(F32)
+    placed = jnp.concatenate(
+        [
+            jnp.where(token == by_slot[:slots, e : e + 1], 1.0, 0.0).astype(BF16)
+            for e in range(experts)
+        ],
+        axis=0,
+    )
+    gains = gain_ref[...].astype(F32)
+    groups = share // lanes
+    gain_row = lax.broadcasted_iota(jnp.int32, gains.shape, 0)
+    gain = jnp.concatenate(
+        [
+            jnp.sum(
+                jnp.where(gain_row == column * groups + i, gains, 0.0), axis=0, keepdims=True
+            )
+            for i in range(groups)
+        ],
+        axis=1,
+    )
+    load.wait()
+    x = held[...].astype(F32)
     scale = lax.rsqrt(jnp.mean(x * x, axis=-1, keepdims=True) + EPSILON)
-    own = (own_ref[...].astype(F32) * scale * gain_ref[...].astype(F32)).astype(BF16)
-    tokens = own.shape[0]
-    sel = sel_ref[...]
-    hit = lax.broadcasted_iota(jnp.int32, (tokens, sel.shape[1]), 0) == sel
-    placed = jnp.where(hit, 1.0, 0.0).astype(BF16)
-    out_ref[...] = lax.dot_general(
-        placed, own, (((0,), (0,)), ((), ())), preferred_element_type=F32
-    ).astype(BF16)
-
-
-def outgoing_rows(column, stream, gain, sel, share):
+    start = pl.multiple_of(column * share, lanes)
+    own = (held[:, pl.ds(start, share)].astype(F32) * scale * gain).astype(BF16)
+    out_ref[...] = jnp.dot(placed, own, preferred_element_type=F32).astype(BF16)
+
+
+def outgoing_rows(where, chosen, stream, gain, slots, share):
     tokens, width = stream.shape
-    slots = sel.shape[1]
-    return pl.pallas_call(
-        send_kernel,
+    experts = chosen.shape[0]
+    return pl.pallas_call(
+        functools.partial(send_kernel, slots),
         grid_spec=pltpu.PrefetchScalarGridSpec(
             num_scalar_prefetch=1,
             grid=(1,),
             in_specs=[
-                whole((tokens, width)),
-                pl.BlockSpec((tokens, share), lambda i, col: (0, col[0])),
-                pl.BlockSpec((1, share), lambda i, col: (0, col[0])),
-                whole((1, slots)),
+                whole(chosen.shape),
+                pl.BlockSpec(memory_space=pltpu.MemorySpace.HBM),
+                whole(gain.shape),
             ],
-            out_specs=whole((slots, share)),
-        ),
-        out_shape=shape_of((slots, share), BF16),
-        cost_estimate=cost(2 * slots * tokens * share, 2 * tokens * width + 2 * slots * share),
-        compiler_params=PARAMS,
+            out_specs=whole((experts * slots, share)),
+            scratch_shapes=[pltpu.VMEM((tokens, width), BF16), pltpu.SemaphoreType.DMA],
+        ),
+        out_shape=shape_of((experts * slots, share), BF16),
+        cost_estimate=cost(
+            2 * experts * slots * tokens * share, 2 * tokens * width + 2 * experts * slots * share
+        ),
         name="send_rows",
-    )(column, stream, stream, gain, sel)
-
-
-def compact_kernel(inv_ref, arrived_ref, out_ref):
+    )(where, chosen, stream, gain)
+
+
+def compact_kernel(base, inv_ref, arrived_ref, out_ref):
     tile, slots = out_ref.shape[0], inv_ref.shape[1]
-    at = lax.broadcasted_iota(jnp.int32, (tile, slots), 0) + pl.program_id(0) * tile
+    at = lax.broadcasted_iota(jnp.int32, (tile, slots), 0) + (base + pl.program_id(0) * tile)
     hit = jnp.where(at == inv_ref[...], 1.0, 0.0).astype(BF16)
     out_ref[...] = jnp.dot(hit, arrived_ref[...], preferred_element_type=F32).astype(BF16)
 
 
-def compacted(inv, arrived, picks):
+def compacted(inv, arrived, base, picks):
     slots, width = arrived.shape
     tile = picks // 2
     return pl.pallas_call(
-        compact_kernel,
+        functools.partial(compact_kernel, base),
         grid=(picks // tile,),
         in_specs=[whole((1, slots)), whole((slots, width))],
         out_specs=pl.BlockSpec((tile, width), lambda i: (i, 0)),
@@ -130,7 +173,7 @@
 def early_products(group, pieces, w_gate, w_up):
     picks, share = pieces[0].shape
     units = w_gate.shape[1]
-    tile = 256
+    tile = picks // 2
     n = len(EARLY)
     return pl.pallas_call(
         early_kernel,
@@ -152,7 +195,7 @@
     half, share = halves[0].shape
     picks = 2 * half
     units = w_gate.shape[1]
-    tile = 256
+    tile = half
     steps = picks // tile
     low_spec = pl.BlockSpec((tile, share), lambda i, g: (jnp.minimum(i, steps // 2 - 1), 0))
     high_spec = pl.BlockSpec((tile, share), lambda i, g: (jnp.maximum(i - steps // 2, 0), 0))
@@ -182,7 +225,7 @@
 def down_products(group, hidden, w_down, core):
     picks, units = hidden.shape
     share = w_down.shape[1] // 8
-    tile = 256
+    tile = picks // 2
 
     def spec(mask):
         return pl.BlockSpec((units, share), lambda i, g: (0, g[0] ^ mask))
@@ -222,8 +265,7 @@
 
 def pair_sums(keep, came, share):
     picks = keep.shape[0]
-    half = picks // 2
-    tile = half // 2
+    half = tile = picks // 2
 
     def spec(side, d):
         return pl.BlockSpec((tile, share), lambda i: (i + side * (half // tile), d))
@@ -244,69 +286,86 @@
     )(*([keep, came] * 4))
 
 
-def quad_kernel(a0, a1, a2, b0, b1, b2, a_ref, b_ref):
+def quad_kernel(a0, a1, a2, b0, b1, b2, low0, low1, low2, high0, high1, high2, a_ref, b_ref, own_ref):
     a_ref[...] = added(a0, a1, a2).astype(BF16)
     b_ref[...] = added(b0, b1, b2).astype(BF16)
+    half = a_ref.shape[0]
+    own_ref[:half] = added(low0, low1, low2)
+    own_ref[half:] = added(high0, high1, high2)
 
 
 def quad_sums(keep, came, a_came, b_came, share):
     picks = keep.shape[0]
     half = picks // 2
-    tile = half // 2
 
     def spec(side, d):
-        return pl.BlockSpec((tile, share), lambda i: (i + side * (half // tile), d))
-
-    second = pl.BlockSpec((tile, share), lambda i: (i, 1))
-    out = pl.BlockSpec((tile, share), lambda i: (i, 0))
+        return pl.BlockSpec((half, share), lambda i: (side, d))
+
+    first, second = spec(0, 0), spec(0, 1)
+    out = spec(0, 0)
     return pl.pallas_call(
         quad_kernel,
-        grid=(half // tile,),
-        in_specs=[spec(0, 3), spec(0, 3), second, spec(1, 1), spec(1, 1), second],
-        out_specs=[out, out],
-        out_shape=[shape_of((half, share), BF16)] * 2,
-        cost_estimate=cost(half * 4 * share, 16 * half * share),
+        grid=(1,),
+        in_specs=[spec(0, 3)] * 2
+        + [second]
+        + [spec(1, 1)] * 2
+        + [second]
+        + [spec(0, 0)] * 2
+        + [first]
+        + [spec(1, 0)] * 2
+        + [first],
+        out_specs=[out, out, whole((picks, share))],
+        out_shape=[shape_of((half, share), BF16)] * 2 + [shape_of((picks, share), F32)],
+        cost_estimate=cost(picks * 4 * share, 16 * picks * share),
         compiler_params=PARAMS,
         name="quad_sums",
-    )(keep, came, a_came, keep, came, b_came)
-
-
-def leave_kernel(keep, came, a1, b1, a2, b2, weight_ref, arrival_ref, out_ref, rows_ref):
-    half = a1.shape[0]
+    )(keep, came, a_came, keep, came, b_came, keep, came, a_came, keep, came, b_came)
+
+
+def leave_kernel(own_ref, a2, b2, weight_ref, arrival_ref, *refs):
+    out_ref, rows_ref = refs[-2:]
+    half = a2.shape[0]
 
     @pl.when(pl.program_id(0) == 0)
     def _():
-        total = added(keep, came)
         weight = weight_ref[...]
-        rows_ref[:half] = ((total[:half] + added(a1, a2)) * weight[:half]).astype(BF16)
-        rows_ref[half:] = ((total[half:] + added(b1, b2)) * weight[half:]).astype(BF16)
+        rows_ref[:half] = (added(own_ref.at[:half], a2) * weight[:half]).astype(BF16)
+        rows_ref[half:] = (added(own_ref.at[half:], b2) * weight[half:]).astype(BF16)
 
     tile, picks = out_ref.shape[0], arrival_ref.shape[1]
     at = lax.broadcasted_iota(jnp.int32, (tile, picks), 0) + pl.program_id(0) * tile
     hit = jnp.where(at == arrival_ref[...], 1.0, 0.0).astype(BF16)
-    out_ref[...] = jnp.dot(hit, rows_ref[...], preferred_element_type=F32).astype(BF16)
-
-
-def leaving_rows(keep, came, a1, b1, a2, b2, weight, arrival, slots, share):
-    picks = keep.shape[0]
+    total = jnp.dot(hit, rows_ref[...], preferred_element_type=F32)
+    if len(refs) == 3:
+        total = total + refs[0][...].astype(F32)
+    out_ref[...] = total.astype(BF16)
+
+
+def leaving_rows(own, a2, b2, weight, arrival, before, slots, share):
+    picks = own.shape[0]
     half = picks // 2
     tile = slots // 3
+    row_spec = pl.BlockSpec((tile, share), lambda i: (i, 0))
     return pl.pallas_call(
         leave_kernel,
         grid=(slots // tile,),
-        in_specs=[whole((picks, share))] * 2
-        + [whole((half, share))] * 4
-        + [whole((picks, 1)), whole((1, picks))],
-        out_specs=pl.BlockSpec((tile, share), lambda i: (i, 0)),
+        in_specs=[whole((picks, share))]
+        + [whole((half, share))] * 2
+        + [
+            whole((picks, 1)),
+            whole((1, picks)),
+        ]
+        + [row_spec] * len(before),
+        out_specs=row_spec,
         out_shape=shape_of((slots, share), BF16),
         scratch_shapes=[pltpu.VMEM((picks, share), BF16)],
         cost_estimate=cost(2 * slots * picks * share, 2 * (slots + 4 * picks) * share),
         compiler_params=PARAMS,
         name="leave_rows",
-    )(keep, came, a1, b1, a2, b2, weight, arrival)
-
-
-def merge_kernel(column_ref, own_ref, sel_ref, came_ref, merged_ref, square_ref):
+    )(own, a2, b2, weight, arrival, *before)
+
+
+def merge_kernel(own_ref, sel_ref, came_ref, merged_ref, square_ref):
     tokens = own_ref.shape[0]
     sel = sel_ref[...]
     hit = lax.broadcasted_iota(jnp.int32, (tokens, sel.shape[1]), 0) == sel
@@ -317,26 +376,15 @@
     square_ref[...] = jnp.sum(merged * merged, axis=1, keepdims=True)
 
 
-def merged_rows(column, stream, sel, came, share):
-    tokens = stream.shape[0]
-    slots = sel.shape[1]
+def merged_rows(own, sel, came):
+    tokens, share = own.shape
     return pl.pallas_call(
         merge_kernel,
-        grid_spec=pltpu.PrefetchScalarGridSpec(
-            num_scalar_prefetch=1,
-            grid=(1,),
-            in_specs=[
-                pl.BlockSpec((tokens, share), lambda i, col: (0, col[0])),
-                whole((1, slots)),
-                whole((slots, share)),
-            ],
-            out_specs=[whole((tokens, share)), whole((tokens, 1))],
-        ),
         out_shape=[shape_of((tokens, share), F32), shape_of((tokens, 1), F32)],
-        cost_estimate=cost(2 * slots * tokens * share, 2 * slots * share),
+        cost_estimate=cost(2 * came.size * tokens, 2 * came.size),
         compiler_params=PARAMS,
         name="merge_rows",
-    )(column, stream, sel, came)
+    )(own, sel, came)
 
 
 def on_device(stream, ffn_gain, chosen, affinity, w_gate, w_up, w_down, final_gain):
@@ -381,41 +429,61 @@
     )
     weight = affinity.reshape(picks, 1)
 
-    half = picks // 2
+    edges_of = (0, FIRST_ROWS, picks)
+    parts = len(edges_of) - 1
     gate_rows, up_rows, down_rows = w_gate[0], w_up[0], w_down[0]
-    outgoing = outgoing_rows(group, stream, ffn_gain.reshape(1, -1), sel, share)
+    own_stream = lax.dynamic_slice_in_dim(stream, column * share, share, 1)
+    where = jnp.stack([column, base.astype(jnp.int32)])
+    outgoing = outgoing_rows(where, chosen, stream, ffn_gain.reshape(-1, 128), slots, share)
     arrived = lax.all_to_all(
         outgoing.reshape(experts, slots, share), "ep", split_axis=0, concat_axis=0, tiled=True
+    ).reshape(-1, share)
+
+    def moved(array, mask):
+        return exchanged(array, "tp", mask)
+
+    keeps, cames, sends, leaving = [], [], [], []
+    for part in range(parts):
+        rows_from, rows_to = edges_of[part], edges_of[part + 1]
+        half = (rows_to - rows_from) // 2
+        own = compacted(inv, arrived, rows_from, rows_to - rows_from)
+        near = moved(own, 2)
+        back = moved(own, 6)
+        far_low = moved(near[:half], 6)
+        far_high = moved(back[half:], 2)
+        pieces = [own, moved(own, 1), near, moved(near, 1), back, moved(back, 1)]
+        halves = [far_low, far_high, moved(far_low, 1), moved(far_high, 1)]
+        acc = early_products(group, pieces, gate_rows, up_rows)
+        hidden = late_products(group, halves, gate_rows, up_rows, acc)
+        give = down_products(group, hidden, down_rows, 1)
+        keeps.append(down_products(group, hidden, down_rows, 0))
+        cames.append(moved(give, 1))
+        sends.append(pair_sums(keeps[part], cames[part], share))
+    for part in range(parts):
+        a1 = moved(sends[part][0], 2)
+        b1 = moved(sends[part][1], 6)
+        a_next, b_next, own_sum = quad_sums(keeps[part], cames[part], a1, b1, share)
+        a2 = moved(a_next, 6)
+        b2 = moved(b_next, 2)
+        leaving = [
+            leaving_rows(
+                own_sum,
+                a2,
+                b2,
+                weight[edges_of[part] : edges_of[part + 1]],
+                arrival[:, edges_of[part] : edges_of[part + 1]],
+                leaving,
+                ep_count * slots,
+                share,
+            )
+        ]
+    returned = lax.all_to_all(
+        leaving[0].reshape(ep_count, slots, share), "ep", split_axis=0, concat_axis=0, tiled=True
     )
-    own = compacted(inv, arrived.reshape(-1, share), picks)
-    near = exchanged(own, "tp", 2)
-    back = exchanged(own, "tp", 6)
-    far_low = exchanged(near[:half], "tp", 6)
-    far_high = exchanged(back[half:], "tp", 2)
-    pieces = []
-    for piece in (own, near, back):
-        pieces += [piece, exchanged(piece, "tp", 1)]
-    acc = early_products(group, pieces, gate_rows, up_rows)
-    far_low, far_high, acc = lax.optimization_barrier((far_low, far_high, acc))
-    halves = [far_low, far_high, exchanged(far_low, "tp", 1), exchanged(far_high, "tp", 1)]
-    hidden = late_products(group, halves, gate_rows, up_rows, acc)
-
-    came = exchanged(down_products(group, hidden, down_rows, 1), "tp", 1)
-    keep = down_products(group, hidden, down_rows, 0)
-    a_send, b_send = pair_sums(keep, came, share)
-    a1, b1 = exchanged(a_send, "tp", 2), exchanged(b_send, "tp", 6)
-    a_next, b_next = quad_sums(keep, came, a1, b1, share)
-    a2, b2 = exchanged(a_next, "tp", 6), exchanged(b_next, "tp", 2)
-    leaving = leaving_rows(
-        keep, came, a1, b1, a2, b2, weight, arrival, ep_count * slots, share
-    )
-    returned = lax.all_to_all(
-        leaving.reshape(ep_count, slots, share), "ep", split_axis=0, concat_axis=0, tiled=True
-    )
-    merged, squares = merged_rows(group, stream, sel, returned.reshape(-1, share), share)
+    merged, squares = merged_rows(own_stream, sel, returned.reshape(-1, share))
     totals = squares.reshape(1, tok_rows)
-    for mask in (1, 2, 6):
-        totals = totals + exchanged(totals, "tp", mask)
+    totals = totals + exchanged(totals, "tp", 1)
+    totals = totals + sum(exchanged(totals, "tp", mask) for mask in (2, 4, 6))
     scale_out = lax.rsqrt(totals.reshape(tok_rows, 1) / model_width + EPSILON)
     return (merged * scale_out * final_gain.astype(F32)[None, :]).astype(BF16)
 

time: 192 us -> 188 us (0.979)
  blocking collectives: 37.4 us -> 0 us
  starting transfers between devices: 23.6 us -> 42.6 us
  waiting for transfers between devices: 85.6 us -> 104 us
  local copies, waits for them, and re-layouts: 13.8 us -> 5.69 us
  Pallas kernels: 23.7 us -> 28 us
    all_to_all x1 -> x0, blocking collectives: 37.4 us -> none  [on_device(): lax.all_to_all(leaving.reshape(ep_count, slots, share), 'ep', split_axis=...]
    all_to_all x0 -> x1, waiting for transfers between devices: none -> 25.6 us  [on_device(): lax.all_to_all(leaving[0].reshape(ep_count, slots, share), 'ep', split_ax...]
    ppermute x17 -> x32, starting transfers between devices: 12.4 us -> 24.1 us  [exchanged(): return lax.ppermute(array, axis, [(i, i ^ mask) for i in range(devices)])]
    ppermute x17 -> x32, waiting for transfers between devices: 62.5 us -> 53.7 us  [exchanged(): return lax.ppermute(array, axis, [(i, i ^ mask) for i in range(devices)])]
    all_to_all x0 -> x1, starting transfers between devices: none -> 7.33 us  [on_device(): lax.all_to_all(leaving[0].reshape(ep_count, slots, share), 'ep', split_ax...]
    unnamed x30 -> x18, local copies, waits for them, and re-layouts: 7.48 us -> 1.91 us
    pallas_call x4 -> x6, Pallas kernels: 5.92 us -> 9.7 us  [the longest x1 4.94 us: outgoing_rows(): pl.pallas_call(functools.partial(send_kernel, slots), grid_spec=pltpu.Pre...]
    all_to_all x1, waiting for transfers between devices: 23.2 us -> 25.1 us  [on_device(): lax.all_to_all(outgoing.reshape(experts, slots, share), 'ep', split_axis=...]
  transfers between devices with their start and end apart: 18 -> 34, of which waited for: 15 -> 19; matrix products, arithmetic and copies ran while one was open for 4% -> 4% of each run, Pallas kernels for 4% -> 8%
where the time goes in v3:
time: 188 us; the launch traced here: 187 us
  waiting for transfers between devices  104 us (55%)
  starting transfers between devices  42.6 us (23%)
  Pallas kernels  28 us (15%)
  local copies, waits for them, and re-layouts  5.69 us (3%)
  other arithmetic  5.54 us (3%)
    ppermute x32, waiting for transfers between devices, exchanged(): return lax.ppermute(array, axis, [(i, i ^ mask) for i in range(devices)])  53.7 us
    all_to_all x1, waiting for transfers between devices, on_device(): lax.all_to_all(leaving[0].reshape(ep_count, slots, share), 'ep', split_ax...  25.6 us
    all_to_all x1, waiting for transfers between devices, on_device(): lax.all_to_all(outgoing.reshape(experts, slots, share), 'ep', split_axis=...  25.1 us
    ppermute x32, starting transfers between devices, exchanged(): return lax.ppermute(array, axis, [(i, i ^ mask) for i in range(devices)])  24.1 us
    all_to_all x1, starting transfers between devices, on_device(): lax.all_to_all(outgoing.reshape(experts, slots, share), 'ep', split_axis=...  11.2 us
    all_to_all x1, starting transfers between devices, on_device(): lax.all_to_all(leaving[0].reshape(ep_count, slots, share), 'ep', split_ax...  7.33 us
    pallas_call x2, Pallas kernels, early_products(): pl.pallas_call(early_kernel, grid_spec=pltpu.PrefetchScalarGridSpec(num_s...  5.57 us
    pallas_call x4, Pallas kernels, down_products(): pl.pallas_call(down_kernel, grid_spec=pltpu.PrefetchScalarGridSpec(num_sc...  5.21 us
  transfers between devices with their start and end apart: 34, of which 19 were waited for; matrix products, arithmetic and copies ran while one was open for 4% of the time, Pallas kernels for 8%

profile of v3, /device:TPU:32, one launch (start us, length us, event | category | flops | bytes accessed | tf_op | source)
XLA Modules:
  0.0 186.6 jit_solution(9161078799692548901)
XLA Ops:
  0.6 4.9 %send_rows.1 = bf16[1536,384]{1,0:T(8,128)(2,1)} custom-call(s32[2]{0:T(128)} %pad_add_fusion.where_ref, s32[32,1024]{1,0:T(8,128)} %chosen_ref.1, bf16[256,3072]{1,0:T(8,128)(2,1)} %stream_ref.1, bf16[24,128]{1,0:T(8,128)(2,1)} %bitcast.74), custom_call_target="tpu_custom_call" | custom-call | flops 301989888 | bytes 2752512 | tf_op jit(solution)/shard_map/send_rows/pallas_call | solution.py:93
  5.5 11.2 %all-to-all-start = ((bf16[32,48,384]{2,1,0:T(8,128)(2,1)}), bf16[32,48,384]{2,1,0:T(8,128)(2,1)S(1)}, u32[]{:S(2)}, u32[]{:S(2)}) async-start(bf16[32,48,384]{2,1,0:T(8,128)(2,1)} %bitcast.69), calls=%async_computation | async-start | bytes 2359296 | tf_op jit(solution)/shard_map/all_to_all | solution.py:438
  21.6 25.1 %all-to-all-done = bf16[32,48,384]{2,1,0:T(8,128)(2,1)S(1)} async-done(((bf16[32,48,384]{2,1,0:T(8,128)(2,1)}), bf16[32,48,384]{2,1,0:T(8,128)(2,1)S(1)}, u32[]{:S(2)}, u32[]{:S(2)}) %all-to-all-start) | async-done | bytes 1179680 | tf_op jit(solution)/shard_map/all_to_all | solution.py:438
  49.8 2.2 %collective-permute-start.16 = (bf16[640,384]{1,0:T(8,128)(2,1)S(1)}, bf16[640,384]{1,0:T(8,128)(2,1)S(1)}, u32[]{:S(2)}, u32[]{:S(2)}) collective-permute-start(bf16[640,384]{1,0:T(8,128)(2,1)S(1)} %compact_rows.3.refs_0_), channel_id=1, source_target_pairs={{0,6},{1,7},{2,4},{3,5},{4,2},{5,3},{6,0},{7,1},{8,14},{9,15},{10,... | collective-permute-start | bytes 1474568 | tf_op jit(solution)/shard_map/ppermute | solution.py:19
  51.9 7.3 %collective-permute-done.14.refs_2_ = bf16[640,384]{1,0:T(8,128)(2,1)S(1)} collective-permute-done((bf16[640,384]{1,0:T(8,128)(2,1)S(1)}, bf16[640,384]{1,0:T(8,128)(2,1)S(1)}, u32[]{:S(2)}, u32[]{:S(2)}) %collective-permute-start.14) | collective-permute-done | bytes 491552 | tf_op jit(solution)/shard_map/ppermute | solution.py:19
  59.2 2.5 %collective-permute-done.16.refs_4_ = bf16[640,384]{1,0:T(8,128)(2,1)S(1)} collective-permute-done((bf16[640,384]{1,0:T(8,128)(2,1)S(1)}, bf16[640,384]{1,0:T(8,128)(2,1)S(1)}, u32[]{:S(2)}, u32[]{:S(2)}) %collective-permute-start.16) | collective-permute-done | bytes 491552 | tf_op jit(solution)/shard_map/ppermute | solution.py:19
  61.8 2.3 %collective-permute-start.15 = (bf16[320,384]{1,0:T(8,128)(2,1)S(1)}, bf16[320,384]{1,0:T(8,128)(2,1)S(1)}, u32[]{:S(2)}, u32[]{:S(2)}) collective-permute-start(bf16[320,384]{1,0:T(8,128)(2,1)S(1)} %slice.43), channel_id=1, source_target_pairs={{0,6},{1,7},{2,4},{3,5},{4,2},{5,3},{6,0},{7,1},{8,14},{9,15},{10,... | collective-permute-start | bytes 737288 | tf_op jit(solution)/shard_map/ppermute | solution.py:19
  64.2 7.3 %collective-permute-done.15.low = bf16[320,384]{1,0:T(8,128)(2,1)S(1)} collective-permute-done((bf16[320,384]{1,0:T(8,128)(2,1)S(1)}, bf16[320,384]{1,0:T(8,128)(2,1)S(1)}, u32[]{:S(2)}, u32[]{:S(2)}) %collective-permute-start.15) | collective-permute-done | bytes 245792 | tf_op jit(solution)/shard_map/ppermute | solution.py:19
  74.0 3.4 %gate_up_early.3.acc_ref = f32[640,768]{1,0:T(8,128)S(1)} custom-call(s32[1]{0:T(128)} %bitcast.group_ref, bf16[640,384]{1,0:T(8,128)(2,1)S(1)} %compact_rows.3.refs_0_, bf16[640,384]{1,0:T(8,128)(2,1)S(1)} %collective-permute-done.20.refs_1_, bf16[640,384]{1,0:T(8,128)(2,1)S(1)} %collective-permute-done.14.refs_2_, ...), custom_call_target="tpu_custom_call" | custom-call | flops 2264924160 | bytes 6488064 | tf_op jit(solution)/shard_map/gate_up_early/pallas_call | solution.py:178
  84.0 7.2 %collective-permute-done.refs_2_ = bf16[384,384]{1,0:T(8,128)(2,1)S(1)} collective-permute-done((bf16[384,384]{1,0:T(8,128)(2,1)S(1)}, bf16[384,384]{1,0:T(8,128)(2,1)S(1)}, u32[]{:S(2)}, u32[]{:S(2)}) %collective-permute-start) | collective-permute-done | bytes 294944 | tf_op jit(solution)/shard_map/ppermute | solution.py:19
  92.6 1.9 %collective-permute-start.1 = (bf16[192,384]{1,0:T(8,128)(2,1)S(1)}, bf16[192,384]{1,0:T(8,128)(2,1)S(1)}, u32[]{:S(2)}, u32[]{:S(2)}) collective-permute-start(bf16[192,384]{1,0:T(8,128)(2,1)S(1)} %slice.40), channel_id=1, source_target_pairs={{0,6},{1,7},{2,4},{3,5},{4,2},{5,3},{6,0},{7,1},{8,14},{9,15},{10,... | collective-permute-start | bytes 442376 | tf_op jit(solution)/shard_map/ppermute | solution.py:19
  94.7 5.5 %collective-permute-done.1.low = bf16[192,384]{1,0:T(8,128)(2,1)S(1)} collective-permute-done((bf16[192,384]{1,0:T(8,128)(2,1)S(1)}, bf16[192,384]{1,0:T(8,128)(2,1)S(1)}, u32[]{:S(2)}, u32[]{:S(2)}) %collective-permute-start.1) | collective-permute-done | bytes 147488 | tf_op jit(solution)/shard_map/ppermute | solution.py:19
  100.7 2.2 %gate_up_early.2.acc_ref = f32[384,768]{1,0:T(8,128)S(1)} custom-call(s32[1]{0:T(128)} %bitcast.group_ref, bf16[384,384]{1,0:T(8,128)(2,1)S(1)} %compact_rows.2.refs_0_, bf16[384,384]{1,0:T(8,128)(2,1)S(1)} %collective-permute-done.6.refs_1_, bf16[384,384]{1,0:T(8,128)(2,1)S(1)} %collective-permute-done.refs_2_, ...), custom_call_target="tpu_custom_call" | custom-call | flops 1358954496 | bytes 5308416 | tf_op jit(solution)/shard_map/gate_up_early/pallas_call | solution.py:178
  112.2 1.8 collective-permute-start.11
  114.0 7.9 %collective-permute-done.24.a2.low2 = bf16[320,768]{1,0:T(8,128)(2,1)S(1)} collective-permute-done((bf16[320,768]{1,0:T(8,128)(2,1)S(1)}, bf16[320,768]{1,0:T(8,128)(2,1)S(1)}, u32[]{:S(2)}, u32[]{:S(2)}) %collective-permute-start.24) | collective-permute-done | bytes 491552 | tf_op jit(solution)/shard_map/ppermute | solution.py:19
  124.2 1.7 collective-permute-start.26
  127.6 2.1 %collective-permute-done.11.b2.high2 = bf16[192,768]{1,0:T(8,128)(2,1)S(1)} collective-permute-done((bf16[192,768]{1,0:T(8,128)(2,1)S(1)}, bf16[192,768]{1,0:T(8,128)(2,1)S(1)}, u32[]{:S(2)}, u32[]{:S(2)}) %collective-permute-start.11) | collective-permute-done | bytes 294944 | tf_op jit(solution)/shard_map/ppermute | solution.py:19
  132.4 2.6 %collective-permute-done.26.a2 = bf16[320,384]{1,0:T(8,128)(2,1)S(1)} collective-permute-done((bf16[320,384]{1,0:T(8,128)(2,1)S(1)}, bf16[320,384]{1,0:T(8,128)(2,1)S(1)}, u32[]{:S(2)}, u32[]{:S(2)}) %collective-permute-start.26) | collective-permute-done | bytes 245792 | tf_op jit(solution)/shard_map/ppermute | solution.py:19
  135.0 1.8 leave_rows.2.refs_0_
  137.3 2.4 %leave_rows.3 = bf16[1536,384]{1,0:T(8,128)(2,1)} custom-call(f32[384,384]{1,0:T(8,128)S(1)} %get-tuple-element.19.own_ref, bf16[192,384]{1,0:T(8,128)(2,1)S(1)} %collective-permute-done.12.a2, bf16[192,384]{1,0:T(8,128)(2,1)S(1)} %collective-permute-done.13.b2, f32[384,1]{1,0:T(8,128)S(1)} %copy.12.weight_ref, s32[1,384]{1,0:T(1,128)S(1)} %slice.42.arrival_ref, ...), custom_call_target="tpu_custom_call" | custom-call | flops 452984832 | bytes 2359296 | tf_op jit(solution)/shard_map/leave_rows/pallas_call | solution.py:349
  139.7 7.3 %all-to-all-start.1 = ((bf16[32,48,384]{2,1,0:T(8,128)(2,1)}), bf16[32,48,384]{2,1,0:T(8,128)(2,1)S(1)}, u32[]{:S(2)}, u32[]{:S(2)}) async-start(bf16[32,48,384]{2,1,0:T(8,128)(2,1)} %bitcast.12), calls=%async_computation.1 | async-start | bytes 2359296 | tf_op jit(solution)/shard_map/all_to_all | solution.py:480
  149.7 25.6 %all-to-all-done.1 = bf16[32,48,384]{2,1,0:T(8,128)(2,1)S(1)} async-done(((bf16[32,48,384]{2,1,0:T(8,128)(2,1)}), bf16[32,48,384]{2,1,0:T(8,128)(2,1)S(1)}, u32[]{:S(2)}, u32[]{:S(2)}) %all-to-all-start.1) | async-done | bytes 1179680 | tf_op jit(solution)/shard_map/all_to_all | solution.py:480
  178.3 2.7 %collective-permute-start.30 = (f32[1,256]{1,0:T(1,128)S(1)}, f32[1,256]{1,0:T(1,128)S(1)}, u32[]{:S(2)}, u32[]{:S(2)}) collective-permute-start(f32[1,256]{1,0:T(1,128)S(1)} %add.118), channel_id=1, source_target_pairs={{0,4},{1,5},{2,6},{3,7},{4,0},{5,1},{6,2},{7,3},{8,12},{9,13},{10,... | collective-permute-start | bytes 3080 | tf_op jit(solution)/shard_map/ppermute | solution.py:19
  183.4 2.4 %collective-permute-done.31 = f32[1,256]{1,0:T(1,128)S(1)} collective-permute-done((f32[1,256]{1,0:T(1,128)S(1)}, f32[1,256]{1,0:T(1,128)S(1)}, u32[]{:S(2)}, u32[]{:S(2)}) %collective-permute-start.31) | collective-permute-done | bytes 1056 | tf_op jit(solution)/shard_map/ppermute | solution.py:19
  (112 shorter events, 44.9 us)
Async XLA Ops:
  5.5 41.2 %all-to-all-start = ((bf16[32,48,384]{2,1,0:T(8,128)(2,1)}), bf16[32,48,384]{2,1,0:T(8,128)(2,1)S(1)}, u32[]{:S(2)}, u32[]{:S(2)}) async-start(bf16[32,48,384]{2,1,0:T(8,128)(2,1)} %bitcast.69), calls=%async_computation | async-start | bytes 2359296 | tf_op jit(solution)/shard_map/all_to_all | solution.py:438
  48.1 11.1 %collective-permute-start.14 = (bf16[640,384]{1,0:T(8,128)(2,1)S(1)}, bf16[640,384]{1,0:T(8,128)(2,1)S(1)}, u32[]{:S(2)}, u32[]{:S(2)}) collective-permute-start(bf16[640,384]{1,0:T(8,128)(2,1)S(1)} %compact_rows.3.refs_0_), channel_id=1, source_target_pairs={{0,2},{1,3},{2,0},{3,1},{4,6},{5,7},{6,4},{7,5},{8,10},{9,11},{10,... | collective-permute-start | bytes 1474568 | tf_op jit(solution)/shard_map/ppermute | solution.py:19
  49.8 12.0 %collective-permute-start.16 = (bf16[640,384]{1,0:T(8,128)(2,1)S(1)}, bf16[640,384]{1,0:T(8,128)(2,1)S(1)}, u32[]{:S(2)}, u32[]{:S(2)}) collective-permute-start(bf16[640,384]{1,0:T(8,128)(2,1)S(1)} %compact_rows.3.refs_0_), channel_id=1, source_target_pairs={{0,6},{1,7},{2,4},{3,5},{4,2},{5,3},{6,0},{7,1},{8,14},{9,15},{10,... | collective-permute-start | bytes 1474568 | tf_op jit(solution)/shard_map/ppermute | solution.py:19
  51.9 20.3 %collective-permute-start.20 = (bf16[640,384]{1,0:T(8,128)(2,1)S(1)}, bf16[640,384]{1,0:T(8,128)(2,1)S(1)}, u32[]{:S(2)}, u32[]{:S(2)}) collective-permute-start(bf16[640,384]{1,0:T(8,128)(2,1)S(1)} %compact_rows.3.refs_0_), channel_id=1, source_target_pairs={{0,1},{1,0},{2,3},{3,2},{4,5},{5,4},{6,7},{7,6},{8,9},{9,8},{10,11... | collective-permute-start | bytes 1474568 | tf_op jit(solution)/shard_map/ppermute | solution.py:19
  59.2 13.0 %collective-permute-start.21 = (bf16[640,384]{1,0:T(8,128)(2,1)S(1)}, bf16[640,384]{1,0:T(8,128)(2,1)S(1)}, u32[]{:S(2)}, u32[]{:S(2)}) collective-permute-start(bf16[640,384]{1,0:T(8,128)(2,1)S(1)} %collective-permute-done.14.refs_2_), channel_id=1, source_target_pairs={{0,1},{1,0},{2,3},{3,2},{4,5},{5,4},{6,7},{7,6},{8,9},{9,8},{10,11... | collective-permute-start | bytes 1474568 | tf_op jit(solution)/shard_map/ppermute | solution.py:19
  61.8 10.5 %collective-permute-start.22 = (bf16[640,384]{1,0:T(8,128)(2,1)S(1)}, bf16[640,384]{1,0:T(8,128)(2,1)S(1)}, u32[]{:S(2)}, u32[]{:S(2)}) collective-permute-start(bf16[640,384]{1,0:T(8,128)(2,1)S(1)} %collective-permute-done.16.refs_4_), channel_id=1, source_target_pairs={{0,1},{1,0},{2,3},{3,2},{4,5},{5,4},{6,7},{7,6},{8,9},{9,8},{10,11... | collective-permute-start | bytes 1474568 | tf_op jit(solution)/shard_map/ppermute | solution.py:19
  61.8 9.7 %collective-permute-start.15 = (bf16[320,384]{1,0:T(8,128)(2,1)S(1)}, bf16[320,384]{1,0:T(8,128)(2,1)S(1)}, u32[]{:S(2)}, u32[]{:S(2)}) collective-permute-start(bf16[320,384]{1,0:T(8,128)(2,1)S(1)} %slice.43), channel_id=1, source_target_pairs={{0,6},{1,7},{2,4},{3,5},{4,2},{5,3},{6,0},{7,1},{8,14},{9,15},{10,... | collective-permute-start | bytes 737288 | tf_op jit(solution)/shard_map/ppermute | solution.py:19
  64.1 8.2 %collective-permute-start.17 = (bf16[320,384]{1,0:T(8,128)(2,1)S(1)}, bf16[320,384]{1,0:T(8,128)(2,1)S(1)}, u32[]{:S(2)}, u32[]{:S(2)}) collective-permute-start(bf16[320,384]{1,0:T(8,128)(2,1)S(1)} %slice.44), channel_id=1, source_target_pairs={{0,2},{1,3},{2,0},{3,1},{4,6},{5,7},{6,4},{7,5},{8,10},{9,11},{10,... | collective-permute-start | bytes 737288 | tf_op jit(solution)/shard_map/ppermute | solution.py:19
  80.5 26.6 %collective-permute-start.23 = (bf16[640,1536]{1,0:T(8,128)(2,1)S(1)}, bf16[640,1536]{1,0:T(8,128)(2,1)S(1)}, u32[]{:S(2)}, u32[]{:S(2)}) collective-permute-start(bf16[640,1536]{1,0:T(8,128)(2,1)S(1)} %down.7), channel_id=1, source_target_pairs={{0,1},{1,0},{2,3},{3,2},{4,5},{5,4},{6,7},{7,6},{8,9},{9,8},{10,11... | collective-permute-start | bytes 5898248 | tf_op jit(solution)/shard_map/ppermute | solution.py:19
  82.1 9.2 %collective-permute-start = (bf16[384,384]{1,0:T(8,128)(2,1)S(1)}, bf16[384,384]{1,0:T(8,128)(2,1)S(1)}, u32[]{:S(2)}, u32[]{:S(2)}) collective-permute-start(bf16[384,384]{1,0:T(8,128)(2,1)S(1)} %compact_rows.2.refs_0_), channel_id=1, source_target_pairs={{0,2},{1,3},{2,0},{3,1},{4,6},{5,7},{6,4},{7,5},{8,10},{9,11},{10,... | collective-permute-start | bytes 884744 | tf_op jit(solution)/shard_map/ppermute | solution.py:19
  82.6 10.0 %collective-permute-start.2 = (bf16[384,384]{1,0:T(8,128)(2,1)S(1)}, bf16[384,384]{1,0:T(8,128)(2,1)S(1)}, u32[]{:S(2)}, u32[]{:S(2)}) collective-permute-start(bf16[384,384]{1,0:T(8,128)(2,1)S(1)} %compact_rows.2.refs_0_), channel_id=1, source_target_pairs={{0,6},{1,7},{2,4},{3,5},{4,2},{5,3},{6,0},{7,1},{8,14},{9,15},{10,... | collective-permute-start | bytes 884744 | tf_op jit(solution)/shard_map/ppermute | solution.py:19
  83.8 10.7 %collective-permute-start.6 = (bf16[384,384]{1,0:T(8,128)(2,1)S(1)}, bf16[384,384]{1,0:T(8,128)(2,1)S(1)}, u32[]{:S(2)}, u32[]{:S(2)}) collective-permute-start(bf16[384,384]{1,0:T(8,128)(2,1)S(1)} %compact_rows.2.refs_0_), channel_id=1, source_target_pairs={{0,1},{1,0},{2,3},{3,2},{4,5},{5,4},{6,7},{7,6},{8,9},{9,8},{10,11... | collective-permute-start | bytes 884744 | tf_op jit(solution)/shard_map/ppermute | solution.py:19
  91.3 9.4 %collective-permute-start.7 = (bf16[384,384]{1,0:T(8,128)(2,1)S(1)}, bf16[384,384]{1,0:T(8,128)(2,1)S(1)}, u32[]{:S(2)}, u32[]{:S(2)}) collective-permute-start(bf16[384,384]{1,0:T(8,128)(2,1)S(1)} %collective-permute-done.refs_2_), channel_id=1, source_target_pairs={{0,1},{1,0},{2,3},{3,2},{4,5},{5,4},{6,7},{7,6},{8,9},{9,8},{10,11... | collective-permute-start | bytes 884744 | tf_op jit(solution)/shard_map/ppermute | solution.py:19
  92.6 8.1 %collective-permute-start.8 = (bf16[384,384]{1,0:T(8,128)(2,1)S(1)}, bf16[384,384]{1,0:T(8,128)(2,1)S(1)}, u32[]{:S(2)}, u32[]{:S(2)}) collective-permute-start(bf16[384,384]{1,0:T(8,128)(2,1)S(1)} %collective-permute-done.2.refs_4_), channel_id=1, source_target_pairs={{0,1},{1,0},{2,3},{3,2},{4,5},{5,4},{6,7},{7,6},{8,9},{9,8},{10,11... | collective-permute-start | bytes 884744 | tf_op jit(solution)/shard_map/ppermute | solution.py:19
  92.6 7.6 %collective-permute-start.1 = (bf16[192,384]{1,0:T(8,128)(2,1)S(1)}, bf16[192,384]{1,0:T(8,128)(2,1)S(1)}, u32[]{:S(2)}, u32[]{:S(2)}) collective-permute-start(bf16[192,384]{1,0:T(8,128)(2,1)S(1)} %slice.40), channel_id=1, source_target_pairs={{0,6},{1,7},{2,4},{3,5},{4,2},{5,3},{6,0},{7,1},{8,14},{9,15},{10,... | collective-permute-start | bytes 442376 | tf_op jit(solution)/shard_map/ppermute | solution.py:19
  94.6 6.1 %collective-permute-start.3 = (bf16[192,384]{1,0:T(8,128)(2,1)S(1)}, bf16[192,384]{1,0:T(8,128)(2,1)S(1)}, u32[]{:S(2)}, u32[]{:S(2)}) collective-permute-start(bf16[192,384]{1,0:T(8,128)(2,1)S(1)} %slice.41), channel_id=1, source_target_pairs={{0,2},{1,3},{2,0},{3,1},{4,6},{5,7},{6,4},{7,5},{8,10},{9,11},{10,... | collective-permute-start | bytes 442376 | tf_op jit(solution)/shard_map/ppermute | solution.py:19
  107.7 14.2 %collective-permute-start.24 = (bf16[320,768]{1,0:T(8,128)(2,1)S(1)}, bf16[320,768]{1,0:T(8,128)(2,1)S(1)}, u32[]{:S(2)}, u32[]{:S(2)}) collective-permute-start(bf16[320,768]{1,0:T(8,128)(2,1)S(1)} %get-tuple-element.22), channel_id=1, source_target_pairs={{0,2},{1,3},{2,0},{3,1},{4,6},{5,7},{6,4},{7,5},{8,10},{9,11},{10,... | collective-permute-start | bytes 1474568 | tf_op jit(solution)/shard_map/ppermute | solution.py:19
  108.1 15.3 %collective-permute-start.25 = (bf16[320,768]{1,0:T(8,128)(2,1)S(1)}, bf16[320,768]{1,0:T(8,128)(2,1)S(1)}, u32[]{:S(2)}, u32[]{:S(2)}) collective-permute-start(bf16[320,768]{1,0:T(8,128)(2,1)S(1)} %get-tuple-element.23), channel_id=1, source_target_pairs={{0,6},{1,7},{2,4},{3,5},{4,2},{5,3},{6,0},{7,1},{8,14},{9,15},{10,... | collective-permute-start | bytes 1474568 | tf_op jit(solution)/shard_map/ppermute | solution.py:19
  110.9 16.7 %collective-permute-start.10 = (bf16[192,768]{1,0:T(8,128)(2,1)S(1)}, bf16[192,768]{1,0:T(8,128)(2,1)S(1)}, u32[]{:S(2)}, u32[]{:S(2)}) collective-permute-start(bf16[192,768]{1,0:T(8,128)(2,1)S(1)} %get-tuple-element.17), channel_id=1, source_target_pairs={{0,2},{1,3},{2,0},{3,1},{4,6},{5,7},{6,4},{7,5},{8,10},{9,11},{10,... | collective-permute-start | bytes 884744 | tf_op jit(solution)/shard_map/ppermute | solution.py:19
  112.2 17.5 %collective-permute-start.11 = (bf16[192,768]{1,0:T(8,128)(2,1)S(1)}, bf16[192,768]{1,0:T(8,128)(2,1)S(1)}, u32[]{:S(2)}, u32[]{:S(2)}) collective-permute-start(bf16[192,768]{1,0:T(8,128)(2,1)S(1)} %get-tuple-element.18), channel_id=1, source_target_pairs={{0,6},{1,7},{2,4},{3,5},{4,2},{5,3},{6,0},{7,1},{8,14},{9,15},{10,... | collective-permute-start | bytes 884744 | tf_op jit(solution)/shard_map/ppermute | solution.py:19
  124.2 10.8 %collective-permute-start.26 = (bf16[320,384]{1,0:T(8,128)(2,1)S(1)}, bf16[320,384]{1,0:T(8,128)(2,1)S(1)}, u32[]{:S(2)}, u32[]{:S(2)}) collective-permute-start(bf16[320,384]{1,0:T(8,128)(2,1)S(1)} %get-tuple-element.25), channel_id=1, source_target_pairs={{0,6},{1,7},{2,4},{3,5},{4,2},{5,3},{6,0},{7,1},{8,14},{9,15},{10,... | collective-permute-start | bytes 737288 | tf_op jit(solution)/shard_map/ppermute | solution.py:19
  125.9 9.1 %collective-permute-start.27 = (bf16[320,384]{1,0:T(8,128)(2,1)S(1)}, bf16[320,384]{1,0:T(8,128)(2,1)S(1)}, u32[]{:S(2)}, u32[]{:S(2)}) collective-permute-start(bf16[320,384]{1,0:T(8,128)(2,1)S(1)} %get-tuple-element.26), channel_id=1, source_target_pairs={{0,2},{1,3},{2,0},{3,1},{4,6},{5,7},{6,4},{7,5},{8,10},{9,11},{10,... | collective-permute-start | bytes 737288 | tf_op jit(solution)/shard_map/ppermute | solution.py:19
  130.7 6.6 %collective-permute-start.12 = (bf16[192,384]{1,0:T(8,128)(2,1)}, bf16[192,384]{1,0:T(8,128)(2,1)S(1)}, u32[]{:S(2)}, u32[]{:S(2)}) collective-permute-start(bf16[192,384]{1,0:T(8,128)(2,1)} %get-tuple-element.20), channel_id=1, source_target_pairs={{0,6},{1,7},{2,4},{3,5},{4,2},{5,3},{6,0},{7,1},{8,14},{9,15},{10,... | collective-permute-start | bytes 442376 | tf_op jit(solution)/shard_map/ppermute | solution.py:19
  139.7 35.5 %all-to-all-start.1 = ((bf16[32,48,384]{2,1,0:T(8,128)(2,1)}), bf16[32,48,384]{2,1,0:T(8,128)(2,1)S(1)}, u32[]{:S(2)}, u32[]{:S(2)}) async-start(bf16[32,48,384]{2,1,0:T(8,128)(2,1)} %bitcast.12), calls=%async_computation.1 | async-start | bytes 2359296 | tf_op jit(solution)/shard_map/all_to_all | solution.py:480
  (19 other events, 193.4 us)

commit v4 on v3

--- a/solution.py
+++ b/solution.py
@@ -9,7 +9,7 @@
 
 
 EPSILON = 1e-06
-FIRST_ROWS = 640
+FIRST_ROWS = 576
 F32 = jnp.float32
 BF16 = jnp.bfloat16
 
@@ -34,12 +34,13 @@
     return pl.BlockSpec(shape, lambda *_: (0,) * len(shape))
 
 
-def send_kernel(slots, where_ref, chosen_ref, stream_ref, gain_ref, out_ref, held, copied):
+def send_kernel(slots, chosen_ref, stream_ref, gain_ref, out_ref, held, copied):
     load = pltpu.make_async_copy(stream_ref, held, copied)
     load.start()
     tokens, _ = held.shape
     share = out_ref.shape[1]
-    column, base = where_ref[0], where_ref[1]
+    column = lax.axis_index("tp").astype(jnp.int32)
+    base = lax.axis_index("ep").astype(jnp.int32) * tokens
     chosen = chosen_ref[...]
     experts = chosen.shape[0]
     lane = lax.broadcasted_iota(jnp.int32, chosen.shape, 1)
@@ -87,28 +88,25 @@
     out_ref[...] = jnp.dot(placed, own, preferred_element_type=F32).astype(BF16)
 
 
-def outgoing_rows(where, chosen, stream, gain, slots, share):
+def outgoing_rows(chosen, stream, gain, slots, share):
     tokens, width = stream.shape
     experts = chosen.shape[0]
     return pl.pallas_call(
         functools.partial(send_kernel, slots),
-        grid_spec=pltpu.PrefetchScalarGridSpec(
-            num_scalar_prefetch=1,
-            grid=(1,),
-            in_specs=[
-                whole(chosen.shape),
-                pl.BlockSpec(memory_space=pltpu.MemorySpace.HBM),
-                whole(gain.shape),
-            ],
-            out_specs=whole((experts * slots, share)),
-            scratch_shapes=[pltpu.VMEM((tokens, width), BF16), pltpu.SemaphoreType.DMA],
-        ),
+        grid=(1,),
+        in_specs=[
+            whole(chosen.shape),
+            pl.BlockSpec(memory_space=pltpu.MemorySpace.HBM),
+            whole(gain.shape),
+        ],
+        out_specs=whole((experts * slots, share)),
+        scratch_shapes=[pltpu.VMEM((tokens, width), BF16), pltpu.SemaphoreType.DMA],
         out_shape=shape_of((experts * slots, share), BF16),
         cost_estimate=cost(
             2 * experts * slots * tokens * share, 2 * tokens * width + 2 * experts * slots * share
         ),
         name="send_rows",
-    )(where, chosen, stream, gain)
+    )(chosen, stream, gain)
 
 
 def compact_kernel(base, inv_ref, arrived_ref, out_ref):
@@ -131,6 +129,24 @@
         compiler_params=PARAMS,
         name="compact_rows",
     )(inv, arrived)
+
+
+def cut_kernel(near_ref, back_ref, low_ref, high_ref):
+    half = low_ref.shape[0]
+    low_ref[...] = near_ref[:half]
+    high_ref[...] = back_ref[half:]
+
+
+def halves_of(near, back):
+    rows, share = near.shape
+    half = shape_of((rows // 2, share), near.dtype)
+    return pl.pallas_call(
+        cut_kernel,
+        out_shape=[half, half],
+        cost_estimate=cost(0, 4 * rows * share),
+        compiler_params=PARAMS,
+        name="halves",
+    )(near, back)
 
 
 EARLY = (0, 1, 2, 3, 6, 7)
@@ -173,7 +189,7 @@
 def early_products(group, pieces, w_gate, w_up):
     picks, share = pieces[0].shape
     units = w_gate.shape[1]
-    tile = picks // 2
+    tile = picks
     n = len(EARLY)
     return pl.pallas_call(
         early_kernel,
@@ -225,7 +241,7 @@
 def down_products(group, hidden, w_down, core):
     picks, units = hidden.shape
     share = w_down.shape[1] // 8
-    tile = picks // 2
+    tile = picks
 
     def spec(mask):
         return pl.BlockSpec((units, share), lambda i, g: (0, g[0] ^ mask))
@@ -427,30 +443,35 @@
         axis=0,
         keepdims=True,
     )
-    weight = affinity.reshape(picks, 1)
 
     edges_of = (0, FIRST_ROWS, picks)
+    spans = list(zip(edges_of, edges_of[1:]))
+    weights = [affinity[0, low:high].reshape(-1, 1) for low, high in spans]
+    arrivals = [arrival[:, low:high] for low, high in spans]
     parts = len(edges_of) - 1
     gate_rows, up_rows, down_rows = w_gate[0], w_up[0], w_down[0]
     own_stream = lax.dynamic_slice_in_dim(stream, column * share, share, 1)
-    where = jnp.stack([column, base.astype(jnp.int32)])
-    outgoing = outgoing_rows(where, chosen, stream, ffn_gain.reshape(-1, 128), slots, share)
+    outgoing = outgoing_rows(chosen, stream, ffn_gain.reshape(-1, 128), slots, share)
     arrived = lax.all_to_all(
         outgoing.reshape(experts, slots, share), "ep", split_axis=0, concat_axis=0, tiled=True
     ).reshape(-1, share)
 
+    arrived, sel, inv, arrivals, weights, own_stream = lax.optimization_barrier(
+        (arrived, sel, inv, arrivals, weights, own_stream)
+    )
+
     def moved(array, mask):
         return exchanged(array, "tp", mask)
 
     keeps, cames, sends, leaving = [], [], [], []
     for part in range(parts):
         rows_from, rows_to = edges_of[part], edges_of[part + 1]
-        half = (rows_to - rows_from) // 2
         own = compacted(inv, arrived, rows_from, rows_to - rows_from)
         near = moved(own, 2)
         back = moved(own, 6)
-        far_low = moved(near[:half], 6)
-        far_high = moved(back[half:], 2)
+        low, high = halves_of(near, back)
+        far_low = moved(low, 6)
+        far_high = moved(high, 2)
         pieces = [own, moved(own, 1), near, moved(near, 1), back, moved(back, 1)]
         halves = [far_low, far_high, moved(far_low, 1), moved(far_high, 1)]
         acc = early_products(group, pieces, gate_rows, up_rows)
@@ -467,14 +488,7 @@
         b2 = moved(b_next, 2)
         leaving = [
             leaving_rows(
-                own_sum,
-                a2,
-                b2,
-                weight[edges_of[part] : edges_of[part + 1]],
-                arrival[:, edges_of[part] : edges_of[part + 1]],
-                leaving,
-                ep_count * slots,
-                share,
+                own_sum, a2, b2, weights[part], arrivals[part], leaving, ep_count * slots, share
             )
         ]
     returned = lax.all_to_all(

time: 188 us -> 178 us (0.947)
  blocking collectives: 0 us -> 36.5 us
  waiting for transfers between devices: 104 us -> 73.5 us
  starting transfers between devices: 42.6 us -> 35.8 us
  local copies, waits for them, and re-layouts: 5.69 us -> 2.08 us
  Pallas kernels: 28 us -> 25 us
  other arithmetic: 5.54 us -> 3.02 us
    all_to_all x0 -> x1, blocking collectives: none -> 36.5 us  [on_device(): lax.all_to_all(leaving[0].reshape(ep_count, slots, share), 'ep', split_ax...]
    all_to_all x1 -> x0, waiting for transfers between devices: 25.6 us -> none  [on_device(): lax.all_to_all(leaving[0].reshape(ep_count, slots, share), 'ep', split_ax...]
    all_to_all x1 -> x0, starting transfers between devices: 7.33 us -> none  [on_device(): lax.all_to_all(leaving[0].reshape(ep_count, slots, share), 'ep', split_ax...]
    ppermute x32, waiting for transfers between devices: 53.7 us -> 47.2 us  [exchanged(): return lax.ppermute(array, axis, [(i, i ^ mask) for i in range(devices)])]
    pallas_call x1 -> x3, Pallas kernels: 4.94 us -> 4.36 us  [the longest x1 4.29 us: outgoing_rows(): pl.pallas_call(functools.partial(send_kernel, slots), grid=(1,), in_specs...]
  transfers between devices with their start and end apart: 34 -> 33, of which waited for: 19 -> 18; matrix products, arithmetic and copies ran while one was open for 4% -> 2% of each run, Pallas kernels for 8% -> 10%
where the time goes in v4:
time: 178 us; the launch traced here: 176 us
  waiting for transfers between devices  73.5 us (41%)
  blocking collectives  36.5 us (21%)
  starting transfers between devices  35.8 us (20%)
  Pallas kernels  25 us (14%)
  other arithmetic  3.02 us (2%)
  local copies, waits for them, and re-layouts  2.08 us (1%)
    ppermute x32, waiting for transfers between devices, exchanged(): return lax.ppermute(array, axis, [(i, i ^ mask) for i in range(devices)])  47.2 us
    all_to_all x1, blocking collectives, on_device(): lax.all_to_all(leaving[0].reshape(ep_count, slots, share), 'ep', split_ax...  36.5 us
    all_to_all x1, waiting for transfers between devices, on_device(): lax.all_to_all(outgoing.reshape(experts, slots, share), 'ep', split_axis=...  26.3 us
    ppermute x32, starting transfers between devices, exchanged(): return lax.ppermute(array, axis, [(i, i ^ mask) for i in range(devices)])  24.5 us
    all_to_all x1, starting transfers between devices, on_device(): lax.all_to_all(outgoing.reshape(experts, slots, share), 'ep', split_axis=...  11.3 us
    pallas_call x2, Pallas kernels, early_products(): pl.pallas_call(early_kernel, grid_spec=pltpu.PrefetchScalarGridSpec(num_s...  5.19 us
    pallas_call x1, Pallas kernels, outgoing_rows(): pl.pallas_call(functools.partial(send_kernel, slots), grid=(1,), in_specs...  4.29 us
    pallas_call x4, Pallas kernels, down_products(): pl.pallas_call(down_kernel, grid_spec=pltpu.PrefetchScalarGridSpec(num_sc...  4.16 us
  transfers between devices with their start and end apart: 33, of which 18 were waited for; matrix products, arithmetic and copies ran while one was open for 2% of the time, Pallas kernels for 10%

profile of v4, /device:TPU:32, one launch (start us, length us, event | category | flops | bytes accessed | tf_op | source)
XLA Modules:
  0.0 176.4 jit_solution(17137487523405836218)
XLA Ops:
  0.0 4.3 %send_rows.1 = bf16[1536,384]{1,0:T(8,128)(2,1)} custom-call(s32[32,1024]{1,0:T(8,128)} %chosen_ref.1, bf16[256,3072]{1,0:T(8,128)(2,1)} %stream_ref.1, bf16[24,128]{1,0:T(8,128)(2,1)} %bitcast.74), custom_call_target="tpu_custom_call" | custom-call | flops 301989888 | bytes 2752512 | tf_op jit(solution)/shard_map/send_rows/pallas_call | solution.py:94
  4.3 11.3 %all-to-all-start = ((bf16[32,48,384]{2,1,0:T(8,128)(2,1)}), bf16[32,48,384]{2,1,0:T(8,128)(2,1)S(1)}, u32[]{:S(2)}, u32[]{:S(2)}) async-start(bf16[32,48,384]{2,1,0:T(8,128)(2,1)} %bitcast.69), calls=%async_computation | async-start | bytes 2359296 | tf_op jit(solution)/shard_map/all_to_all | solution.py:455
  19.3 26.3 %all-to-all-done = bf16[32,48,384]{2,1,0:T(8,128)(2,1)S(1)} async-done(((bf16[32,48,384]{2,1,0:T(8,128)(2,1)}), bf16[32,48,384]{2,1,0:T(8,128)(2,1)S(1)}, u32[]{:S(2)}, u32[]{:S(2)}) %all-to-all-start) | async-done | bytes 1179680 | tf_op jit(solution)/shard_map/all_to_all | solution.py:455
  48.6 2.2 %collective-permute-start.15 = (bf16[576,384]{1,0:T(8,128)(2,1)S(1)}, bf16[576,384]{1,0:T(8,128)(2,1)S(1)}, u32[]{:S(2)}, u32[]{:S(2)}) collective-permute-start(bf16[576,384]{1,0:T(8,128)(2,1)S(1)} %compact_rows.3.refs_0_), channel_id=1, source_target_pairs={{0,6},{1,7},{2,4},{3,5},{4,2},{5,3},{6,0},{7,1},{8,14},{9,15},{10,... | collective-permute-start | bytes 1327112 | tf_op jit(solution)/shard_map/ppermute | solution.py:19
  50.8 6.2 %collective-permute-done.14.near_ref.refs_2_ = bf16[576,384]{1,0:T(8,128)(2,1)S(1)} collective-permute-done((bf16[576,384]{1,0:T(8,128)(2,1)S(1)}, bf16[576,384]{1,0:T(8,128)(2,1)S(1)}, u32[]{:S(2)}, u32[]{:S(2)}) %collective-permute-start.14) | collective-permute-done | bytes 442400 | tf_op jit(solution)/shard_map/ppermute | solution.py:19
  57.0 2.5 %collective-permute-done.15.back_ref.refs_4_ = bf16[576,384]{1,0:T(8,128)(2,1)S(1)} collective-permute-done((bf16[576,384]{1,0:T(8,128)(2,1)S(1)}, bf16[576,384]{1,0:T(8,128)(2,1)S(1)}, u32[]{:S(2)}, u32[]{:S(2)}) %collective-permute-start.15) | collective-permute-done | bytes 442400 | tf_op jit(solution)/shard_map/ppermute | solution.py:19
  59.6 2.3 %collective-permute-start.16 = (bf16[288,384]{1,0:T(8,128)(2,1)S(1)}, bf16[288,384]{1,0:T(8,128)(2,1)S(1)}, u32[]{:S(2)}, u32[]{:S(2)}) collective-permute-start(bf16[288,384]{1,0:T(8,128)(2,1)S(1)} %get-tuple-element.42), channel_id=1, source_target_pairs={{0,6},{1,7},{2,4},{3,5},{4,2},{5,3},{6,0},{7,1},{8,14},{9,15},{10,... | collective-permute-start | bytes 663560 | tf_op jit(solution)/shard_map/ppermute | solution.py:19
  61.9 6.9 %collective-permute-done.16.low = bf16[288,384]{1,0:T(8,128)(2,1)S(1)} collective-permute-done((bf16[288,384]{1,0:T(8,128)(2,1)S(1)}, bf16[288,384]{1,0:T(8,128)(2,1)S(1)}, u32[]{:S(2)}, u32[]{:S(2)}) %collective-permute-start.16) | collective-permute-done | bytes 221216 | tf_op jit(solution)/shard_map/ppermute | solution.py:19
  70.9 1.8 %collective-permute-start.1 = (bf16[448,384]{1,0:T(8,128)(2,1)S(1)}, bf16[448,384]{1,0:T(8,128)(2,1)S(1)}, u32[]{:S(2)}, u32[]{:S(2)}) collective-permute-start(bf16[448,384]{1,0:T(8,128)(2,1)S(1)} %compact_rows.2.refs_0_), channel_id=1, source_target_pairs={{0,6},{1,7},{2,4},{3,5},{4,2},{5,3},{6,0},{7,1},{8,14},{9,15},{10,... | collective-permute-start | bytes 1032200 | tf_op jit(solution)/shard_map/ppermute | solution.py:19
  72.7 2.9 %gate_up_early.3.acc_ref = f32[576,768]{1,0:T(8,128)S(1)} custom-call(s32[1]{0:T(128)} %bitcast.7.group_ref, bf16[576,384]{1,0:T(8,128)(2,1)S(1)} %compact_rows.3.refs_0_, bf16[576,384]{1,0:T(8,128)(2,1)S(1)} %collective-permute-done.20.refs_1_, bf16[576,384]{1,0:T(8,128)(2,1)S(1)} %collective-permute-done.14.near_ref.refs_2_, ...), custom_call_target="tpu_custom_call" | custom-call | flops 2038431744 | bytes 6193152 | tf_op jit(solution)/shard_map/gate_up_early/pallas_call | solution.py:194
  79.0 2.0 %collective-permute-done.near_ref.refs_2_ = bf16[448,384]{1,0:T(8,128)(2,1)S(1)} collective-permute-done((bf16[448,384]{1,0:T(8,128)(2,1)S(1)}, bf16[448,384]{1,0:T(8,128)(2,1)S(1)}, u32[]{:S(2)}, u32[]{:S(2)}) %collective-permute-start) | collective-permute-done | bytes 344096 | tf_op jit(solution)/shard_map/ppermute | solution.py:19
  84.0 6.5 %collective-permute-done.2.low = bf16[224,384]{1,0:T(8,128)(2,1)S(1)} collective-permute-done((bf16[224,384]{1,0:T(8,128)(2,1)S(1)}, bf16[224,384]{1,0:T(8,128)(2,1)S(1)}, u32[]{:S(2)}, u32[]{:S(2)}) %collective-permute-start.2) | collective-permute-done | bytes 172064 | tf_op jit(solution)/shard_map/ppermute | solution.py:19
  91.0 2.3 %gate_up_early.2.acc_ref = f32[448,768]{1,0:T(8,128)S(1)} custom-call(s32[1]{0:T(128)} %bitcast.7.group_ref, bf16[448,384]{1,0:T(8,128)(2,1)S(1)} %compact_rows.2.refs_0_, bf16[448,384]{1,0:T(8,128)(2,1)S(1)} %collective-permute-done.6.refs_1_, bf16[448,384]{1,0:T(8,128)(2,1)S(1)} %collective-permute-done.near_ref.refs_2_, ...), custom_call_target="tpu_custom_call" | custom-call | flops 1585446912 | bytes 5603328 | tf_op jit(solution)/shard_map/gate_up_early/pallas_call | solution.py:194
  97.8 1.7 collective-permute-start.25
  103.6 7.0 %collective-permute-done.24.a2.low2 = bf16[288,768]{1,0:T(8,128)(2,1)S(1)} collective-permute-done((bf16[288,768]{1,0:T(8,128)(2,1)S(1)}, bf16[288,768]{1,0:T(8,128)(2,1)S(1)}, u32[]{:S(2)}, u32[]{:S(2)}) %collective-permute-start.24) | collective-permute-done | bytes 442400 | tf_op jit(solution)/shard_map/ppermute | solution.py:19
  112.7 1.8 %collective-permute-start.26 = (bf16[288,384]{1,0:T(8,128)(2,1)S(1)}, bf16[288,384]{1,0:T(8,128)(2,1)S(1)}, u32[]{:S(2)}, u32[]{:S(2)}) collective-permute-start(bf16[288,384]{1,0:T(8,128)(2,1)S(1)} %get-tuple-element.47), channel_id=1, source_target_pairs={{0,6},{1,7},{2,4},{3,5},{4,2},{5,3},{6,0},{7,1},{8,14},{9,15},{10,... | collective-permute-start | bytes 663560 | tf_op jit(solution)/shard_map/ppermute | solution.py:19
  114.5 3.3 %collective-permute-done.10.a2.low2 = bf16[224,768]{1,0:T(8,128)(2,1)S(1)} collective-permute-done((bf16[224,768]{1,0:T(8,128)(2,1)S(1)}, bf16[224,768]{1,0:T(8,128)(2,1)S(1)}, u32[]{:S(2)}, u32[]{:S(2)}) %collective-permute-start.10) | collective-permute-done | bytes 344096 | tf_op jit(solution)/shard_map/ppermute | solution.py:19
  120.4 1.7 collective-permute-start.12
  123.7 1.8 %leave_rows.2.refs_0_ = bf16[1536,384]{1,0:T(8,128)(2,1)S(1)} custom-call(f32[576,384]{1,0:T(8,128)S(1)} %get-tuple-element.46.own_ref, bf16[288,384]{1,0:T(8,128)(2,1)S(1)} %collective-permute-done.26.a2, bf16[288,384]{1,0:T(8,128)(2,1)S(1)} %collective-permute-done.27.b2, f32[576,1]{1,0:T(8,128)S(1)} %copy.11.weight_ref, s32[1,576]{1,0:T(1,128)S(1)} %slice.16.arrival_ref), custom_call_target="tpu_custom_call" | custom-call | flops 679477248 | bytes 2949120 | tf_op jit(solution)/shard_map/leave_rows/pallas_call | solution.py:365
  125.5 1.8 %collective-permute-done.12.a2 = bf16[224,384]{1,0:T(8,128)(2,1)S(1)} collective-permute-done((bf16[224,384]{1,0:T(8,128)(2,1)}, bf16[224,384]{1,0:T(8,128)(2,1)S(1)}, u32[]{:S(2)}, u32[]{:S(2)}) %collective-permute-start.12) | collective-permute-done | bytes 172064 | tf_op jit(solution)/shard_map/ppermute | solution.py:19
  129.3 36.5 %all_to_all.10 = bf16[32,48,384]{2,1,0:T(8,128)(2,1)S(1)} all-to-all(bf16[32,48,384]{2,1,0:T(8,128)(2,1)S(1)} %bitcast.65), channel_id=1, replica_groups=mesh['ep'=32,'tp'=8] {'ep'}, dimensions={0} | all-to-all | bytes 2359296 | tf_op jit(solution)/shard_map/all_to_all | solution.py:494
  167.8 1.7 collective-permute-start.29
  170.8 1.7 collective-permute-start.31
  172.5 2.0 %collective-permute-done.30 = f32[1,256]{1,0:T(1,128)S(1)} collective-permute-done((f32[1,256]{1,0:T(1,128)S(1)}, f32[1,256]{1,0:T(1,128)S(1)}, u32[]{:S(2)}, u32[]{:S(2)}) %collective-permute-start.30) | collective-permute-done | bytes 1056 | tf_op jit(solution)/shard_map/ppermute | solution.py:19
  (102 shorter events, 37.4 us)
Async XLA Ops:
  4.3 41.3 %all-to-all-start = ((bf16[32,48,384]{2,1,0:T(8,128)(2,1)}), bf16[32,48,384]{2,1,0:T(8,128)(2,1)S(1)}, u32[]{:S(2)}, u32[]{:S(2)}) async-start(bf16[32,48,384]{2,1,0:T(8,128)(2,1)} %bitcast.69), calls=%async_computation | async-start | bytes 2359296 | tf_op jit(solution)/shard_map/all_to_all | solution.py:455
  46.9 10.1 %collective-permute-start.14 = (bf16[576,384]{1,0:T(8,128)(2,1)S(1)}, bf16[576,384]{1,0:T(8,128)(2,1)S(1)}, u32[]{:S(2)}, u32[]{:S(2)}) collective-permute-start(bf16[576,384]{1,0:T(8,128)(2,1)S(1)} %compact_rows.3.refs_0_), channel_id=1, source_target_pairs={{0,2},{1,3},{2,0},{3,1},{4,6},{5,7},{6,4},{7,5},{8,10},{9,11},{10,... | collective-permute-start | bytes 1327112 | tf_op jit(solution)/shard_map/ppermute | solution.py:19
  48.6 10.9 %collective-permute-start.15 = (bf16[576,384]{1,0:T(8,128)(2,1)S(1)}, bf16[576,384]{1,0:T(8,128)(2,1)S(1)}, u32[]{:S(2)}, u32[]{:S(2)}) collective-permute-start(bf16[576,384]{1,0:T(8,128)(2,1)S(1)} %compact_rows.3.refs_0_), channel_id=1, source_target_pairs={{0,6},{1,7},{2,4},{3,5},{4,2},{5,3},{6,0},{7,1},{8,14},{9,15},{10,... | collective-permute-start | bytes 1327112 | tf_op jit(solution)/shard_map/ppermute | solution.py:19
  50.8 19.7 %collective-permute-start.20 = (bf16[576,384]{1,0:T(8,128)(2,1)S(1)}, bf16[576,384]{1,0:T(8,128)(2,1)S(1)}, u32[]{:S(2)}, u32[]{:S(2)}) collective-permute-start(bf16[576,384]{1,0:T(8,128)(2,1)S(1)} %compact_rows.3.refs_0_), channel_id=1, source_target_pairs={{0,1},{1,0},{2,3},{3,2},{4,5},{5,4},{6,7},{7,6},{8,9},{9,8},{10,11... | collective-permute-start | bytes 1327112 | tf_op jit(solution)/shard_map/ppermute | solution.py:19
  57.0 13.8 %collective-permute-start.21 = (bf16[576,384]{1,0:T(8,128)(2,1)S(1)}, bf16[576,384]{1,0:T(8,128)(2,1)S(1)}, u32[]{:S(2)}, u32[]{:S(2)}) collective-permute-start(bf16[576,384]{1,0:T(8,128)(2,1)S(1)} %collective-permute-done.14.near_ref.refs_2_), channel_id=1, source_target_pairs={{0,1},{1,0},{2,3},{3,2},{4,5},{5,4},{6,7},{7,6},{8,9},{9,8},{10,11... | collective-permute-start | bytes 1327112 | tf_op jit(solution)/shard_map/ppermute | solution.py:19
  59.5 13.2 %collective-permute-start.22 = (bf16[576,384]{1,0:T(8,128)(2,1)S(1)}, bf16[576,384]{1,0:T(8,128)(2,1)S(1)}, u32[]{:S(2)}, u32[]{:S(2)}) collective-permute-start(bf16[576,384]{1,0:T(8,128)(2,1)S(1)} %collective-permute-done.15.back_ref.refs_4_), channel_id=1, source_target_pairs={{0,1},{1,0},{2,3},{3,2},{4,5},{5,4},{6,7},{7,6},{8,9},{9,8},{10,11... | collective-permute-start | bytes 1327112 | tf_op jit(solution)/shard_map/ppermute | solution.py:19
  59.6 9.1 %collective-permute-start.16 = (bf16[288,384]{1,0:T(8,128)(2,1)S(1)}, bf16[288,384]{1,0:T(8,128)(2,1)S(1)}, u32[]{:S(2)}, u32[]{:S(2)}) collective-permute-start(bf16[288,384]{1,0:T(8,128)(2,1)S(1)} %get-tuple-element.42), channel_id=1, source_target_pairs={{0,6},{1,7},{2,4},{3,5},{4,2},{5,3},{6,0},{7,1},{8,14},{9,15},{10,... | collective-permute-start | bytes 663560 | tf_op jit(solution)/shard_map/ppermute | solution.py:19
  61.8 7.6 %collective-permute-start.17 = (bf16[288,384]{1,0:T(8,128)(2,1)S(1)}, bf16[288,384]{1,0:T(8,128)(2,1)S(1)}, u32[]{:S(2)}, u32[]{:S(2)}) collective-permute-start(bf16[288,384]{1,0:T(8,128)(2,1)S(1)} %get-tuple-element.43), channel_id=1, source_target_pairs={{0,2},{1,3},{2,0},{3,1},{4,6},{5,7},{6,4},{7,5},{8,10},{9,11},{10,... | collective-permute-start | bytes 663560 | tf_op jit(solution)/shard_map/ppermute | solution.py:19
  68.7 6.9 %collective-permute-start.18 = (bf16[288,384]{1,0:T(8,128)(2,1)S(1)}, bf16[288,384]{1,0:T(8,128)(2,1)S(1)}, u32[]{:S(2)}, u32[]{:S(2)}) collective-permute-start(bf16[288,384]{1,0:T(8,128)(2,1)S(1)} %collective-permute-done.16.low), channel_id=1, source_target_pairs={{0,1},{1,0},{2,3},{3,2},{4,5},{5,4},{6,7},{7,6},{8,9},{9,8},{10,11... | collective-permute-start | bytes 663560 | tf_op jit(solution)/shard_map/ppermute | solution.py:19
  70.5 10.6 %collective-permute-start = (bf16[448,384]{1,0:T(8,128)(2,1)S(1)}, bf16[448,384]{1,0:T(8,128)(2,1)S(1)}, u32[]{:S(2)}, u32[]{:S(2)}) collective-permute-start(bf16[448,384]{1,0:T(8,128)(2,1)S(1)} %compact_rows.2.refs_0_), channel_id=1, source_target_pairs={{0,2},{1,3},{2,0},{3,1},{4,6},{5,7},{6,4},{7,5},{8,10},{9,11},{10,... | collective-permute-start | bytes 1032200 | tf_op jit(solution)/shard_map/ppermute | solution.py:19
  70.9 11.5 %collective-permute-start.1 = (bf16[448,384]{1,0:T(8,128)(2,1)S(1)}, bf16[448,384]{1,0:T(8,128)(2,1)S(1)}, u32[]{:S(2)}, u32[]{:S(2)}) collective-permute-start(bf16[448,384]{1,0:T(8,128)(2,1)S(1)} %compact_rows.2.refs_0_), channel_id=1, source_target_pairs={{0,6},{1,7},{2,4},{3,5},{4,2},{5,3},{6,0},{7,1},{8,14},{9,15},{10,... | collective-permute-start | bytes 1032200 | tf_op jit(solution)/shard_map/ppermute | solution.py:19
  72.7 11.3 %collective-permute-start.6 = (bf16[448,384]{1,0:T(8,128)(2,1)S(1)}, bf16[448,384]{1,0:T(8,128)(2,1)S(1)}, u32[]{:S(2)}, u32[]{:S(2)}) collective-permute-start(bf16[448,384]{1,0:T(8,128)(2,1)S(1)} %compact_rows.2.refs_0_), channel_id=1, source_target_pairs={{0,1},{1,0},{2,3},{3,2},{4,5},{5,4},{6,7},{7,6},{8,9},{9,8},{10,11... | collective-permute-start | bytes 1032200 | tf_op jit(solution)/shard_map/ppermute | solution.py:19
  78.4 18.2 %collective-permute-start.23 = (bf16[576,1536]{1,0:T(8,128)(2,1)S(1)}, bf16[576,1536]{1,0:T(8,128)(2,1)S(1)}, u32[]{:S(2)}, u32[]{:S(2)}) collective-permute-start(bf16[576,1536]{1,0:T(8,128)(2,1)S(1)} %down.7), channel_id=1, source_target_pairs={{0,1},{1,0},{2,3},{3,2},{4,5},{5,4},{6,7},{7,6},{8,9},{9,8},{10,11... | collective-permute-start | bytes 5308424 | tf_op jit(solution)/shard_map/ppermute | solution.py:19
  81.0 10.0 %collective-permute-start.7 = (bf16[448,384]{1,0:T(8,128)(2,1)S(1)}, bf16[448,384]{1,0:T(8,128)(2,1)S(1)}, u32[]{:S(2)}, u32[]{:S(2)}) collective-permute-start(bf16[448,384]{1,0:T(8,128)(2,1)S(1)} %collective-permute-done.near_ref.refs_2_), channel_id=1, source_target_pairs={{0,1},{1,0},{2,3},{3,2},{4,5},{5,4},{6,7},{7,6},{8,9},{9,8},{10,11... | collective-permute-start | bytes 1032200 | tf_op jit(solution)/shard_map/ppermute | solution.py:19
  82.4 8.6 %collective-permute-start.8 = (bf16[448,384]{1,0:T(8,128)(2,1)S(1)}, bf16[448,384]{1,0:T(8,128)(2,1)S(1)}, u32[]{:S(2)}, u32[]{:S(2)}) collective-permute-start(bf16[448,384]{1,0:T(8,128)(2,1)S(1)} %collective-permute-done.1.back_ref.refs_4_), channel_id=1, source_target_pairs={{0,1},{1,0},{2,3},{3,2},{4,5},{5,4},{6,7},{7,6},{8,9},{9,8},{10,11... | collective-permute-start | bytes 1032200 | tf_op jit(solution)/shard_map/ppermute | solution.py:19
  82.4 8.1 %collective-permute-start.2 = (bf16[224,384]{1,0:T(8,128)(2,1)S(1)}, bf16[224,384]{1,0:T(8,128)(2,1)S(1)}, u32[]{:S(2)}, u32[]{:S(2)}) collective-permute-start(bf16[224,384]{1,0:T(8,128)(2,1)S(1)} %get-tuple-element.33), channel_id=1, source_target_pairs={{0,6},{1,7},{2,4},{3,5},{4,2},{5,3},{6,0},{7,1},{8,14},{9,15},{10,... | collective-permute-start | bytes 516104 | tf_op jit(solution)/shard_map/ppermute | solution.py:19
  84.0 6.5 %collective-permute-start.3 = (bf16[224,384]{1,0:T(8,128)(2,1)S(1)}, bf16[224,384]{1,0:T(8,128)(2,1)S(1)}, u32[]{:S(2)}, u32[]{:S(2)}) collective-permute-start(bf16[224,384]{1,0:T(8,128)(2,1)S(1)} %get-tuple-element.34), channel_id=1, source_target_pairs={{0,2},{1,3},{2,0},{3,1},{4,6},{5,7},{6,4},{7,5},{8,10},{9,11},{10,... | collective-permute-start | bytes 516104 | tf_op jit(solution)/shard_map/ppermute | solution.py:19
  97.2 13.3 %collective-permute-start.24 = (bf16[288,768]{1,0:T(8,128)(2,1)S(1)}, bf16[288,768]{1,0:T(8,128)(2,1)S(1)}, u32[]{:S(2)}, u32[]{:S(2)}) collective-permute-start(bf16[288,768]{1,0:T(8,128)(2,1)S(1)} %get-tuple-element.44), channel_id=1, source_target_pairs={{0,2},{1,3},{2,0},{3,1},{4,6},{5,7},{6,4},{7,5},{8,10},{9,11},{10,... | collective-permute-start | bytes 1327112 | tf_op jit(solution)/shard_map/ppermute | solution.py:19
  97.8 14.3 %collective-permute-start.25 = (bf16[288,768]{1,0:T(8,128)(2,1)S(1)}, bf16[288,768]{1,0:T(8,128)(2,1)S(1)}, u32[]{:S(2)}, u32[]{:S(2)}) collective-permute-start(bf16[288,768]{1,0:T(8,128)(2,1)S(1)} %get-tuple-element.45), channel_id=1, source_target_pairs={{0,6},{1,7},{2,4},{3,5},{4,2},{5,3},{6,0},{7,1},{8,14},{9,15},{10,... | collective-permute-start | bytes 1327112 | tf_op jit(solution)/shard_map/ppermute | solution.py:19
  100.8 17.1 %collective-permute-start.10 = (bf16[224,768]{1,0:T(8,128)(2,1)S(1)}, bf16[224,768]{1,0:T(8,128)(2,1)S(1)}, u32[]{:S(2)}, u32[]{:S(2)}) collective-permute-start(bf16[224,768]{1,0:T(8,128)(2,1)S(1)} %get-tuple-element.35), channel_id=1, source_target_pairs={{0,2},{1,3},{2,0},{3,1},{4,6},{5,7},{6,4},{7,5},{8,10},{9,11},{10,... | collective-permute-start | bytes 1032200 | tf_op jit(solution)/shard_map/ppermute | solution.py:19
  102.1 17.3 %collective-permute-start.11 = (bf16[224,768]{1,0:T(8,128)(2,1)S(1)}, bf16[224,768]{1,0:T(8,128)(2,1)S(1)}, u32[]{:S(2)}, u32[]{:S(2)}) collective-permute-start(bf16[224,768]{1,0:T(8,128)(2,1)S(1)} %get-tuple-element.36), channel_id=1, source_target_pairs={{0,6},{1,7},{2,4},{3,5},{4,2},{5,3},{6,0},{7,1},{8,14},{9,15},{10,... | collective-permute-start | bytes 1032200 | tf_op jit(solution)/shard_map/ppermute | solution.py:19
  112.7 11.0 %collective-permute-start.26 = (bf16[288,384]{1,0:T(8,128)(2,1)S(1)}, bf16[288,384]{1,0:T(8,128)(2,1)S(1)}, u32[]{:S(2)}, u32[]{:S(2)}) collective-permute-start(bf16[288,384]{1,0:T(8,128)(2,1)S(1)} %get-tuple-element.47), channel_id=1, source_target_pairs={{0,6},{1,7},{2,4},{3,5},{4,2},{5,3},{6,0},{7,1},{8,14},{9,15},{10,... | collective-permute-start | bytes 663560 | tf_op jit(solution)/shard_map/ppermute | solution.py:19
  114.5 9.2 %collective-permute-start.27 = (bf16[288,384]{1,0:T(8,128)(2,1)S(1)}, bf16[288,384]{1,0:T(8,128)(2,1)S(1)}, u32[]{:S(2)}, u32[]{:S(2)}) collective-permute-start(bf16[288,384]{1,0:T(8,128)(2,1)S(1)} %get-tuple-element.48), channel_id=1, source_target_pairs={{0,2},{1,3},{2,0},{3,1},{4,6},{5,7},{6,4},{7,5},{8,10},{9,11},{10,... | collective-permute-start | bytes 663560 | tf_op jit(solution)/shard_map/ppermute | solution.py:19
  120.4 6.8 %collective-permute-start.12 = (bf16[224,384]{1,0:T(8,128)(2,1)}, bf16[224,384]{1,0:T(8,128)(2,1)S(1)}, u32[]{:S(2)}, u32[]{:S(2)}) collective-permute-start(bf16[224,384]{1,0:T(8,128)(2,1)} %get-tuple-element.38), channel_id=1, source_target_pairs={{0,6},{1,7},{2,4},{3,5},{4,2},{5,3},{6,0},{7,1},{8,14},{9,15},{10,... | collective-permute-start | bytes 516104 | tf_op jit(solution)/shard_map/ppermute | solution.py:19
  (15 other events, 162.4 us)
